TPU v7x, 512 devices: a whole 4x8x8 slice. The times are simulated.
512 devices in a mesh: sp: 32 (over z, x), tp: 16 (over y, core).
Axes of the slice: x: 4, y: 8, z: 8, core: 2. Of those that a mesh axis runs over, the one named last changes fastest.
Arguments:
- residual: bfloat16 [8192, 2048], P('sp', 'tp'), may hold values from -6 to 6
- queries: bfloat16 [8192, 1024], P('sp', 'tp'), may hold values from -5.5 to 5.5
- keys: bfloat16 [8192, 128], P('sp'), may hold values from -5.5 to 5.5
- values: bfloat16 [8192, 128], P('sp'), may hold values from -6 to 6
- documents: int32 [8192], P('sp'), may hold values from 0 to 15, never falling along the last dimension, each value on 1 to 1024 neighbouring positions
- sinks: float32 [16], P('tp'), may hold values from 1 to 6
- head_gain: float32 [1024], replicated, may hold values from 0.1 to 1.9
- out_weight: bfloat16 [1024, 2048], P(None, 'tp'), may hold values from -0.1875 to 0.1875
- norm_gain: float32 [2048], P('tp'), may hold values from 0.1 to 1.9
- norm_shift: float32 [2048], P('tp'), may hold values from -3 to 3
- routes: int32 [8192, 2], P('sp'), may hold values from 0 to 31, all different within a row; in each aligned block of 256 rows (0 to 255, 256 to 511, ...) at most 24 rows name the same one
- route_logits: float32 [8192, 2], P('sp'), may hold values from -150 to 150
- gate_weight: bfloat16 [32, 2048, 6144], P('sp', None, 'tp'), may hold values from -0.125 to 0.125
- up_weight: bfloat16 [32, 2048, 6144], P('sp', None, 'tp'), may hold values from -0.125 to 0.125
- down_weight: bfloat16 [32, 6144, 2048], P('sp', 'tp'), may hold values from -0.15625 to 0.15625
- final_gain: float32 [2048], P('tp'), may hold values from 0.1 to 1.9
- final_shift: float32 [2048], P('tp'), may hold values from -3 to 3
Outputs:
- layer_out: bfloat16 [8192, 2048], P('sp', 'tp')
Inputs may be any that keep to these rules, and one draw needn't show every extreme that they name: `documents`: document numbers never fall along the sequence; each document has at least one position and at most 1024, and some document has exactly 1024. `routes`: each row names 2 different experts. In each aligned block of 256 rows (the rows of one index of sp) no expert is named by more than 24 rows, a bound that some block reaches.
All inputs are finite; a program needn't handle non-finite values.
Results may differ from a plain program's by a relative error of at most 0.014.
Values may be sent and summed in bfloat16 or wider, within the bound.
No kernel may reach another device: no remote copies, remote signals or barrier semaphores. Data moves between devices by JAX's collectives and lax.ppermute only.
A program may use at most 128 MiB of HBM per device.

v0:
```python
import jax
import jax.numpy as jnp
from jax import lax
from jax.sharding import PartitionSpec as P

D = 2048
QUERY_HEADS = 16
KEY_VALUE_HEADS = 2
HEAD_SIZE = 64
WINDOW_SIZE = 128
TOP = 2


DEEP_ALPHA = 8.0**0.25
NORM_EPS = 1e-05


def sent_to_all(value, axis):
    length = lax.axis_size(axis)
    return lax.all_to_all(
        jnp.broadcast_to(value[None], (length, *value.shape)), axis, 0, 0, tiled=True
    )


def over_copies(value, axis):
    return sent_to_all(value, axis).sum(axis=0)


def in_one(arrays, axis):
    line, at, gathered = (jnp.concatenate([a.reshape(-1) for a in arrays]), 0, [])
    total = over_copies(line, axis)
    for a in arrays:
        gathered.append(total[at : at + a.size].reshape(a.shape))
        at += a.size
    return tuple(gathered)


def shifted(block, axis, distance):
    devices = range(lax.axis_size(axis))
    route = [(i - distance, i) for i in devices if i - distance in devices]
    return lax.ppermute(block, axis, route)


def split_norm(total, gain, shift):
    totals = in_one((jnp.sum(total, axis=1), jnp.sum(total * total, axis=1)), "tp")
    center = totals[0] / D
    spread = totals[1] / D - center * center
    return (total - center[:, None]) * lax.rsqrt(spread + NORM_EPS)[:, None] * gain + shift


def expert_rows(arrived, gate_weight, up_weight, down_weight):
    sources, count, width = arrived.shape
    flat_rows = arrived.reshape(sources * count, width)
    gate = jnp.dot(flat_rows, gate_weight[0], preferred_element_type=jnp.float32)
    up_val = jnp.dot(flat_rows, up_weight[0], preferred_element_type=jnp.float32)
    middle = (jax.nn.silu(gate) * up_val).astype(jnp.bfloat16)
    share_out = jnp.dot(middle, down_weight[0], preferred_element_type=jnp.float32).astype(
        jnp.bfloat16
    )
    groups = lax.axis_size("tp")
    pieces = share_out.reshape(sources, count, groups, width // groups)
    traded = lax.all_to_all(pieces, "tp", split_axis=2, concat_axis=2, tiled=True)
    summed = jnp.sum(traded.astype(jnp.float32), axis=2)
    return lax.all_to_all(
        summed.astype(jnp.bfloat16), "sp", split_axis=0, concat_axis=0, tiled=True
    )


def pack_rows(source_rows, table, expert_count, capacity):
    padded = jnp.concatenate(
        [source_rows, jnp.zeros((1, source_rows.shape[1]), source_rows.dtype)], axis=0
    )
    return padded[table].reshape(expert_count, capacity, source_rows.shape[1])


def local(
    residual,
    queries,
    keys,
    values,
    documents,
    sinks,
    head_gain,
    out_weight,
    norm_gain,
    norm_shift,
    routes,
    route_logits,
    gate_weight,
    up_weight,
    down_weight,
    final_gain,
    final_shift,
):
    tokens = queries.shape[0]
    head_list = sinks.shape[0]
    tails = shifted(
        (
            keys[tokens - WINDOW_SIZE :],
            values[tokens - WINDOW_SIZE :],
            documents[tokens - WINDOW_SIZE :].astype(jnp.bfloat16),
        ),
        "sp",
        1,
    )
    offset = lax.axis_index("sp") * tokens
    shared_key_head = lax.axis_index("tp") * head_list // (QUERY_HEADS // KEY_VALUE_HEADS)
    all_keys = jnp.concatenate([tails[0], keys], axis=0)
    all_values = jnp.concatenate([tails[1], values], axis=0)
    all_docs = jnp.concatenate([tails[2].astype(jnp.int32), documents], axis=0)
    key_head = lax.dynamic_slice_in_dim(all_keys, shared_key_head * HEAD_SIZE, HEAD_SIZE, 1)
    value_head = lax.dynamic_slice_in_dim(all_values, shared_key_head * HEAD_SIZE, HEAD_SIZE, 1)
    query_heads = queries.reshape(tokens, head_list, HEAD_SIZE)
    scores = jnp.einsum(
        "qhd,kd->hqk", query_heads, key_head, preferred_element_type=jnp.float32
    ) * HEAD_SIZE ** (-0.5)
    query_pos = offset + jnp.arange(tokens, dtype=jnp.int32)
    key_pos = offset - WINDOW_SIZE + jnp.arange(tokens + WINDOW_SIZE, dtype=jnp.int32)
    distance = query_pos[:, None] - key_pos[None, :]
    allowed = (
        (distance >= 0)
        & (distance < WINDOW_SIZE)
        & (key_pos[None, :] >= 0)
        & (documents[:, None] == all_docs[None, :])
    )
    scores = jnp.where(allowed[None], scores, -jnp.inf)
    sink_col = sinks[:, None]
    top = jnp.maximum(jnp.max(scores, axis=2), sink_col)
    expd = jnp.exp(scores - top[..., None])
    probs = (expd / (jnp.sum(expd, axis=2) + jnp.exp(sink_col - top))[..., None]).astype(
        jnp.bfloat16
    )
    attended = jnp.einsum("hqk,kd->qhd", probs, value_head, preferred_element_type=jnp.float32)
    attended = attended.astype(jnp.bfloat16).reshape(tokens, head_list * HEAD_SIZE)
    all_heads = lax.all_gather(attended, "tp", axis=1, tiled=True).astype(jnp.float32)
    scaled = (
        all_heads
        * lax.rsqrt(jnp.mean(all_heads * all_heads, axis=1, keepdims=True) + NORM_EPS)
        * head_gain
    ).astype(jnp.bfloat16)
    mix = jnp.dot(scaled, out_weight, preferred_element_type=jnp.float32)
    first = DEEP_ALPHA * residual.astype(jnp.float32) + mix
    hidden = split_norm(first, norm_gain, norm_shift)
    hidden_rows = hidden.astype(jnp.bfloat16)
    expert_count = lax.axis_size("sp")
    capacity = 3 * tokens * TOP // (2 * expert_count)
    flat = routes.reshape(-1)
    onehot = (flat[:, None] == jnp.arange(expert_count, dtype=jnp.int32)[None, :]).astype(jnp.int32)
    rank = jnp.sum(jnp.cumsum(onehot, axis=0) * onehot, axis=1) - 1
    target = flat * capacity + rank
    owner = jnp.arange(tokens * TOP, dtype=jnp.int32) // TOP
    table = jnp.full((expert_count * capacity,), tokens, jnp.int32).at[target].set(owner)
    outgoing = pack_rows(hidden_rows, table, expert_count, capacity)
    joined = lax.all_gather(
        lax.all_to_all(outgoing, "sp", split_axis=0, concat_axis=0, tiled=True),
        "tp",
        axis=2,
        tiled=True,
    )
    returned = expert_rows(joined, gate_weight, up_weight, down_weight)
    picked = (
        returned.reshape(expert_count * capacity, -1)[target]
        .reshape(tokens, TOP, -1)
        .astype(jnp.float32)
    )
    share = jax.nn.softmax(route_logits, axis=-1)
    moe = jnp.sum(share[:, :, None] * picked, axis=1)
    second = DEEP_ALPHA * hidden + moe
    return split_norm(second, final_gain, final_shift).astype(jnp.bfloat16)


def solution(mesh):
    return jax.shard_map(
        local,
        mesh=mesh,
        in_specs=(
            P("sp", "tp"),
            P("sp", "tp"),
            P("sp", None),
            P("sp", None),
            P("sp"),
            P("tp"),
            P(),
            P(None, "tp"),
            P("tp"),
            P("tp"),
            P("sp", None),
            P("sp", None),
            P("sp", None, "tp"),
            P("sp", None, "tp"),
            P("sp", "tp", None),
            P("tp"),
            P("tp"),
        ),
        out_specs=P("sp", "tp"),
        check_vma=False,
    )
```

profile of v0, /device:TPU:1, one launch (start us, length us, event | category | flops | bytes accessed | tf_op | source)
XLA Modules:
  0.0 268.2 jit_solution(7688286295900288744)
XLA Ops:
  6.5 0.9 slice.30
  7.4 3.9 %collective-permute-start.2 = (bf16[128,128]{1,0:T(8,128)(2,1)S(1)}, bf16[128,128]{1,0:T(8,128)(2,1)S(1)}, u32[]{:S(2)}, u32[]{:S(2)}) collective-permute-start(bf16[128,128]{1,0:T(8,128)(2,1)S(1)} %slice.30), channel_id=1, source_target_pairs={{0,16},{16,32},{32,48},{48,64},{64,80},{80,96},{96,112},{112,128},... | collective-permute-start | bytes 98312 | tf_op jit(solution)/shard_map/ppermute | solution.py:41
  11.4 0.7 convert.5
  12.0 3.1 %collective-permute-start.1 = (bf16[128]{0:T(256)(128)(2,1)S(1)}, bf16[128]{0:T(256)(128)(2,1)S(1)}, u32[]{:S(2)}, u32[]{:S(2)}) collective-permute-start(bf16[128]{0:T(256)(128)(2,1)S(1)} %slice.29), channel_id=1, source_target_pairs={{0,16},{16,32},{32,48},{48,64},{64,80},{80,96},{96,112},{112,128},... | collective-permute-start | bytes 776 | tf_op jit(solution)/shard_map/ppermute | solution.py:41
  15.2 0.8 slice.28
  15.9 2.8 %collective-permute-start = (bf16[128,128]{1,0:T(8,128)(2,1)S(1)}, bf16[128,128]{1,0:T(8,128)(2,1)S(1)}, u32[]{:S(2)}, u32[]{:S(2)}) collective-permute-start(bf16[128,128]{1,0:T(8,128)(2,1)S(1)} %slice.28), channel_id=1, source_target_pairs={{0,16},{16,32},{32,48},{48,64},{64,80},{80,96},{96,112},{112,128},... | collective-permute-start | bytes 98312 | tf_op jit(solution)/shard_map/ppermute | solution.py:41
  18.8 0.8 copy.39
  19.9 0.7 broadcast_multiply_fusion
  20.6 1.2 reduce-window.6
  22.5 2.4 scatter_custom_fusion
  25.6 0.7 pad_add_fusion
  26.3 1.2 fusion.55
  28.0 20.4 %all-gather = bf16[256,1,1024]{0,2,1:T(8,128)(2,1)S(1)} all-gather(bf16[256,1,64]{0,2,1:T(8,128)(2,1)S(1)} %fusion.14), channel_id=2, replica_groups=mesh['sp'=32,'tp'=16] {'tp'}, dimensions={2}, use_global_device_ids=true | all-gather | bytes 557056 | tf_op jit(solution)/shard_map/all_gather | solution.py:135
  48.6 0.7 fusion.54
  49.2 0.6 broadcast_in_dim.13
  49.9 4.5 %all-to-all-start = ((f32[16,1,512]{2,1,0:T(1,128)}), f32[16,1,512]{2,1,0:T(1,128)S(1)}, u32[]{:S(2)}, u32[]{:S(2)}) async-start(f32[16,1,512]{2,1,0:T(1,128)} %broadcast_in_dim.13), calls=%async_computation | async-start | bytes 65536 | tf_op jit(solution)/shard_map/all_to_all | solution.py:20
  54.4 7.3 %all-to-all-done = f32[16,1,512]{2,1,0:T(1,128)S(1)} async-done(((f32[16,1,512]{2,1,0:T(1,128)}), f32[16,1,512]{2,1,0:T(1,128)S(1)}, u32[]{:S(2)}, u32[]{:S(2)}) %all-to-all-start) | async-done | bytes 32800 | tf_op jit(solution)/shard_map/all_to_all | solution.py:20
  62.0 1.9 gather_fusion
  63.9 23.3 %all_to_all.27 = bf16[32,24,128]{2,1,0:T(8,128)(2,1)} all-to-all(bf16[32,24,128]{2,1,0:T(8,128)(2,1)S(1)} %bitcast.72), channel_id=1, replica_groups=mesh['sp'=32,'tp'=16] {'sp'}, dimensions={0} | all-to-all | bytes 393216 | tf_op jit(solution)/shard_map/all_to_all | solution.py:155
  87.2 39.9 %all-gather.3.cloned.1.call-done = bf16[32,24,2048]{2,1,0:T(8,128)(2,1)} async-done(((bf16[32,24,128]{2,1,0:T(8,128)(2,1)}), bf16[32,24,2048]{2,1,0:T(8,128)(2,1)}) %all-gather.3.cloned.1.call-update) | async-done | bytes 3145744 | tf_op jit(solution)/shard_map/all_gather | solution.py:154
  127.1 5.3 %fusion.4 = f32[768,384]{1,0:T(8,128)} fusion(bf16[768,2048]{1,0:T(8,128)(2,1)} %bitcast.77, bf16[1,2048,384]{2,1,0:T(8,128)(2,1)} %param.29), kind=kOutput, calls=%fused_computation.8 | convolution fusion | flops 1207959552 | bytes 5898240 | tf_op jit(solution)/shard_map/dot_general | solution.py:54
  132.4 7.4 %fusion = bf16[96,8,16,128]{3,1,2,0:T(8,128)(2,1)} fusion(bf16[1,384,2048]{2,1,0:T(8,128)(2,1)S(1)} %copy-done, bf16[768,2048]{1,0:T(8,128)(2,1)} %bitcast.78, bf16[1,2048,384]{2,1,0:T(8,128)(2,1)S(1)} %copy-done.7, f32[768,384]{1,0:T(8,128)} %fusion.4), kind=kOutput, calls=%fused_computation.4 | convolution fusion | flops 2419261440 | bytes 10616832 | tf_op jit(solution)/shard_map/dot_general | solution.py:57
  139.7 2.9 %copy.51 = bf16[96,8,16,128]{3,2,1,0:T(8,128)(2,1)S(1)} copy(bf16[96,8,16,128]{3,1,2,0:T(8,128)(2,1)} %fusion) | data formatting | bytes 6291456
  142.6 2.5 copy.42
  145.2 4.6 %all-to-all-start.2 = ((bf16[32,24,16,128]{3,1,0,2:T(8,128)(2,1)}), bf16[32,24,16,128]{3,1,0,2:T(8,128)(2,1)}, u32[]{:S(2)}, u32[]{:S(2)}) async-start(bf16[32,24,16,128]{3,1,0,2:T(8,128)(2,1)} %copy.42), calls=%async_computation.2 | async-start | bytes 6291456 | tf_op jit(solution)/shard_map/all_to_all | solution.py:62
  149.8 71.1 %all-to-all-done.2 = bf16[32,24,16,128]{3,1,0,2:T(8,128)(2,1)} async-done(((bf16[32,24,16,128]{3,1,0,2:T(8,128)(2,1)}), bf16[32,24,16,128]{3,1,0,2:T(8,128)(2,1)}, u32[]{:S(2)}, u32[]{:S(2)}) %all-to-all-start.2) | async-done | bytes 3145760 | tf_op jit(solution)/shard_map/all_to_all | solution.py:62
  220.9 3.1 %reduce_sum.118 = bf16[32,24,128]{2,1,0:T(8,128)(2,1)} reduce(bf16[32,24,16,128]{3,1,0,2:T(8,128)(2,1)} %all-to-all-done.2, bf16[]{:T(256)} %constant.87.clone.1), dimensions={2}, to_apply=%region_12.13 | reduce | flops 1474560 | bytes 3342338 | tf_op jit(solution)/shard_map/reduce_sum | solution.py:63
  223.9 9.7 %all-to-all-start.3 = ((bf16[32,24,128]{2,1,0:T(8,128)(2,1)}), bf16[32,24,128]{2,1,0:T(8,128)(2,1)S(1)}, u32[]{:S(2)}, u32[]{:S(2)}) async-start(bf16[32,24,128]{2,1,0:T(8,128)(2,1)} %reduce_sum.118), calls=%async_computation.3 | async-start | bytes 393216 | tf_op jit(solution)/shard_map/all_to_all | solution.py:64
  233.9 9.7 %all-to-all-done.3 = bf16[32,24,128]{2,1,0:T(8,128)(2,1)S(1)} async-done(((bf16[32,24,128]{2,1,0:T(8,128)(2,1)}), bf16[32,24,128]{2,1,0:T(8,128)(2,1)S(1)}, u32[]{:S(2)}, u32[]{:S(2)}) %all-to-all-start.3) | async-done | bytes 196640 | tf_op jit(solution)/shard_map/all_to_all | solution.py:64
  243.6 1.3 gather_fusion.1
  245.6 14.9 %all_to_all.28 = f32[16,1,512]{2,1,0:T(1,128)S(1)} all-to-all(f32[16,1,512]{2,1,0:T(1,128)S(1)} %broadcast_in_dim.16), channel_id=1, replica_groups=mesh['sp'=32,'tp'=16] {'tp'}, dimensions={0} | all-to-all | bytes 65536 | tf_op jit(solution)/shard_map/all_to_all | solution.py:20
  260.6 0.8 add_convert_fusion
  (68 shorter events, 2.8 us)
Async XLA Ops:
  6.5 125.8 %copy-start = (bf16[1,384,2048]{2,1,0:T(8,128)(2,1)S(1)}, bf16[1,384,2048]{2,1,0:T(8,128)(2,1)}, u32[]{:S(2)}) copy-start(bf16[1,384,2048]{2,1,0:T(8,128)(2,1)} %param.31) | copy-start | bytes 4718596
  6.5 21.1 %copy-start.2 = (bf16[256,128]{1,0:T(8,128)(2,1)S(1)}, bf16[256,128]{1,0:T(8,128)(2,1)}, u32[]{:S(2)}) copy-start(bf16[256,128]{1,0:T(8,128)(2,1)} %param.20) | copy-start | bytes 196612
  7.4 18.9 %collective-permute-start.2 = (bf16[128,128]{1,0:T(8,128)(2,1)S(1)}, bf16[128,128]{1,0:T(8,128)(2,1)S(1)}, u32[]{:S(2)}, u32[]{:S(2)}) collective-permute-start(bf16[128,128]{1,0:T(8,128)(2,1)S(1)} %slice.30), channel_id=1, source_target_pairs={{0,16},{16,32},{32,48},{48,64},{64,80},{80,96},{96,112},{112,128},... | collective-permute-start | bytes 98312 | tf_op jit(solution)/shard_map/ppermute | solution.py:41
  12.0 13.5 %collective-permute-start.1 = (bf16[128]{0:T(256)(128)(2,1)S(1)}, bf16[128]{0:T(256)(128)(2,1)S(1)}, u32[]{:S(2)}, u32[]{:S(2)}) collective-permute-start(bf16[128]{0:T(256)(128)(2,1)S(1)} %slice.29), channel_id=1, source_target_pairs={{0,16},{16,32},{32,48},{48,64},{64,80},{80,96},{96,112},{112,128},... | collective-permute-start | bytes 776 | tf_op jit(solution)/shard_map/ppermute | solution.py:41
  15.9 11.7 %collective-permute-start = (bf16[128,128]{1,0:T(8,128)(2,1)S(1)}, bf16[128,128]{1,0:T(8,128)(2,1)S(1)}, u32[]{:S(2)}, u32[]{:S(2)}) collective-permute-start(bf16[128,128]{1,0:T(8,128)(2,1)S(1)} %slice.28), channel_id=1, source_target_pairs={{0,16},{16,32},{32,48},{48,64},{64,80},{80,96},{96,112},{112,128},... | collective-permute-start | bytes 98312 | tf_op jit(solution)/shard_map/ppermute | solution.py:41
  27.5 21.0 %copy-start.8 = (bf16[1024,128]{1,0:T(8,128)(2,1)S(1)}, bf16[1024,128]{1,0:T(8,128)(2,1)}, u32[]{:S(2)}) copy-start(bf16[1024,128]{1,0:T(8,128)(2,1)} %param.24) | copy-start | bytes 786436
  27.5 21.0 %copy-start.9 = (bf16[256,128]{1,0:T(8,128)(2,1)S(1)}, bf16[256,128]{1,0:T(8,128)(2,1)}, u32[]{:S(2)}) copy-start(bf16[256,128]{1,0:T(8,128)(2,1)} %param.17) | copy-start | bytes 196612
  27.5 21.0 %copy-start.10 = (f32[1024]{0:T(1024)S(1)}, f32[1024]{0:T(1024)}, u32[]{:S(2)}) copy-start(f32[1024]{0:T(1024)} %param.23) | copy-start | bytes 12292
  27.9 33.9 %copy-start.3 = (f32[128]{0:T(128)S(1)}, f32[128]{0:T(128)}, u32[]{:S(2)}) copy-start(f32[128]{0:T(128)} %param.26) | copy-start | bytes 1540
  28.0 33.8 %copy-start.4 = (f32[128]{0:T(128)S(1)}, f32[128]{0:T(128)}, u32[]{:S(2)}) copy-start(f32[128]{0:T(128)} %param.25) | copy-start | bytes 1540
  49.9 11.9 %all-to-all-start = ((f32[16,1,512]{2,1,0:T(1,128)}), f32[16,1,512]{2,1,0:T(1,128)S(1)}, u32[]{:S(2)}, u32[]{:S(2)}) async-start(f32[16,1,512]{2,1,0:T(1,128)} %broadcast_in_dim.13), calls=%async_computation | async-start | bytes 65536 | tf_op jit(solution)/shard_map/all_to_all | solution.py:20
  54.4 72.7 %all-gather.3.cloned.1.call-start = ((), (), s32[]{:S(2)}) async-start(), calls=%async_computation.5 | async-start | bytes 3342336 | tf_op jit(solution)/shard_map/all_gather | solution.py:154
  127.1 5.3 %copy-start.7 = (bf16[1,2048,384]{2,1,0:T(8,128)(2,1)S(1)}, bf16[1,2048,384]{2,1,0:T(8,128)(2,1)}, u32[]{:S(2)}) copy-start(bf16[1,2048,384]{2,1,0:T(8,128)(2,1)} %param.30) | copy-start | bytes 4718596
  145.2 4.6 %copy-start.1 = (f32[256,2]{0,1:T(2,128)S(1)}, f32[256,2]{0,1:T(2,128)}, u32[]{:S(2)}) copy-start(f32[256,2]{0,1:T(2,128)} %param.28) | copy-start | bytes 6148
  145.2 75.7 %all-to-all-start.2 = ((bf16[32,24,16,128]{3,1,0,2:T(8,128)(2,1)}), bf16[32,24,16,128]{3,1,0,2:T(8,128)(2,1)}, u32[]{:S(2)}, u32[]{:S(2)}) async-start(bf16[32,24,16,128]{3,1,0,2:T(8,128)(2,1)} %copy.42), calls=%async_computation.2 | async-start | bytes 6291456 | tf_op jit(solution)/shard_map/all_to_all | solution.py:62
  223.9 36.6 %copy-start.5 = (f32[128]{0:T(128)S(1)}, f32[128]{0:T(128)}, u32[]{:S(2)}) copy-start(f32[128]{0:T(128)} %param.33) | copy-start | bytes 1540
  223.9 36.6 %copy-start.6 = (f32[128]{0:T(128)S(1)}, f32[128]{0:T(128)}, u32[]{:S(2)}) copy-start(f32[128]{0:T(128)} %param.32) | copy-start | bytes 1540
  223.9 19.6 %all-to-all-start.3 = ((bf16[32,24,128]{2,1,0:T(8,128)(2,1)}), bf16[32,24,128]{2,1,0:T(8,128)(2,1)S(1)}, u32[]{:S(2)}, u32[]{:S(2)}) async-start(bf16[32,24,128]{2,1,0:T(8,128)(2,1)} %reduce_sum.118), calls=%async_computation.3 | async-start | bytes 393216 | tf_op jit(solution)/shard_map/all_to_all | solution.py:64
Sparse Core Ops, SparseCore 0:
  87.3 39.7 all-gather.2
where the time goes:
time: 269 us; the launch traced here: 268 us
  waiting for transfers between devices  128 us (48%)
  blocking collectives  58.5 us (22%)
  starting transfers between devices  28.7 us (11%)
  local copies, waits for them, and re-layouts  15.2 us (6%)
  matrix products  14.8 us (6%)
  between operations  14.4 us (5%)
  other arithmetic  8.54 us (3%)
    all_to_all x1, waiting for transfers between devices, expert_rows(): lax.all_to_all(pieces, 'tp', split_axis=2, concat_axis=2, tiled=True)  71.1 us
    all_gather x1, waiting for transfers between devices, local(): lax.all_gather(lax.all_to_all(outgoing, 'sp', split_axis=0, concat_axis=0...  39.9 us
    all_to_all x1, blocking collectives, local(): lax.all_to_all(outgoing, 'sp', split_axis=0, concat_axis=0, tiled=True)  23.3 us
    all_gather x1, blocking collectives, local(): lax.all_gather(attended, 'tp', axis=1, tiled=True).astype(jnp.float32)  20.4 us
    all_to_all x1, blocking collectives, sent_to_all(): lax.all_to_all(jnp.broadcast_to(value[None], (length, *value.shape)), axi...  14.9 us
    ppermute x3, starting transfers between devices, shifted(): return lax.ppermute(block, axis, route)  9.84 us
    all_to_all x1, starting transfers between devices, expert_rows(): lax.all_to_all(summed.astype(jnp.bfloat16), 'sp', split_axis=0, concat_ax...  9.73 us
    all_to_all x1, waiting for transfers between devices, expert_rows(): lax.all_to_all(summed.astype(jnp.bfloat16), 'sp', split_axis=0, concat_ax...  9.68 us
  transfers between devices with their start and end apart: 7, of which 4 were waited for; matrix products, arithmetic and copies ran while one was open for 4% of the time, Pallas kernels for 0%

commit v1 on v0

v1 whole, which is shorter than its diff:
```python
import functools

import jax
import jax.numpy as jnp
from jax import lax
from jax.experimental import pallas as pl
from jax.experimental.pallas import tpu as pltpu
from jax.sharding import Mesh, PartitionSpec as P

D = 2048
QUERY_HEADS = 16
KEY_VALUE_HEADS = 2
HEAD_SIZE = 64
WINDOW = 128
TOP = 2
TOKENS = 256
CAP = 24
N_SP = 32
N_TP = 16
SLOTS = N_SP * CAP
FF_LOCAL = 384
LANES = 128
STAT_ROWS = 8
ROWS = SLOTS + STAT_ROWS
ROW_TILE = 256

DEEP_ALPHA = 8.0**0.25
NORM_EPS = 1e-05

SP = ("z", "x")
TP = ("y", "c")
Y = 8

f32 = jnp.float32
bf16 = jnp.bfloat16


def eye():
    return lax.broadcasted_iota(jnp.int32, (LANES, LANES), 0) == lax.broadcasted_iota(
        jnp.int32, (LANES, LANES), 1
    )


def column(row):
    return jnp.sum(jnp.where(eye(), row, jnp.zeros_like(row)), axis=1, keepdims=True)


def row_of(col):
    return jnp.sum(jnp.where(eye(), col, jnp.zeros_like(col)), axis=0, keepdims=True)


def nt(a, b):
    return lax.dot_general(a, b, (((1,), (1,)), ((), ())), preferred_element_type=f32)


def high_low(v):
    high = v.astype(bf16).astype(f32)
    return high, v - high


def attention_kernel(
    sinks_ref, halo_ref, keys_ref, values_ref, queries_ref, docs_ref, residual_ref,
    weight_ref, gain_ref, shift_ref, out_ref,
):
    kv_head = (lax.axis_index("y") * 2 + lax.axis_index("c")) // (QUERY_HEADS // KEY_VALUE_HEADS)
    first_block = (lax.axis_index("z") * 4 + lax.axis_index("x")) == 0
    sink = sinks_ref[0]
    pick = kv_head == 0

    def head_of(block):
        return jnp.where(pick, block[:, :HEAD_SIZE], block[:, HEAD_SIZE:])

    keys = [head_of(halo_ref[:WINDOW, :LANES].astype(f32)).astype(bf16)]
    vals = [head_of(halo_ref[:WINDOW, LANES:].astype(f32)).astype(bf16)]
    for i in range(2):
        part = slice(i * WINDOW, (i + 1) * WINDOW)
        keys.append(head_of(keys_ref[part, :].astype(f32)).astype(bf16))
        vals.append(head_of(values_ref[part, :].astype(f32)).astype(bf16))
    docs = docs_ref[...].astype(f32)
    halo_docs = halo_ref[WINDOW : WINDOW + 8, :LANES].astype(f32)[0:1]
    halo_docs = jnp.where(first_block, -1.0, halo_docs)
    doc_rows = [halo_docs, docs[:, :WINDOW], docs[:, WINDOW:]]
    qi = lax.broadcasted_iota(jnp.int32, (WINDOW, WINDOW), 0)
    ki = lax.broadcasted_iota(jnp.int32, (WINDOW, WINDOW), 1)
    blocks = []
    for i in range(2):
        q = queries_ref[i * WINDOW : (i + 1) * WINDOW, :]
        q_docs = column(doc_rows[i + 1])
        before = nt(q, keys[i]) * HEAD_SIZE ** (-0.5)
        here = nt(q, keys[i + 1]) * HEAD_SIZE ** (-0.5)
        before = jnp.where((ki > qi) & (q_docs == doc_rows[i]), before, -jnp.inf)
        here = jnp.where((ki <= qi) & (q_docs == doc_rows[i + 1]), here, -jnp.inf)
        top = jnp.maximum(
            jnp.maximum(
                jnp.max(before, axis=1, keepdims=True), jnp.max(here, axis=1, keepdims=True)
            ),
            sink,
        )
        before, here = jnp.exp(before - top), jnp.exp(here - top)
        total = (
            jnp.sum(before, axis=1, keepdims=True)
            + jnp.sum(here, axis=1, keepdims=True)
            + jnp.exp(sink - top)
        )
        before = (before / total).astype(bf16)
        here = (here / total).astype(bf16)
        blocks.append(
            jnp.dot(before, vals[i], preferred_element_type=f32)
            + jnp.dot(here, vals[i + 1], preferred_element_type=f32)
        )
    attended = jnp.concatenate(blocks, axis=1).astype(bf16)
    ones = jnp.ones((8, LANES), bf16)
    means = nt(ones, residual_ref[...])[0:1]
    w_sums = nt(ones, weight_ref[...])[0:1]
    rows = [means[:, :LANES], means[:, LANES:]]
    rows += [w_sums[:, i * LANES : (i + 1) * LANES] for i in range(8)]
    rows += [*high_low(gain_ref[...]), *high_low(shift_ref[...])]
    rows += [jnp.zeros((2, LANES), f32)]
    tail = jnp.concatenate(rows, axis=0).astype(bf16)
    for t in range(N_TP):
        out_ref[t, :WINDOW, :] = attended
        out_ref[t, WINDOW:, :] = tail


def mix_kernel(
    gathered_ref, head_gain_ref, weight_ref, residual_ref, routes_ref,
    first_ref, outgoing_ref, stats_ref, slots_ref, affine_ref,
):
    tails = [gathered_ref[t, WINDOW:, :].astype(f32) for t in range(N_TP)]
    total = functools.reduce(jnp.add, tails)
    for t in range(N_TP):
        lanes = slice(t * LANES, (t + 1) * LANES)
        affine_ref[0:1, lanes] = tails[t][10:11] + tails[t][11:12]
        affine_ref[1:2, lanes] = tails[t][12:13] + tails[t][13:14]
    w_mean = jnp.concatenate([total[2 + i : 3 + i] for i in range(8)], axis=1)
    head_gain = head_gain_ref[...]
    firsts = []
    for h in range(2):
        lanes = slice(h * HEAD_SIZE, (h + 1) * HEAD_SIZE)
        heads = jnp.concatenate(
            [gathered_ref[t, :WINDOW, lanes].astype(f32) for t in range(N_TP)], axis=1
        )
        spread = jnp.mean(heads * heads, axis=1, keepdims=True)
        scaled = (heads * lax.rsqrt(spread + NORM_EPS) * head_gain).astype(bf16)
        mix = jnp.dot(scaled, weight_ref[...], preferred_element_type=f32)
        center = DEEP_ALPHA * column(total[h : h + 1]) + jnp.sum(
            scaled.astype(f32) * w_mean, axis=1, keepdims=True
        )
        rows = slice(h * LANES, (h + 1) * LANES)
        first = DEEP_ALPHA * residual_ref[rows, :].astype(f32) + mix - center * (1.0 / D)
        first_ref[rows, :] = first
        firsts.append(first)
    sums = [row_of(jnp.sum(f, axis=1, keepdims=True)) for f in firsts]
    squares = [row_of(jnp.sum(f * f, axis=1, keepdims=True)) for f in firsts]
    parts = [high_low(v) for v in sums + squares]
    stats_ref[...] = jnp.concatenate(
        [p[0] for p in parts] + [p[1] for p in parts], axis=0
    ).astype(bf16)
    routes = routes_ref[...]
    expert = lax.broadcasted_iota(jnp.int32, (N_SP, TOKENS), 0)
    picks = [expert == routes[r : r + 1, :] for r in range(TOP)]
    named = (picks[0] | picks[1]).astype(f32).astype(bf16)
    earlier = (
        lax.broadcasted_iota(jnp.int32, (TOKENS, TOKENS), 0)
        < lax.broadcasted_iota(jnp.int32, (TOKENS, TOKENS), 1)
    ).astype(f32).astype(bf16)
    rank = jnp.dot(named, earlier, preferred_element_type=f32)
    slots = [
        routes[r : r + 1, :] * CAP
        + jnp.sum(jnp.where(picks[r], rank, 0.0), axis=0, keepdims=True).astype(jnp.int32)
        for r in range(TOP)
    ]
    slots_ref[...] = jnp.concatenate(slots + [jnp.zeros((6, TOKENS), jnp.int32)], axis=0)
    slot = lax.broadcasted_iota(jnp.int32, (SLOTS, TOKENS), 0)
    place = ((slot == slots[0]) | (slot == slots[1])).astype(f32).astype(bf16)
    source = jnp.concatenate(firsts, axis=0).astype(bf16)
    outgoing_ref[...] = jnp.dot(place, source, preferred_element_type=f32).astype(bf16)


def expert_kernel(
    own_ref, mine_ref, other_ref, affine_ref, gate_ref, up_ref, down_ref,
    keep_ref, send_ref, rows_ref, out_ref,
):
    y, c = lax.axis_index("y"), lax.axis_index("c")
    way = 1 - 2 * c

    def lanes_of(chip, half):
        return pl.ds(pl.multiple_of((lax.rem(chip + 2 * Y, Y) * 2 + half) * LANES, LANES), LANES)

    blocks = [(own_ref, h, lanes_of(y, h)) for h in range(2)]
    for k in range(1, 4):
        for h in range(2):
            blocks.append((mine_ref, 2 * k - 2 + h, lanes_of(y - way * k, h)))
            blocks.append((other_ref, 2 * k - 2 + h, lanes_of(y + way * k, h)))
    blocks.append((mine_ref, 6, lanes_of(y + 4, c)))
    blocks.append((other_ref, 6, lanes_of(y + 4, 1 - c)))
    total = square = 0.0
    for ref, i, _ in blocks:
        v = ref[i].astype(f32)
        total = total + v
        square = square + v * v
    center = jnp.sum(total, axis=1, keepdims=True) * (1.0 / D)
    spread = jnp.sum(square, axis=1, keepdims=True) * (1.0 / D) - center * center
    scale = lax.rsqrt(spread + NORM_EPS)
    offset = center * scale
    for ref, i, lanes in blocks:
        v = ref[i].astype(f32) * scale - offset
        rows_ref[:, lanes] = (v * affine_ref[0:1, lanes] + affine_ref[1:2, lanes]).astype(bf16)
    gate = jnp.dot(rows_ref[...], gate_ref[...], preferred_element_type=f32)
    up = jnp.dot(rows_ref[...], up_ref[...], preferred_element_type=f32)
    middle = (gate / (1.0 + jnp.exp(-gate)) * up).astype(bf16)
    out_ref[...] = jnp.dot(middle, down_ref[...], preferred_element_type=f32)
    for k in range(1, 4):
        for h in range(2):
            keep_ref[2 * k - 2 + h] = out_ref[:, lanes_of(y + way * k, h)].astype(bf16)
            send_ref[2 * k - 2 + h] = out_ref[:, lanes_of(y - way * k, h)].astype(bf16)
    keep_ref[6] = out_ref[:, lanes_of(y + 4, c)].astype(bf16)
    send_ref[6] = out_ref[:, lanes_of(y + 4, 1 - c)].astype(bf16)
    keep_ref[7] = out_ref[:, lanes_of(y, c)].astype(bf16)
    send_ref[7] = out_ref[:, lanes_of(y, 1 - c)].astype(bf16)


def combine_kernel(
    returned_ref, first_ref, totals_ref, slots_ref, logits_ref, gain_ref, shift_ref,
    second_ref, stats_ref,
):
    totals = totals_ref[...]
    totals = totals[0:4] + totals[4:8]
    sums, squares = [], []
    for h in range(2):
        rows = slice(h * LANES, (h + 1) * LANES)
        center = column(totals[h : h + 1]) * (1.0 / D)
        spread = column(totals[2 + h : 3 + h]) * (1.0 / D) - center * center
        hidden = (first_ref[rows, :] - center) * lax.rsqrt(spread + NORM_EPS)
        hidden = hidden * gain_ref[...] + shift_ref[...]
        slot = lax.broadcasted_iota(jnp.int32, (LANES, SLOTS), 1).astype(f32)
        logits = [column(logits_ref[r : r + 1, rows]) for r in range(TOP)]
        top = jnp.maximum(logits[0], logits[1])
        weights = [jnp.exp(v - top) for v in logits]
        norm = weights[0] + weights[1]
        moe = 0.0
        for r in range(TOP):
            at = column(slots_ref[r : r + 1, rows].astype(f32))
            place = (slot == at).astype(f32).astype(bf16)
            picked = jnp.dot(place, returned_ref[...], preferred_element_type=f32)
            moe = moe + weights[r] / norm * picked
        second = DEEP_ALPHA * hidden + moe
        second_ref[rows, :] = second
        sums.append(row_of(jnp.sum(second, axis=1, keepdims=True)))
        squares.append(row_of(jnp.sum(second * second, axis=1, keepdims=True)))
    stats = jnp.concatenate(sums + squares + [jnp.zeros((4, LANES), f32)], axis=0)
    for t in range(N_TP):
        stats_ref[t] = stats


def norm_kernel(stats_ref, second_ref, gain_ref, shift_ref, out_ref):
    totals = functools.reduce(jnp.add, [stats_ref[t] for t in range(N_TP)])
    for h in range(2):
        rows = slice(h * LANES, (h + 1) * LANES)
        center = column(totals[h : h + 1]) * (1.0 / D)
        spread = column(totals[2 + h : 3 + h]) * (1.0 / D) - center * center
        out = (second_ref[rows, :] - center) * lax.rsqrt(spread + NORM_EPS)
        out_ref[rows, :] = (out * gain_ref[...] + shift_ref[...]).astype(bf16)


def call(kernel, outs, flops, moved, **more):
    return pl.pallas_call(
        kernel,
        out_shape=outs,
        cost_estimate=pl.CostEstimate(flops=flops, bytes_accessed=moved, transcendentals=0),
        compiler_params=pltpu.CompilerParams(vmem_limit_bytes=48 * 1024 * 1024),
        **more,
    )


def shape(dims, dtype):
    return jax.ShapeDtypeStruct(dims, dtype)


def swap(v):
    return lax.ppermute(v, "c", [(0, 1), (1, 0)])


def onward(v, distance):
    pairs = []
    for y in range(Y):
        pairs.append((2 * y, 2 * ((y + distance) % Y)))
        pairs.append((2 * y + 1, 2 * ((y - distance) % Y) + 1))
    return lax.ppermute(v, TP, pairs)


def by_core(even, odd):
    return jnp.where(lax.axis_index("c") == 0, even, odd)


def to_all(value):
    return lax.all_to_all(value, TP, 0, 0, tiled=True)


def over_sp(value):
    return lax.all_to_all(value, SP, 0, 0, tiled=True)


def gather_columns(block):
    partner = swap(block)
    own = by_core(jnp.stack([block, partner]), jnp.stack([partner, block]))
    two = onward(own, 2)
    one = onward(own, 1)
    three = onward(two, 1)
    four = onward(by_core(two[0:1], two[1:2]), 2)
    mine = jnp.concatenate([one, two, three, four], axis=0)
    return own, mine, swap(mine)


def scatter_sum(keep, send):
    total = keep.astype(f32) + swap(send).astype(f32)
    rounded = total.astype(bf16)
    three = onward(rounded[4:6], 1)
    four = onward(rounded[6:7], 2)
    one = onward(rounded[0:2], 1)
    four = four.astype(f32)
    none = jnp.zeros_like(four)
    four = by_core(jnp.concatenate([four, none]), jnp.concatenate([none, four]))
    two = onward((total[2:4] + three.astype(f32) + four).astype(bf16), 2)
    side = one.astype(f32) + two.astype(f32)
    other = swap(by_core(side[1], side[0]).astype(bf16))
    return (by_core(side[0], side[1]) + other.astype(f32) + total[7]).astype(bf16)


def local(
    residual, queries, keys, values, documents, sinks, head_gain, out_weight, norm_gain,
    norm_shift, routes, route_logits, gate_weight, up_weight, down_weight, final_gain,
    final_shift,
):
    edge = jnp.concatenate([keys[TOKENS - WINDOW :], values[TOKENS - WINDOW :]], axis=1)
    edge_docs = documents[TOKENS - WINDOW :].astype(bf16)
    edge_docs = jnp.pad(edge_docs[None], ((0, 7), (0, LANES)))
    halo = lax.ppermute(
        jnp.concatenate([edge, edge_docs], axis=0), SP, [(i - 1, i) for i in range(1, N_SP)]
    )
    gain, shift = norm_gain[None], norm_shift[None]
    whole = pl.BlockSpec(memory_space=pltpu.VMEM)
    payload = call(
        attention_kernel,
        shape((N_TP, WINDOW + 16, LANES), bf16),
        60_000_000,
        1_500_000,
        in_specs=[pl.BlockSpec(memory_space=pltpu.SMEM)] + [whole] * 9,
    )(sinks, halo, keys, values, queries, documents[None], residual, out_weight, gain, shift)
    gathered = to_all(payload)
    first, outgoing, stats, slots, affine = call(
        mix_kernel,
        (
            shape((TOKENS, LANES), f32),
            shape((SLOTS, LANES), bf16),
            shape((STAT_ROWS, LANES), bf16),
            shape((8, TOKENS), jnp.int32),
            shape((2, D), f32),
        ),
        140_000_000,
        1_500_000,
    )(gathered, head_gain[None], out_weight, residual, routes.T)
    arrived = over_sp(outgoing.reshape(N_SP, CAP, LANES)).reshape(SLOTS, LANES)
    own, mine, other = gather_columns(jnp.concatenate([arrived, stats], axis=0))
    totals = sum(jnp.sum(v[:, SLOTS:].astype(f32), axis=0) for v in (own, mine, other))

    def tile(count, width):
        return pl.BlockSpec((count, ROW_TILE, width), lambda i: (0, i, 0))

    def fixed(*dims):
        return pl.BlockSpec(dims, lambda i: (0,) * len(dims))

    keep, send = call(
        expert_kernel,
        (shape((8, SLOTS, LANES), bf16),) * 2,
        2 * SLOTS * D * FF_LOCAL * 3,
        12_000_000,
        grid=(SLOTS // ROW_TILE,),
        in_specs=[
            tile(2, LANES),
            tile(7, LANES),
            tile(7, LANES),
            fixed(2, D),
            fixed(D, FF_LOCAL),
            fixed(D, FF_LOCAL),
            fixed(FF_LOCAL, D),
        ],
        out_specs=(tile(8, LANES), tile(8, LANES)),
        scratch_shapes=[pltpu.VMEM((ROW_TILE, D), bf16), pltpu.VMEM((ROW_TILE, D), f32)],
    )(own, mine, other, affine, gate_weight[0], up_weight[0], down_weight[0])
    summed = scatter_sum(keep, send)
    returned = over_sp(summed.reshape(N_SP, CAP, LANES)).reshape(SLOTS, LANES)
    second, last = call(
        combine_kernel,
        (shape((TOKENS, LANES), f32), shape((N_TP, 8, LANES), f32)),
        110_000_000,
        800_000,
    )(returned, first, totals, slots, route_logits.T, gain, shift)
    return call(norm_kernel, shape((TOKENS, LANES), bf16), 1_000_000, 400_000)(
        to_all(last), second, final_gain[None], final_shift[None]
    )


def solution(mesh):
    physical = Mesh(mesh.devices.reshape(8, 4, Y, 2), SP + TP)
    return jax.shard_map(
        local,
        mesh=physical,
        in_specs=(
            P(SP, TP),
            P(SP, TP),
            P(SP, None),
            P(SP, None),
            P(SP),
            P(TP),
            P(),
            P(None, TP),
            P(TP),
            P(TP),
            P(SP, None),
            P(SP, None),
            P(SP, None, TP),
            P(SP, None, TP),
            P(SP, TP, None),
            P(TP),
            P(TP),
        ),
        out_specs=P(SP, TP),
        check_vma=False,
    )
```

time: 269 us -> 192 us (0.71)
  waiting for transfers between devices: 128 us -> 51 us
  starting transfers between devices: 28.7 us -> 47.5 us
  Pallas kernels: 0 us -> 16.2 us
  matrix products: 14.8 us -> 0 us
  between operations: 14.4 us -> 1.02 us
  local copies, waits for them, and re-layouts: 15.2 us -> 8.13 us
  other arithmetic: 8.54 us -> 2.51 us
  blocking collectives: 58.5 us -> 64.5 us
    all_to_all x3 -> x1, waiting for transfers between devices: 88.1 us -> 10.6 us  [over_sp(): return lax.all_to_all(value, SP, 0, 0, tiled=True)]
    ppermute x3 -> x13, waiting for transfers between devices: 0.01 us -> 40.4 us  [the longest x8 32.3 us: onward(): return lax.ppermute(v, TP, pairs)]
    all_gather x1 -> x0, waiting for transfers between devices: 39.9 us -> none  [local(): lax.all_gather(lax.all_to_all(outgoing, 'sp', split_axis=0, concat_axis=0...]
    ppermute x3 -> x13, starting transfers between devices: 9.84 us -> 43.6 us  [the longest x8 21 us: onward(): return lax.ppermute(v, TP, pairs)]
    all_to_all x2 -> x3, blocking collectives: 38.2 us -> 64.5 us  [the longest x2 39.6 us: to_all(): return lax.all_to_all(value, TP, 0, 0, tiled=True)]
    all_gather x1 -> x0, blocking collectives: 20.4 us -> none  [local(): lax.all_gather(attended, 'tp', axis=1, tiled=True).astype(jnp.float32)]
    pallas_call x0 -> x5, Pallas kernels: none -> 16.2 us  [the longest x1 12.8 us: local(): call(expert_kernel, (shape((8, SLOTS, LANES), bf16),) * 2, 2 * SLOTS * D...]
    all_to_all x3 -> x1, starting transfers between devices: 18.8 us -> 3.86 us  [over_sp(): return lax.all_to_all(value, SP, 0, 0, tiled=True)]
  transfers between devices with their start and end apart: 7 -> 14, of which waited for: 4 -> 10; matrix products, arithmetic and copies ran while one was open for 4% -> 1% of each run, Pallas kernels for 0% -> 0%
where the time goes in v1:
time: 192 us; the launch traced here: 191 us
  blocking collectives  64.5 us (34%)
  waiting for transfers between devices  51 us (27%)
  starting transfers between devices  47.5 us (25%)
  Pallas kernels  16.2 us (8%)
  local copies, waits for them, and re-layouts  8.13 us (4%)
  other arithmetic  2.51 us (1%)
    all_to_all x2, blocking collectives, to_all(): return lax.all_to_all(value, TP, 0, 0, tiled=True)  39.6 us
    ppermute x8, waiting for transfers between devices, onward(): return lax.ppermute(v, TP, pairs)  32.3 us
    all_to_all x1, blocking collectives, over_sp(): return lax.all_to_all(value, SP, 0, 0, tiled=True)  24.9 us
    ppermute x8, starting transfers between devices, onward(): return lax.ppermute(v, TP, pairs)  21 us
    ppermute x4, starting transfers between devices, swap(): return lax.ppermute(v, 'c', [(0, 1), (1, 0)])  18.6 us
    pallas_call x1, Pallas kernels, local(): call(expert_kernel, (shape((8, SLOTS, LANES), bf16),) * 2, 2 * SLOTS * D...  12.8 us
    all_to_all x1, waiting for transfers between devices, over_sp(): return lax.all_to_all(value, SP, 0, 0, tiled=True)  10.6 us
    ppermute x4, waiting for transfers between devices, swap(): return lax.ppermute(v, 'c', [(0, 1), (1, 0)])  8.06 us
  transfers between devices with their start and end apart: 14, of which 10 were waited for; matrix products, arithmetic and copies ran while one was open for 1% of the time, Pallas kernels for 0%

profile of v1, /device:TPU:1, one launch (start us, length us, event | category | flops | bytes accessed | tf_op | source)
XLA Modules:
  0.0 190.8 jit_solution(1484124373454567336)
XLA Ops:
  2.3 3.9 %collective-permute-start = (bf16[136,256]{1,0:T(8,128)(2,1)S(1)}, bf16[136,256]{1,0:T(8,128)(2,1)S(1)}, u32[]{:S(2)}, u32[]{:S(2)}) collective-permute-start(bf16[136,256]{1,0:T(8,128)(2,1)S(1)} %fusion.6), channel_id=1, source_target_pairs={{0,16},{16,32},{32,48},{48,64},{64,80},{80,96},{96,112},{112,128},... | collective-permute-start | bytes 208904 | tf_op jit(solution)/shard_map/ppermute | solution.py:338
  6.9 0.9 copy.18.queries_ref
  7.8 0.9 copy-done
  13.2 1.0 shard_map.163
  14.3 27.2 %all_to_all.20.gathered_ref = bf16[16,144,128]{2,1,0:T(8,128)(2,1)S(1)} all-to-all(bf16[16,144,128]{2,1,0:T(8,128)(2,1)S(1)} %shard_map.163), channel_id=1, replica_groups=mesh['z'=8,'x'=4,'y'=8,'c'=2] {'y','c'}, dimensions={0} | all-to-all | bytes 1179648 | tf_op jit(solution)/shard_map/all_to_all | solution.py:297
  41.5 1.0 shard_map.164
  42.5 24.9 %all_to_all.21 = bf16[32,24,128]{2,1,0:T(8,128)(2,1)S(1)} all-to-all(bf16[32,24,128]{2,1,0:T(8,128)(2,1)S(1)} %bitcast.33), channel_id=1, replica_groups=mesh['z'=8,'x'=4,'y'=8,'c'=2] {'z','x'}, dimensions={0} | all-to-all | bytes 393216 | tf_op jit(solution)/shard_map/all_to_all | solution.py:301
  67.5 4.0 %collective-permute-start.1 = (bf16[776,128]{1,0:T(8,128)(2,1)S(1)}, bf16[776,128]{1,0:T(8,128)(2,1)S(1)}, u32[]{:S(2)}, u32[]{:S(2)}) collective-permute-start(bf16[776,128]{1,0:T(8,128)(2,1)S(1)} %get-tuple-element.28), channel_id=1, source_target_pairs={{0,1},{1,0},{2,3},{3,2},{4,5},{5,4},{6,7},{7,6},{8,9},{9,8},{10,11... | collective-permute-start | bytes 595976 | tf_op jit(solution)/shard_map/ppermute | solution.py:281
  71.5 1.0 collective-permute-done.1
  72.7 2.3 %collective-permute-start.3 = (bf16[2,776,128]{2,1,0:T(8,128)(2,1)S(1)}, bf16[2,776,128]{2,1,0:T(8,128)(2,1)S(1)}, u32[]{:S(2)}, u32[]{:S(2)}) collective-permute-start(bf16[2,776,128]{2,1,0:T(8,128)(2,1)S(1)} %maximum_select_fusion.own_ref), channel_id=1, source_target_pairs={{0,4},{1,13},{2,6},{3,15},{4,8},{5,1},{6,10},{7,3},{8,12},{9,5},{1... | collective-permute-start | bytes 1191944 | tf_op jit(solution)/shard_map/ppermute | solution.py:289
  74.9 2.2 %collective-permute-start.2 = (bf16[2,776,128]{2,1,0:T(8,128)(2,1)S(1)}, bf16[2,776,128]{2,1,0:T(8,128)(2,1)S(1)}, u32[]{:S(2)}, u32[]{:S(2)}) collective-permute-start(bf16[2,776,128]{2,1,0:T(8,128)(2,1)S(1)} %maximum_select_fusion.own_ref), channel_id=1, source_target_pairs={{0,2},{1,15},{2,4},{3,1},{4,6},{5,3},{6,8},{7,5},{8,10},{9,7},{10,... | collective-permute-start | bytes 1191944 | tf_op jit(solution)/shard_map/ppermute | solution.py:289
  77.2 9.5 %collective-permute-done.3 = bf16[2,776,128]{2,1,0:T(8,128)(2,1)S(1)} collective-permute-done((bf16[2,776,128]{2,1,0:T(8,128)(2,1)S(1)}, bf16[2,776,128]{2,1,0:T(8,128)(2,1)S(1)}, u32[]{:S(2)}, u32[]{:S(2)}) %collective-permute-start.3) | collective-permute-done | bytes 397344 | tf_op jit(solution)/shard_map/ppermute | solution.py:289
  86.7 1.9 %collective-permute-start.4 = (bf16[2,776,128]{2,1,0:T(8,128)(2,1)S(1)}, bf16[2,776,128]{2,1,0:T(8,128)(2,1)S(1)}, u32[]{:S(2)}, u32[]{:S(2)}) collective-permute-start(bf16[2,776,128]{2,1,0:T(8,128)(2,1)S(1)} %collective-permute-done.3), channel_id=1, source_target_pairs={{0,2},{1,15},{2,4},{3,1},{4,6},{5,3},{6,8},{7,5},{8,10},{9,7},{10,... | collective-permute-start | bytes 1191944 | tf_op jit(solution)/shard_map/ppermute | solution.py:289
  88.7 3.3 %collective-permute-start.5 = (bf16[1,776,128]{2,1,0:T(8,128)(2,1)S(1)}, bf16[1,776,128]{2,1,0:T(8,128)(2,1)S(1)}, u32[]{:S(2)}, u32[]{:S(2)}) collective-permute-start(bf16[1,776,128]{2,1,0:T(8,128)(2,1)S(1)} %slice_select_fusion), channel_id=1, source_target_pairs={{0,4},{1,13},{2,6},{3,15},{4,8},{5,1},{6,10},{7,3},{8,12},{9,5},{1... | collective-permute-start | bytes 595976 | tf_op jit(solution)/shard_map/ppermute | solution.py:289
  92.1 4.7 %collective-permute-done.4 = bf16[2,776,128]{2,1,0:T(8,128)(2,1)S(1)} collective-permute-done((bf16[2,776,128]{2,1,0:T(8,128)(2,1)S(1)}, bf16[2,776,128]{2,1,0:T(8,128)(2,1)S(1)}, u32[]{:S(2)}, u32[]{:S(2)}) %collective-permute-start.4) | collective-permute-done | bytes 397344 | tf_op jit(solution)/shard_map/ppermute | solution.py:289
  96.8 1.4 collective-permute-done.5
  98.2 5.9 %collective-permute-start.6 = (bf16[7,776,128]{2,1,0:T(8,128)(2,1)S(1)}, bf16[7,776,128]{2,1,0:T(8,128)(2,1)S(1)}, u32[]{:S(2)}, u32[]{:S(2)}) collective-permute-start(bf16[7,776,128]{2,1,0:T(8,128)(2,1)S(1)} %constant_dynamic-update-slice_fusion.mine_ref), channel_id=1, source_target_pairs={{0,1},{1,0},{2,3},{3,2},{4,5},{5,4},{6,7},{7,6},{8,9},{9,8},{10,11... | collective-permute-start | bytes 4171784 | tf_op jit(solution)/shard_map/ppermute | solution.py:281
  104.2 2.8 %collective-permute-done.6.other_ref = bf16[7,776,128]{2,1,0:T(8,128)(2,1)S(1)} collective-permute-done((bf16[7,776,128]{2,1,0:T(8,128)(2,1)S(1)}, bf16[7,776,128]{2,1,0:T(8,128)(2,1)S(1)}, u32[]{:S(2)}, u32[]{:S(2)}) %collective-permute-start.6) | collective-permute-done | bytes 1390624 | tf_op jit(solution)/shard_map/ppermute | solution.py:281
  106.9 12.8 %shard_map.165 = (bf16[8,768,128]{2,1,0:T(8,128)(2,1)S(1)}, bf16[8,768,128]{2,1,0:T(8,128)(2,1)}) custom-call(bf16[2,776,128]{2,1,0:T(8,128)(2,1)S(1)} %maximum_select_fusion.own_ref, bf16[7,776,128]{2,1,0:T(8,128)(2,1)S(1)} %constant_dynamic-update-slice_fusion.mine_ref, bf16[7,776,128]{2,1,0:T(8,128)(2,1)S(1)} %collective-permute-done.6.other_ref, ...), custom_call_target="tpu_custom_call" | custom-call | flops 3623878656 | bytes 12000000 | tf_op jit(solution)/shard_map/pallas_call | solution.py:373
  119.7 2.3 %collective-permute-start.7 = (bf16[8,768,128]{2,1,0:T(8,128)(2,1)}, bf16[8,768,128]{2,1,0:T(8,128)(2,1)S(1)}, u32[]{:S(2)}, u32[]{:S(2)}) collective-permute-start(bf16[8,768,128]{2,1,0:T(8,128)(2,1)} %get-tuple-element.18), channel_id=1, source_target_pairs={{0,1},{1,0},{2,3},{3,2},{4,5},{5,4},{6,7},{7,6},{8,9},{9,8},{10,11... | collective-permute-start | bytes 4718600 | tf_op jit(solution)/shard_map/ppermute | solution.py:281
  122.0 3.2 %collective-permute-done.7 = bf16[8,768,128]{2,1,0:T(8,128)(2,1)S(1)} collective-permute-done((bf16[8,768,128]{2,1,0:T(8,128)(2,1)}, bf16[8,768,128]{2,1,0:T(8,128)(2,1)S(1)}, u32[]{:S(2)}, u32[]{:S(2)}) %collective-permute-start.7) | collective-permute-done | bytes 1572896 | tf_op jit(solution)/shard_map/ppermute | solution.py:281
  125.8 3.8 %collective-permute-start.9 = (bf16[2,768,128]{2,1,0:T(8,128)(2,1)S(1)}, bf16[2,768,128]{2,1,0:T(8,128)(2,1)S(1)}, u32[]{:S(2)}, u32[]{:S(2)}) collective-permute-start(bf16[2,768,128]{2,1,0:T(8,128)(2,1)S(1)} %get-tuple-element.26), channel_id=1, source_target_pairs={{0,2},{1,15},{2,4},{3,1},{4,6},{5,3},{6,8},{7,5},{8,10},{9,7},{10,... | collective-permute-start | bytes 1179656 | tf_op jit(solution)/shard_map/ppermute | solution.py:289
  129.6 1.9 %collective-permute-start.10 = (bf16[1,768,128]{2,1,0:T(8,128)(2,1)S(1)}, bf16[1,768,128]{2,1,0:T(8,128)(2,1)S(1)}, u32[]{:S(2)}, u32[]{:S(2)}) collective-permute-start(bf16[1,768,128]{2,1,0:T(8,128)(2,1)S(1)} %slice.68), channel_id=1, source_target_pairs={{0,4},{1,13},{2,6},{3,15},{4,8},{5,1},{6,10},{7,3},{8,12},{9,5},{1... | collective-permute-start | bytes 589832 | tf_op jit(solution)/shard_map/ppermute | solution.py:289
  131.5 2.7 %collective-permute-start.8 = (bf16[2,768,128]{2,1,0:T(8,128)(2,1)S(1)}, bf16[2,768,128]{2,1,0:T(8,128)(2,1)S(1)}, u32[]{:S(2)}, u32[]{:S(2)}) collective-permute-start(bf16[2,768,128]{2,1,0:T(8,128)(2,1)S(1)} %get-tuple-element.25), channel_id=1, source_target_pairs={{0,2},{1,15},{2,4},{3,1},{4,6},{5,3},{6,8},{7,5},{8,10},{9,7},{10,... | collective-permute-start | bytes 1179656 | tf_op jit(solution)/shard_map/ppermute | solution.py:289
  134.2 7.3 %collective-permute-done.10 = bf16[1,768,128]{2,1,0:T(8,128)(2,1)S(1)} collective-permute-done((bf16[1,768,128]{2,1,0:T(8,128)(2,1)S(1)}, bf16[1,768,128]{2,1,0:T(8,128)(2,1)S(1)}, u32[]{:S(2)}, u32[]{:S(2)}) %collective-permute-start.10) | collective-permute-done | bytes 196640 | tf_op jit(solution)/shard_map/ppermute | solution.py:289
  141.7 3.0 %collective-permute-start.11 = (bf16[2,768,128]{2,1,0:T(8,128)(2,1)S(1)}, bf16[2,768,128]{2,1,0:T(8,128)(2,1)S(1)}, u32[]{:S(2)}, u32[]{:S(2)}) collective-permute-start(bf16[2,768,128]{2,1,0:T(8,128)(2,1)S(1)} %fusion.1), channel_id=1, source_target_pairs={{0,4},{1,13},{2,6},{3,15},{4,8},{5,1},{6,10},{7,3},{8,12},{9,5},{1... | collective-permute-start | bytes 1179656 | tf_op jit(solution)/shard_map/ppermute | solution.py:289
  144.7 9.4 %collective-permute-done.11 = bf16[2,768,128]{2,1,0:T(8,128)(2,1)S(1)} collective-permute-done((bf16[2,768,128]{2,1,0:T(8,128)(2,1)S(1)}, bf16[2,768,128]{2,1,0:T(8,128)(2,1)S(1)}, u32[]{:S(2)}, u32[]{:S(2)}) %collective-permute-start.11) | collective-permute-done | bytes 393248 | tf_op jit(solution)/shard_map/ppermute | solution.py:289
  154.4 6.4 %collective-permute-start.12 = (bf16[768,128]{1,0:T(8,128)(2,1)S(1)}, bf16[768,128]{1,0:T(8,128)(2,1)S(1)}, u32[]{:S(2)}, u32[]{:S(2)}) collective-permute-start(bf16[768,128]{1,0:T(8,128)(2,1)S(1)} %fusion.4), channel_id=1, source_target_pairs={{0,1},{1,0},{2,3},{3,2},{4,5},{5,4},{6,7},{7,6},{8,9},{9,8},{10,11... | collective-permute-start | bytes 589832 | tf_op jit(solution)/shard_map/ppermute | solution.py:281
  160.7 1.0 collective-permute-done.12
  162.5 3.9 %all-to-all-start.2 = ((bf16[32,24,128]{2,1,0:T(8,128)(2,1)}), bf16[32,24,128]{2,1,0:T(8,128)(2,1)S(1)}, u32[]{:S(2)}, u32[]{:S(2)}) async-start(bf16[32,24,128]{2,1,0:T(8,128)(2,1)} %bitcast.16), calls=%async_computation.2 | async-start | bytes 393216 | tf_op jit(solution)/shard_map/all_to_all | solution.py:301
  166.5 10.6 %all-to-all-done.2 = bf16[32,24,128]{2,1,0:T(8,128)(2,1)S(1)} async-done(((bf16[32,24,128]{2,1,0:T(8,128)(2,1)}), bf16[32,24,128]{2,1,0:T(8,128)(2,1)S(1)}, u32[]{:S(2)}, u32[]{:S(2)}) %all-to-all-start.2) | async-done | bytes 196640 | tf_op jit(solution)/shard_map/all_to_all | solution.py:301
  177.6 12.4 %all_to_all.22.stats_ref = f32[16,8,128]{2,1,0:T(8,128)S(1)} all-to-all(f32[16,8,128]{2,1,0:T(8,128)S(1)} %get-tuple-element.21), channel_id=1, replica_groups=mesh['z'=8,'x'=4,'y'=8,'c'=2] {'y','c'}, dimensions={0} | all-to-all | bytes 131072 | tf_op jit(solution)/shard_map/all_to_all | solution.py:297
  (61 shorter events, 10.2 us)
Async XLA Ops:
  0.0 41.4 %copy-start.1 = (bf16[1024,128]{1,0:T(8,128)(2,1)S(1)}, bf16[1024,128]{1,0:T(8,128)(2,1)}, u32[]{:S(2)}) copy-start(bf16[1024,128]{1,0:T(8,128)(2,1)} %weight_ref.3) | copy-start | bytes 786436
  0.0 41.4 %copy-start.3 = (bf16[256,128]{1,0:T(8,128)(2,1)S(1)}, bf16[256,128]{1,0:T(8,128)(2,1)}, u32[]{:S(2)}) copy-start(bf16[256,128]{1,0:T(8,128)(2,1)} %residual_ref.3) | copy-start | bytes 196612
  0.0 41.4 %copy-start.7 = (s32[256,2]{0,1:T(2,128)S(1)}, s32[256,2]{0,1:T(2,128)}, u32[]{:S(2)}) copy-start(s32[256,2]{0,1:T(2,128)} %param.27) | copy-start | bytes 6148
  0.0 41.4 %copy-start.6 = (f32[1024]{0:T(1024)S(1)}, f32[1024]{0:T(1024)}, u32[]{:S(2)}) copy-start(f32[1024]{0:T(1024)} %param.23) | copy-start | bytes 12292
  2.3 5.5 %collective-permute-start = (bf16[136,256]{1,0:T(8,128)(2,1)S(1)}, bf16[136,256]{1,0:T(8,128)(2,1)S(1)}, u32[]{:S(2)}, u32[]{:S(2)}) collective-permute-start(bf16[136,256]{1,0:T(8,128)(2,1)S(1)} %fusion.6), channel_id=1, source_target_pairs={{0,16},{16,32},{32,48},{48,64},{64,80},{80,96},{96,112},{112,128},... | collective-permute-start | bytes 208904 | tf_op jit(solution)/shard_map/ppermute | solution.py:338
  7.8 1.0 copy-start
  8.7 0.8 copy-start.2
  9.6 0.8 copy-start.4
  10.4 0.8 copy-start.5
  11.2 0.7 copy-start.8
  11.9 0.7 copy-start.9
  12.6 0.7 copy-start.11
  67.5 5.1 %collective-permute-start.1 = (bf16[776,128]{1,0:T(8,128)(2,1)S(1)}, bf16[776,128]{1,0:T(8,128)(2,1)S(1)}, u32[]{:S(2)}, u32[]{:S(2)}) collective-permute-start(bf16[776,128]{1,0:T(8,128)(2,1)S(1)} %get-tuple-element.28), channel_id=1, source_target_pairs={{0,1},{1,0},{2,3},{3,2},{4,5},{5,4},{6,7},{7,6},{8,9},{9,8},{10,11... | collective-permute-start | bytes 595976 | tf_op jit(solution)/shard_map/ppermute | solution.py:281
  72.7 14.0 %collective-permute-start.3 = (bf16[2,776,128]{2,1,0:T(8,128)(2,1)S(1)}, bf16[2,776,128]{2,1,0:T(8,128)(2,1)S(1)}, u32[]{:S(2)}, u32[]{:S(2)}) collective-permute-start(bf16[2,776,128]{2,1,0:T(8,128)(2,1)S(1)} %maximum_select_fusion.own_ref), channel_id=1, source_target_pairs={{0,4},{1,13},{2,6},{3,15},{4,8},{5,1},{6,10},{7,3},{8,12},{9,5},{1... | collective-permute-start | bytes 1191944 | tf_op jit(solution)/shard_map/ppermute | solution.py:289
  74.9 17.0 %collective-permute-start.2 = (bf16[2,776,128]{2,1,0:T(8,128)(2,1)S(1)}, bf16[2,776,128]{2,1,0:T(8,128)(2,1)S(1)}, u32[]{:S(2)}, u32[]{:S(2)}) collective-permute-start(bf16[2,776,128]{2,1,0:T(8,128)(2,1)S(1)} %maximum_select_fusion.own_ref), channel_id=1, source_target_pairs={{0,2},{1,15},{2,4},{3,1},{4,6},{5,3},{6,8},{7,5},{8,10},{9,7},{10,... | collective-permute-start | bytes 1191944 | tf_op jit(solution)/shard_map/ppermute | solution.py:289
  86.7 10.1 %collective-permute-start.4 = (bf16[2,776,128]{2,1,0:T(8,128)(2,1)S(1)}, bf16[2,776,128]{2,1,0:T(8,128)(2,1)S(1)}, u32[]{:S(2)}, u32[]{:S(2)}) collective-permute-start(bf16[2,776,128]{2,1,0:T(8,128)(2,1)S(1)} %collective-permute-done.3), channel_id=1, source_target_pairs={{0,2},{1,15},{2,4},{3,1},{4,6},{5,3},{6,8},{7,5},{8,10},{9,7},{10,... | collective-permute-start | bytes 1191944 | tf_op jit(solution)/shard_map/ppermute | solution.py:289
  88.7 9.5 %collective-permute-start.5 = (bf16[1,776,128]{2,1,0:T(8,128)(2,1)S(1)}, bf16[1,776,128]{2,1,0:T(8,128)(2,1)S(1)}, u32[]{:S(2)}, u32[]{:S(2)}) collective-permute-start(bf16[1,776,128]{2,1,0:T(8,128)(2,1)S(1)} %slice_select_fusion), channel_id=1, source_target_pairs={{0,4},{1,13},{2,6},{3,15},{4,8},{5,1},{6,10},{7,3},{8,12},{9,5},{1... | collective-permute-start | bytes 595976 | tf_op jit(solution)/shard_map/ppermute | solution.py:289
  98.2 8.7 %collective-permute-start.6 = (bf16[7,776,128]{2,1,0:T(8,128)(2,1)S(1)}, bf16[7,776,128]{2,1,0:T(8,128)(2,1)S(1)}, u32[]{:S(2)}, u32[]{:S(2)}) collective-permute-start(bf16[7,776,128]{2,1,0:T(8,128)(2,1)S(1)} %constant_dynamic-update-slice_fusion.mine_ref), channel_id=1, source_target_pairs={{0,1},{1,0},{2,3},{3,2},{4,5},{5,4},{6,7},{7,6},{8,9},{9,8},{10,11... | collective-permute-start | bytes 4171784 | tf_op jit(solution)/shard_map/ppermute | solution.py:281
  119.7 5.5 %collective-permute-start.7 = (bf16[8,768,128]{2,1,0:T(8,128)(2,1)}, bf16[8,768,128]{2,1,0:T(8,128)(2,1)S(1)}, u32[]{:S(2)}, u32[]{:S(2)}) collective-permute-start(bf16[8,768,128]{2,1,0:T(8,128)(2,1)} %get-tuple-element.18), channel_id=1, source_target_pairs={{0,1},{1,0},{2,3},{3,2},{4,5},{5,4},{6,7},{7,6},{8,9},{9,8},{10,11... | collective-permute-start | bytes 4718600 | tf_op jit(solution)/shard_map/ppermute | solution.py:281
  125.8 15.8 %collective-permute-start.9 = (bf16[2,768,128]{2,1,0:T(8,128)(2,1)S(1)}, bf16[2,768,128]{2,1,0:T(8,128)(2,1)S(1)}, u32[]{:S(2)}, u32[]{:S(2)}) collective-permute-start(bf16[2,768,128]{2,1,0:T(8,128)(2,1)S(1)} %get-tuple-element.26), channel_id=1, source_target_pairs={{0,2},{1,15},{2,4},{3,1},{4,6},{5,3},{6,8},{7,5},{8,10},{9,7},{10,... | collective-permute-start | bytes 1179656 | tf_op jit(solution)/shard_map/ppermute | solution.py:289
  129.6 11.9 %collective-permute-start.10 = (bf16[1,768,128]{2,1,0:T(8,128)(2,1)S(1)}, bf16[1,768,128]{2,1,0:T(8,128)(2,1)S(1)}, u32[]{:S(2)}, u32[]{:S(2)}) collective-permute-start(bf16[1,768,128]{2,1,0:T(8,128)(2,1)S(1)} %slice.68), channel_id=1, source_target_pairs={{0,4},{1,13},{2,6},{3,15},{4,8},{5,1},{6,10},{7,3},{8,12},{9,5},{1... | collective-permute-start | bytes 589832 | tf_op jit(solution)/shard_map/ppermute | solution.py:289
  131.5 13.2 %collective-permute-start.8 = (bf16[2,768,128]{2,1,0:T(8,128)(2,1)S(1)}, bf16[2,768,128]{2,1,0:T(8,128)(2,1)S(1)}, u32[]{:S(2)}, u32[]{:S(2)}) collective-permute-start(bf16[2,768,128]{2,1,0:T(8,128)(2,1)S(1)} %get-tuple-element.25), channel_id=1, source_target_pairs={{0,2},{1,15},{2,4},{3,1},{4,6},{5,3},{6,8},{7,5},{8,10},{9,7},{10,... | collective-permute-start | bytes 1179656 | tf_op jit(solution)/shard_map/ppermute | solution.py:289
  141.7 12.5 %collective-permute-start.11 = (bf16[2,768,128]{2,1,0:T(8,128)(2,1)S(1)}, bf16[2,768,128]{2,1,0:T(8,128)(2,1)S(1)}, u32[]{:S(2)}, u32[]{:S(2)}) collective-permute-start(bf16[2,768,128]{2,1,0:T(8,128)(2,1)S(1)} %fusion.1), channel_id=1, source_target_pairs={{0,4},{1,13},{2,6},{3,15},{4,8},{5,1},{6,10},{7,3},{8,12},{9,5},{1... | collective-permute-start | bytes 1179656 | tf_op jit(solution)/shard_map/ppermute | solution.py:289
  154.3 22.7 %copy-start.10 = (f32[128]{0:T(128)S(1)}, f32[128]{0:T(128)}, u32[]{:S(2)}) copy-start(f32[128]{0:T(128)} %param.25) | copy-start | bytes 1540
  154.3 22.7 %copy-start.12 = (f32[128]{0:T(128)S(1)}, f32[128]{0:T(128)}, u32[]{:S(2)}) copy-start(f32[128]{0:T(128)} %param.26) | copy-start | bytes 1540
  154.3 22.7 %copy-start.15 = (f32[256,2]{0,1:T(2,128)S(1)}, f32[256,2]{0,1:T(2,128)}, u32[]{:S(2)}) copy-start(f32[256,2]{0,1:T(2,128)} %param.28) | copy-start | bytes 6148
  154.3 35.7 %copy-start.13 = (f32[128]{0:T(128)S(1)}, f32[128]{0:T(128)}, u32[]{:S(2)}) copy-start(f32[128]{0:T(128)} %param.32) | copy-start | bytes 1540
  154.3 35.7 %copy-start.14 = (f32[128]{0:T(128)S(1)}, f32[128]{0:T(128)}, u32[]{:S(2)}) copy-start(f32[128]{0:T(128)} %param.33) | copy-start | bytes 1540
  154.4 7.4 %collective-permute-start.12 = (bf16[768,128]{1,0:T(8,128)(2,1)S(1)}, bf16[768,128]{1,0:T(8,128)(2,1)S(1)}, u32[]{:S(2)}, u32[]{:S(2)}) collective-permute-start(bf16[768,128]{1,0:T(8,128)(2,1)S(1)} %fusion.4), channel_id=1, source_target_pairs={{0,1},{1,0},{2,3},{3,2},{4,5},{5,4},{6,7},{7,6},{8,9},{9,8},{10,11... | collective-permute-start | bytes 589832 | tf_op jit(solution)/shard_map/ppermute | solution.py:281
  162.5 14.5 %all-to-all-start.2 = ((bf16[32,24,128]{2,1,0:T(8,128)(2,1)}), bf16[32,24,128]{2,1,0:T(8,128)(2,1)S(1)}, u32[]{:S(2)}, u32[]{:S(2)}) async-start(bf16[32,24,128]{2,1,0:T(8,128)(2,1)} %bitcast.16), calls=%async_computation.2 | async-start | bytes 393216 | tf_op jit(solution)/shard_map/all_to_all | solution.py:301

commit v2 on v1

--- a/solution.py
+++ b/solution.py
@@ -21,8 +21,8 @@
 FF_LOCAL = 384
 LANES = 128
 STAT_ROWS = 8
-ROWS = SLOTS + STAT_ROWS
-ROW_TILE = 256
+HALF = SLOTS // 2
+FULL = 67_043_328
 
 DEEP_ALPHA = 8.0**0.25
 NORM_EPS = 1e-05
@@ -31,6 +31,7 @@
 TP = ("y", "c")
 Y = 8
 
+
 f32 = jnp.float32
 bf16 = jnp.bfloat16
 
@@ -58,50 +59,110 @@
     return high, v - high
 
 
-def attention_kernel(
-    sinks_ref, halo_ref, keys_ref, values_ref, queries_ref, docs_ref, residual_ref,
-    weight_ref, gain_ref, shift_ref, out_ref,
+def fetch(pairs, sems):
+    copies = [
+        pltpu.make_async_copy(source, target, sems.at[i]) for i, (source, target) in enumerate(pairs)
+    ]
+    for copy in copies:
+        copy.start()
+    for copy in copies:
+        copy.wait()
+
+
+def halo_kernel(keys_hbm, values_hbm, docs_hbm, out_ref, keys_ref, values_ref, docs_ref, sems):
+    last = pl.ds(TOKENS - WINDOW, WINDOW)
+    fetch(
+        (
+            (keys_hbm.at[last], keys_ref),
+            (values_hbm.at[last], values_ref),
+            (docs_hbm, docs_ref),
+        ),
+        sems,
+    )
+    out_ref[:WINDOW, :LANES] = keys_ref[...]
+    out_ref[:WINDOW, LANES:] = values_ref[...]
+    docs = jnp.broadcast_to(docs_ref[:, WINDOW:].astype(f32), (8, LANES))
+    out_ref[WINDOW:, :LANES] = docs.astype(bf16)
+    out_ref[WINDOW:, LANES:] = jnp.zeros((8, LANES), bf16)
+
+
+def prepare_kernel(
+    residual_hbm, weight_hbm, gain_hbm, shift_hbm, keys_hbm, values_hbm, queries_hbm, docs_hbm,
+    out_ref,
+    residual_ref, weight_ref, gain_ref, shift_ref, keys_ref, values_ref, queries_ref, docs_ref,
+    sems,
 ):
-    kv_head = (lax.axis_index("y") * 2 + lax.axis_index("c")) // (QUERY_HEADS // KEY_VALUE_HEADS)
+    fetch(
+        (
+            (weight_hbm, weight_ref),
+            (residual_hbm, residual_ref),
+            (keys_hbm, keys_ref),
+            (values_hbm, values_ref),
+            (queries_hbm, queries_ref),
+            (docs_hbm, docs_ref),
+            (gain_hbm, gain_ref),
+            (shift_hbm, shift_ref),
+        ),
+        sems,
+    )
+    ones = jnp.ones((8, LANES), bf16)
+    means = nt(ones, residual_ref[...])[0:1]
+    w_sums = nt(ones, weight_ref[...])[0:1]
+    rows = [means[:, :LANES], means[:, LANES:]]
+    rows += [w_sums[:, i * LANES : (i + 1) * LANES] for i in range(8)]
+    rows += [*high_low(gain_ref[...]), *high_low(shift_ref[...])]
+    docs = docs_ref[...].astype(f32)
+    rows += [docs[:, :WINDOW], docs[:, WINDOW:]]
+    pick = kv_head() == 0
+    heads = [head_of(pick, keys_ref[...]), head_of(pick, values_ref[...])]
+    out_ref[:TOKENS, :] = jnp.concatenate(heads, axis=1)
+    queries = queries_ref[...].astype(f32)
+    out_ref[TOKENS : TOKENS + WINDOW, :] = jnp.concatenate(
+        [queries[:, :WINDOW].T, queries[:, WINDOW:].T], axis=1
+    ).astype(bf16)
+    out_ref[TOKENS + WINDOW :, :] = jnp.concatenate(rows, axis=0).astype(bf16)
+
+
+def kv_head():
+    return (lax.axis_index("y") * 2 + lax.axis_index("c")) // (QUERY_HEADS // KEY_VALUE_HEADS)
+
+
+def head_of(pick, block):
+    block = block.astype(f32)
+    return jnp.where(pick, block[:, :HEAD_SIZE], block[:, HEAD_SIZE:]).astype(bf16)
+
+
+def attention_kernel(sinks_ref, halo_ref, prepared_ref, out_ref):
     first_block = (lax.axis_index("z") * 4 + lax.axis_index("x")) == 0
-    sink = sinks_ref[0]
-    pick = kv_head == 0
-
-    def head_of(block):
-        return jnp.where(pick, block[:, :HEAD_SIZE], block[:, HEAD_SIZE:])
-
-    keys = [head_of(halo_ref[:WINDOW, :LANES].astype(f32)).astype(bf16)]
-    vals = [head_of(halo_ref[:WINDOW, LANES:].astype(f32)).astype(bf16)]
+    sink = sinks_ref[0:1, 0:1]
+    pick = kv_head() == 0
+    keys = [head_of(pick, halo_ref[:WINDOW, :LANES])]
+    vals = [head_of(pick, halo_ref[:WINDOW, LANES:])]
     for i in range(2):
         part = slice(i * WINDOW, (i + 1) * WINDOW)
-        keys.append(head_of(keys_ref[part, :].astype(f32)).astype(bf16))
-        vals.append(head_of(values_ref[part, :].astype(f32)).astype(bf16))
-    docs = docs_ref[...].astype(f32)
+        keys.append(prepared_ref[part, :HEAD_SIZE])
+        vals.append(prepared_ref[part, HEAD_SIZE:])
+    queries = prepared_ref[TOKENS : TOKENS + WINDOW, :]
+    tail = prepared_ref[TOKENS + WINDOW :, :]
     halo_docs = halo_ref[WINDOW : WINDOW + 8, :LANES].astype(f32)[0:1]
     halo_docs = jnp.where(first_block, -1.0, halo_docs)
-    doc_rows = [halo_docs, docs[:, :WINDOW], docs[:, WINDOW:]]
+    docs = tail.astype(f32)
+    doc_rows = [halo_docs, docs[14:15], docs[15:16]]
     qi = lax.broadcasted_iota(jnp.int32, (WINDOW, WINDOW), 0)
     ki = lax.broadcasted_iota(jnp.int32, (WINDOW, WINDOW), 1)
     blocks = []
     for i in range(2):
-        q = queries_ref[i * WINDOW : (i + 1) * WINDOW, :]
+        q = queries[:, i * HEAD_SIZE : (i + 1) * HEAD_SIZE]
         q_docs = column(doc_rows[i + 1])
         before = nt(q, keys[i]) * HEAD_SIZE ** (-0.5)
         here = nt(q, keys[i + 1]) * HEAD_SIZE ** (-0.5)
         before = jnp.where((ki > qi) & (q_docs == doc_rows[i]), before, -jnp.inf)
         here = jnp.where((ki <= qi) & (q_docs == doc_rows[i + 1]), here, -jnp.inf)
         top = jnp.maximum(
-            jnp.maximum(
-                jnp.max(before, axis=1, keepdims=True), jnp.max(here, axis=1, keepdims=True)
-            ),
-            sink,
+            jnp.max(jnp.maximum(before, here), axis=1, keepdims=True), sink
         )
         before, here = jnp.exp(before - top), jnp.exp(here - top)
-        total = (
-            jnp.sum(before, axis=1, keepdims=True)
-            + jnp.sum(here, axis=1, keepdims=True)
-            + jnp.exp(sink - top)
-        )
+        total = jnp.sum(before + here, axis=1, keepdims=True) + jnp.exp(sink - top)
         before = (before / total).astype(bf16)
         here = (here / total).astype(bf16)
         blocks.append(
@@ -109,14 +170,6 @@
             + jnp.dot(here, vals[i + 1], preferred_element_type=f32)
         )
     attended = jnp.concatenate(blocks, axis=1).astype(bf16)
-    ones = jnp.ones((8, LANES), bf16)
-    means = nt(ones, residual_ref[...])[0:1]
-    w_sums = nt(ones, weight_ref[...])[0:1]
-    rows = [means[:, :LANES], means[:, LANES:]]
-    rows += [w_sums[:, i * LANES : (i + 1) * LANES] for i in range(8)]
-    rows += [*high_low(gain_ref[...]), *high_low(shift_ref[...])]
-    rows += [jnp.zeros((2, LANES), f32)]
-    tail = jnp.concatenate(rows, axis=0).astype(bf16)
     for t in range(N_TP):
         out_ref[t, :WINDOW, :] = attended
         out_ref[t, WINDOW:, :] = tail
@@ -178,25 +231,30 @@
 
 
 def expert_kernel(
-    own_ref, mine_ref, other_ref, affine_ref, gate_ref, up_ref, down_ref,
-    keep_ref, send_ref, rows_ref, out_ref,
+    own_ref, near_up_ref, near_down_ref, two_up_ref, two_down_ref, four_ref, affine_ref,
+    gate_ref, up_ref, down_ref, gate_other_ref, up_other_ref, down_other_ref,
+    to_near_up_ref, to_near_down_ref, to_two_up_ref, to_two_down_ref, to_four_ref, to_own_ref,
+    totals_ref, rows_ref,
 ):
-    y, c = lax.axis_index("y"), lax.axis_index("c")
-    way = 1 - 2 * c
-
-    def lanes_of(chip, half):
-        return pl.ds(pl.multiple_of((lax.rem(chip + 2 * Y, Y) * 2 + half) * LANES, LANES), LANES)
-
-    blocks = [(own_ref, h, lanes_of(y, h)) for h in range(2)]
-    for k in range(1, 4):
+    y = lax.axis_index("y")
+
+    def lanes_of(away):
+        at = lax.rem(y + away + Y, Y) * 2 * LANES
+        return pl.multiple_of(at, 2 * LANES)
+
+    blocks = []
+    for ref, i, away in (
+        (own_ref, 0, 0), (two_up_ref, 0, -2), (two_down_ref, 0, 2), (near_up_ref, 0, -1),
+        (near_up_ref, 2, -3), (near_down_ref, 0, 1), (near_down_ref, 2, 3), (four_ref, 0, 4),
+    ):
         for h in range(2):
-            blocks.append((mine_ref, 2 * k - 2 + h, lanes_of(y - way * k, h)))
-            blocks.append((other_ref, 2 * k - 2 + h, lanes_of(y + way * k, h)))
-    blocks.append((mine_ref, 6, lanes_of(y + 4, c)))
-    blocks.append((other_ref, 6, lanes_of(y + 4, 1 - c)))
+            blocks.append((ref, i + h, pl.ds(pl.multiple_of(lanes_of(away) + h * LANES, LANES), LANES)))
+    totals_ref[...] = functools.reduce(
+        jnp.add, [ref[i, :STAT_ROWS, :].astype(f32) for ref, i, _ in blocks]
+    )
     total = square = 0.0
     for ref, i, _ in blocks:
-        v = ref[i].astype(f32)
+        v = ref[i, STAT_ROWS:, :].astype(f32)
         total = total + v
         square = square + v * v
     center = jnp.sum(total, axis=1, keepdims=True) * (1.0 / D)
@@ -204,20 +262,23 @@
     scale = lax.rsqrt(spread + NORM_EPS)
     offset = center * scale
     for ref, i, lanes in blocks:
-        v = ref[i].astype(f32) * scale - offset
+        v = ref[i, STAT_ROWS:, :].astype(f32) * scale - offset
         rows_ref[:, lanes] = (v * affine_ref[0:1, lanes] + affine_ref[1:2, lanes]).astype(bf16)
-    gate = jnp.dot(rows_ref[...], gate_ref[...], preferred_element_type=f32)
-    up = jnp.dot(rows_ref[...], up_ref[...], preferred_element_type=f32)
-    middle = (gate / (1.0 + jnp.exp(-gate)) * up).astype(bf16)
-    out_ref[...] = jnp.dot(middle, down_ref[...], preferred_element_type=f32)
-    for k in range(1, 4):
-        for h in range(2):
-            keep_ref[2 * k - 2 + h] = out_ref[:, lanes_of(y + way * k, h)].astype(bf16)
-            send_ref[2 * k - 2 + h] = out_ref[:, lanes_of(y - way * k, h)].astype(bf16)
-    keep_ref[6] = out_ref[:, lanes_of(y + 4, c)].astype(bf16)
-    send_ref[6] = out_ref[:, lanes_of(y + 4, 1 - c)].astype(bf16)
-    keep_ref[7] = out_ref[:, lanes_of(y, c)].astype(bf16)
-    send_ref[7] = out_ref[:, lanes_of(y, 1 - c)].astype(bf16)
+    middles = []
+    for g, u in ((gate_ref, up_ref), (gate_other_ref, up_other_ref)):
+        gate = jnp.dot(rows_ref[...], g[...], preferred_element_type=f32)
+        up = jnp.dot(rows_ref[...], u[...], preferred_element_type=f32)
+        middles.append((gate / (1.0 + jnp.exp(-gate)) * up).astype(bf16))
+    for ref, i, away in (
+        (to_near_up_ref, 0, 1), (to_near_up_ref, 2, 3), (to_near_down_ref, 0, -1),
+        (to_near_down_ref, 2, -3), (to_four_ref, 0, 4), (to_two_up_ref, 0, 2),
+        (to_two_down_ref, 0, -2), (to_own_ref, 0, 0),
+    ):
+        lanes = pl.ds(lanes_of(away), 2 * LANES)
+        out = jnp.dot(middles[0], down_ref[:, lanes], preferred_element_type=f32)
+        out = out + jnp.dot(middles[1], down_other_ref[:, lanes], preferred_element_type=f32)
+        ref[i] = out[:, :LANES].astype(bf16)
+        ref[i + 1] = out[:, LANES:].astype(bf16)
 
 
 def combine_kernel(
@@ -263,12 +324,12 @@
         out_ref[rows, :] = (out * gain_ref[...] + shift_ref[...]).astype(bf16)
 
 
-def call(kernel, outs, flops, moved, **more):
+def call(kernel, outs, flops, moved, limit=16 << 20, **more):
     return pl.pallas_call(
         kernel,
         out_shape=outs,
         cost_estimate=pl.CostEstimate(flops=flops, bytes_accessed=moved, transcendentals=0),
-        compiler_params=pltpu.CompilerParams(vmem_limit_bytes=48 * 1024 * 1024),
+        compiler_params=pltpu.CompilerParams(vmem_limit_bytes=limit),
         **more,
     )
 
@@ -279,6 +340,10 @@
 
 def swap(v):
     return lax.ppermute(v, "c", [(0, 1), (1, 0)])
+
+
+def along(v, distance):
+    return lax.ppermute(v, "y", [(y, (y + distance) % Y) for y in range(Y)])
 
 
 def onward(v, distance):
@@ -301,30 +366,25 @@
     return lax.all_to_all(value, SP, 0, 0, tiled=True)
 
 
-def gather_columns(block):
-    partner = swap(block)
-    own = by_core(jnp.stack([block, partner]), jnp.stack([partner, block]))
-    two = onward(own, 2)
-    one = onward(own, 1)
-    three = onward(two, 1)
-    four = onward(by_core(two[0:1], two[1:2]), 2)
-    mine = jnp.concatenate([one, two, three, four], axis=0)
-    return own, mine, swap(mine)
-
-
-def scatter_sum(keep, send):
-    total = keep.astype(f32) + swap(send).astype(f32)
-    rounded = total.astype(bf16)
-    three = onward(rounded[4:6], 1)
-    four = onward(rounded[6:7], 2)
-    one = onward(rounded[0:2], 1)
-    four = four.astype(f32)
+def gather_columns(own):
+    two_up = along(own, 2)
+    two_down = along(own, -2)
+    near_up = along(jnp.concatenate([own, two_up], axis=0), 1)
+    near_down = along(jnp.concatenate([own, two_down], axis=0), -1)
+    four = onward(by_core(two_up, two_down), 2)
+    return own, near_up, near_down, two_up, two_down, four
+
+
+def scatter_sum(near_up, near_down, two_up, two_down, four, own):
+    four = onward(four, 2).astype(f32)
+    near_up = along(near_up, 1).astype(f32)
+    near_down = along(near_down, -1).astype(f32)
     none = jnp.zeros_like(four)
-    four = by_core(jnp.concatenate([four, none]), jnp.concatenate([none, four]))
-    two = onward((total[2:4] + three.astype(f32) + four).astype(bf16), 2)
-    side = one.astype(f32) + two.astype(f32)
-    other = swap(by_core(side[1], side[0]).astype(bf16))
-    return (by_core(side[0], side[1]) + other.astype(f32) + total[7]).astype(bf16)
+    two_up = two_up.astype(f32) + near_up[2:] + by_core(four, none)
+    two_down = two_down.astype(f32) + near_down[2:] + by_core(none, four)
+    two_up = along(two_up.astype(bf16), 2).astype(f32)
+    two_down = along(two_down.astype(bf16), -2).astype(f32)
+    return own.astype(f32) + near_up[:2] + near_down[:2] + two_up + two_down
 
 
 def local(
@@ -332,21 +392,46 @@
     norm_shift, routes, route_logits, gate_weight, up_weight, down_weight, final_gain,
     final_shift,
 ):
-    edge = jnp.concatenate([keys[TOKENS - WINDOW :], values[TOKENS - WINDOW :]], axis=1)
-    edge_docs = documents[TOKENS - WINDOW :].astype(bf16)
-    edge_docs = jnp.pad(edge_docs[None], ((0, 7), (0, LANES)))
-    halo = lax.ppermute(
-        jnp.concatenate([edge, edge_docs], axis=0), SP, [(i - 1, i) for i in range(1, N_SP)]
-    )
+    docs = documents[None]
+    hbm = pl.BlockSpec(memory_space=pltpu.HBM)
+    halo = call(
+        halo_kernel,
+        shape((WINDOW + 8, 2 * LANES), bf16),
+        1_000,
+        140_000,
+        limit=FULL,
+        in_specs=[hbm] * 3,
+        scratch_shapes=[
+            pltpu.VMEM((WINDOW, LANES), bf16),
+            pltpu.VMEM((WINDOW, LANES), bf16),
+            pltpu.VMEM((1, TOKENS), jnp.int32),
+            pltpu.SemaphoreType.DMA((3,)),
+        ],
+    )(keys, values, docs)
+    halo = lax.ppermute(halo, SP, [(i - 1, i) for i in range(1, N_SP)])
     gain, shift = norm_gain[None], norm_shift[None]
-    whole = pl.BlockSpec(memory_space=pltpu.VMEM)
+    prepared = call(
+        prepare_kernel,
+        shape((TOKENS + WINDOW + 16, LANES), bf16),
+        3_000_000,
+        600_000,
+        limit=FULL,
+        in_specs=[hbm] * 8,
+        scratch_shapes=[
+            pltpu.VMEM((TOKENS, LANES), bf16),
+            pltpu.VMEM((1024, LANES), bf16),
+            pltpu.VMEM((1, LANES), f32),
+            pltpu.VMEM((1, LANES), f32),
+            pltpu.VMEM((TOKENS, LANES), bf16),
+            pltpu.VMEM((TOKENS, LANES), bf16),
+            pltpu.VMEM((HEAD_SIZE, TOKENS), bf16),
+            pltpu.VMEM((1, TOKENS), jnp.int32),
+            pltpu.SemaphoreType.DMA((8,)),
+        ],
+    )(residual, out_weight, gain, shift, keys, values, queries.T, docs)
     payload = call(
-        attention_kernel,
-        shape((N_TP, WINDOW + 16, LANES), bf16),
-        60_000_000,
-        1_500_000,
-        in_specs=[pl.BlockSpec(memory_space=pltpu.SMEM)] + [whole] * 9,
-    )(sinks, halo, keys, values, queries, documents[None], residual, out_weight, gain, shift)
+        attention_kernel, shape((N_TP, WINDOW + 16, LANES), bf16), 60_000_000, 1_000_000
+    )(jnp.broadcast_to(sinks[None], (1, LANES)), halo, prepared)
     gathered = to_all(payload)
     first, outgoing, stats, slots, affine = call(
         mix_kernel,
@@ -361,34 +446,26 @@
         1_500_000,
     )(gathered, head_gain[None], out_weight, residual, routes.T)
     arrived = over_sp(outgoing.reshape(N_SP, CAP, LANES)).reshape(SLOTS, LANES)
-    own, mine, other = gather_columns(jnp.concatenate([arrived, stats], axis=0))
-    totals = sum(jnp.sum(v[:, SLOTS:].astype(f32), axis=0) for v in (own, mine, other))
-
-    def tile(count, width):
-        return pl.BlockSpec((count, ROW_TILE, width), lambda i: (0, i, 0))
-
-    def fixed(*dims):
-        return pl.BlockSpec(dims, lambda i: (0,) * len(dims))
-
-    keep, send = call(
+    low = jnp.concatenate([stats, arrived[:HALF]], axis=0)
+    high = jnp.concatenate([stats, arrived[HALF:]], axis=0)
+    stay, partner = by_core(low, high), swap(by_core(high, low))
+    own = by_core(jnp.stack([stay, partner]), jnp.stack([partner, stay]))
+    weights = (gate_weight[0], up_weight[0], down_weight[0])
+    others = tuple(swap(w) for w in weights)
+    pair = shape((2, HALF, LANES), bf16)
+    quad = shape((4, HALF, LANES), bf16)
+    *partial, totals = call(
         expert_kernel,
-        (shape((8, SLOTS, LANES), bf16),) * 2,
+        (quad, quad, pair, pair, pair, pair, shape((STAT_ROWS, LANES), f32)),
         2 * SLOTS * D * FF_LOCAL * 3,
-        12_000_000,
-        grid=(SLOTS // ROW_TILE,),
-        in_specs=[
-            tile(2, LANES),
-            tile(7, LANES),
-            tile(7, LANES),
-            fixed(2, D),
-            fixed(D, FF_LOCAL),
-            fixed(D, FF_LOCAL),
-            fixed(FF_LOCAL, D),
-        ],
-        out_specs=(tile(8, LANES), tile(8, LANES)),
-        scratch_shapes=[pltpu.VMEM((ROW_TILE, D), bf16), pltpu.VMEM((ROW_TILE, D), f32)],
-    )(own, mine, other, affine, gate_weight[0], up_weight[0], down_weight[0])
-    summed = scatter_sum(keep, send)
+        16_000_000,
+        limit=24 << 20,
+        scratch_shapes=[pltpu.VMEM((HALF, D), bf16)],
+    )(*gather_columns(own), affine, *weights, *others)
+    summed = scatter_sum(*partial).astype(bf16)
+    partner = swap(by_core(summed[1], summed[0]))
+    stay = by_core(summed[0], summed[1])
+    summed = by_core(jnp.concatenate([stay, partner]), jnp.concatenate([partner, stay]))
     returned = over_sp(summed.reshape(N_SP, CAP, LANES)).reshape(SLOTS, LANES)
     second, last = call(
         combine_kernel,

time: 192 us -> 184 us (0.958)
  blocking collectives: 64.5 us -> 28.8 us
  starting transfers between devices: 47.5 us -> 77.8 us
  local copies, waits for them, and re-layouts: 8.13 us -> 1.01 us
  waiting for transfers between devices: 51 us -> 56.2 us
    ppermute x1 -> x9, starting transfers between devices: 3.94 us -> 35.8 us  [the longest x8 31.2 us: along(): return lax.ppermute(v, 'y', [(y, (y + distance) % Y) for y in range(Y)])]
    all_to_all x2 -> x1, blocking collectives: 39.6 us -> 14.7 us  [to_all(): return lax.all_to_all(value, TP, 0, 0, tiled=True)]
    ppermute x8 -> x2, waiting for transfers between devices: 32.3 us -> 10.8 us  [onward(): return lax.ppermute(v, TP, pairs)]
    ppermute x1 -> x9, waiting for transfers between devices: 0.01 us -> 19.6 us  [the longest x8 19.6 us: along(): return lax.ppermute(v, 'y', [(y, (y + distance) % Y) for y in range(Y)])]
    all_to_all x0 -> x1, waiting for transfers between devices: none -> 16.5 us  [to_all(): return lax.all_to_all(value, TP, 0, 0, tiled=True)]
    ppermute x8 -> x2, starting transfers between devices: 21 us -> 9.51 us  [onward(): return lax.ppermute(v, TP, pairs)]
    all_to_all x1, blocking collectives: 24.9 us -> 14.1 us  [over_sp(): return lax.all_to_all(value, SP, 0, 0, tiled=True)]
    all_to_all x1, starting transfers between devices: 3.86 us -> 13.5 us  [over_sp(): return lax.all_to_all(value, SP, 0, 0, tiled=True)]
  transfers between devices with their start and end apart: 14 -> 18, of which waited for: 10 -> 11; matrix products, arithmetic and copies ran while one was open for 1% -> 0% of each run, Pallas kernels for 0% -> 2%
where the time goes in v2:
time: 184 us; the launch traced here: 183 us
  starting transfers between devices  77.8 us (42%)
  waiting for transfers between devices  56.2 us (31%)
  blocking collectives  28.8 us (16%)
  Pallas kernels  17.9 us (10%)
    ppermute x8, starting transfers between devices, along(): return lax.ppermute(v, 'y', [(y, (y + distance) % Y) for y in range(Y)])  31.2 us
    ppermute x8, waiting for transfers between devices, along(): return lax.ppermute(v, 'y', [(y, (y + distance) % Y) for y in range(Y)])  19.6 us
    all_to_all x1, waiting for transfers between devices, to_all(): return lax.all_to_all(value, TP, 0, 0, tiled=True)  16.5 us
    all_to_all x1, blocking collectives, to_all(): return lax.all_to_all(value, TP, 0, 0, tiled=True)  14.7 us
    all_to_all x1, blocking collectives, over_sp(): return lax.all_to_all(value, SP, 0, 0, tiled=True)  14.1 us
    all_to_all x1, starting transfers between devices, over_sp(): return lax.all_to_all(value, SP, 0, 0, tiled=True)  13.5 us
    ppermute x5, starting transfers between devices, swap(): return lax.ppermute(v, 'c', [(0, 1), (1, 0)])  10.9 us
    ppermute x2, waiting for transfers between devices, onward(): return lax.ppermute(v, TP, pairs)  10.8 us
  transfers between devices with their start and end apart: 18, of which 11 were waited for; matrix products, arithmetic and copies ran while one was open for 0% of the time, Pallas kernels for 2%

profile of v2, /device:TPU:1, one launch (start us, length us, event | category | flops | bytes accessed | tf_op | source)
XLA Modules:
  0.0 183.4 jit_solution(4280018440444046126)
XLA Ops:
  1.4 4.6 %collective-permute-start = (bf16[136,256]{1,0:T(8,128)(2,1)}, bf16[136,256]{1,0:T(8,128)(2,1)}, u32[]{:S(2)}, u32[]{:S(2)}) collective-permute-start(bf16[136,256]{1,0:T(8,128)(2,1)} %shard_map.163), channel_id=1, source_target_pairs={{0,16},{16,32},{32,48},{48,64},{64,80},{80,96},{96,112},{112,128},... | collective-permute-start | bytes 208904 | tf_op jit(solution)/shard_map/ppermute | solution.py:411
  6.7 2.0 %shard_map.164.prepared_ref = bf16[400,128]{1,0:T(8,128)(2,1)} custom-call(bf16[256,128]{1,0:T(8,128)(2,1)} %residual_ref.1, bf16[1024,128]{1,0:T(8,128)(2,1)} %weight_ref.1, f32[1,128]{1,0:T(1,128)} %bitcast.31, f32[1,128]{1,0:T(1,128)} %bitcast.33, bf16[256,128]{1,0:T(8,128)(2,1)} %keys_hbm.3, bf16[256,128]{1,0:T(8,128)(2,1)} %values_hbm.3, ...), custom_call_target="tpu_custom_call" | custom-call | flops 3000000 | bytes 600000 | tf_op jit(solution)/shard_map/pallas_call | solution.py:413
  9.6 3.1 %shard_map.165 = bf16[16,144,128]{2,1,0:T(8,128)(2,1)} custom-call(f32[1,128]{1,0:T(1,128)S(1)} %broadcast_in_dim.30.sinks_ref, bf16[136,256]{1,0:T(8,128)(2,1)} %collective-permute-done.halo_ref, bf16[400,128]{1,0:T(8,128)(2,1)S(1)} %copy-done.1), custom_call_target="tpu_custom_call" | custom-call | flops 60000000 | bytes 1000000 | tf_op jit(solution)/shard_map/pallas_call | solution.py:432
  12.8 8.1 %all-to-all-start = ((bf16[16,144,128]{2,1,0:T(8,128)(2,1)}), bf16[16,144,128]{2,1,0:T(8,128)(2,1)S(1)}, u32[]{:S(2)}, u32[]{:S(2)}) async-start(bf16[16,144,128]{2,1,0:T(8,128)(2,1)} %shard_map.165), calls=%async_computation | async-start | bytes 1179648 | tf_op jit(solution)/shard_map/all_to_all | solution.py:362
  20.9 2.0 %collective-permute-start.7 = (bf16[2048,384]{1,0:T(8,128)(2,1)S(1)}, bf16[2048,384]{1,0:T(8,128)(2,1)}, u32[]{:S(2)}, u32[]{:S(2)}) collective-permute-start(bf16[2048,384]{1,0:T(8,128)(2,1)S(1)} %bitcast.37), channel_id=1, source_target_pairs={{0,1},{1,0},{2,3},{3,2},{4,5},{5,4},{6,7},{7,6},{8,9},{9,8},{10,11... | collective-permute-start | bytes 4718600 | tf_op jit(solution)/shard_map/ppermute | solution.py:342
  22.9 16.5 %all-to-all-done.gathered_ref = bf16[16,144,128]{2,1,0:T(8,128)(2,1)S(1)} async-done(((bf16[16,144,128]{2,1,0:T(8,128)(2,1)}), bf16[16,144,128]{2,1,0:T(8,128)(2,1)S(1)}, u32[]{:S(2)}, u32[]{:S(2)}) %all-to-all-start) | async-done | bytes 589856 | tf_op jit(solution)/shard_map/all_to_all | solution.py:362
  39.4 1.7 shard_map.166
  41.1 13.5 %all-to-all-start.1 = ((bf16[32,24,128]{2,1,0:T(8,128)(2,1)}), bf16[32,24,128]{2,1,0:T(8,128)(2,1)S(1)}, u32[]{:S(2)}, u32[]{:S(2)}) async-start(bf16[32,24,128]{2,1,0:T(8,128)(2,1)} %bitcast.8), calls=%async_computation.1 | async-start | bytes 393216 | tf_op jit(solution)/shard_map/all_to_all | solution.py:366
  54.6 1.9 %collective-permute-start.8 = (bf16[2048,384]{1,0:T(8,128)(2,1)}, bf16[2048,384]{1,0:T(8,128)(2,1)S(1)}, u32[]{:S(2)}, u32[]{:S(2)}) collective-permute-start(bf16[2048,384]{1,0:T(8,128)(2,1)} %bitcast.39), channel_id=1, source_target_pairs={{0,1},{1,0},{2,3},{3,2},{4,5},{5,4},{6,7},{7,6},{8,9},{9,8},{10,11... | collective-permute-start | bytes 4718600 | tf_op jit(solution)/shard_map/ppermute | solution.py:342
  56.6 2.4 %collective-permute-start.9 = (bf16[384,2048]{1,0:T(8,128)(2,1)}, bf16[384,2048]{1,0:T(8,128)(2,1)}, u32[]{:S(2)}, u32[]{:S(2)}) collective-permute-start(bf16[384,2048]{1,0:T(8,128)(2,1)} %bitcast.41), channel_id=1, source_target_pairs={{0,1},{1,0},{2,3},{3,2},{4,5},{5,4},{6,7},{7,6},{8,9},{9,8},{10,11... | collective-permute-start | bytes 4718600 | tf_op jit(solution)/shard_map/ppermute | solution.py:342
  59.0 7.1 %all-to-all-done.1 = bf16[32,24,128]{2,1,0:T(8,128)(2,1)S(1)} async-done(((bf16[32,24,128]{2,1,0:T(8,128)(2,1)}), bf16[32,24,128]{2,1,0:T(8,128)(2,1)S(1)}, u32[]{:S(2)}, u32[]{:S(2)}) %all-to-all-start.1) | async-done | bytes 196640 | tf_op jit(solution)/shard_map/all_to_all | solution.py:366
  66.2 2.2 %collective-permute-start.1 = (bf16[392,128]{1,0:T(8,128)(2,1)S(1)}, bf16[392,128]{1,0:T(8,128)(2,1)S(1)}, u32[]{:S(2)}, u32[]{:S(2)}) collective-permute-start(bf16[392,128]{1,0:T(8,128)(2,1)S(1)} %fusion.7), channel_id=1, source_target_pairs={{0,1},{1,0},{2,3},{3,2},{4,5},{5,4},{6,7},{7,6},{8,9},{9,8},{10,11... | collective-permute-start | bytes 301064 | tf_op jit(solution)/shard_map/ppermute | solution.py:342
  69.7 3.2 %collective-permute-start.4 = (bf16[2,392,128]{2,1,0:T(8,128)(2,1)S(1)}, bf16[2,392,128]{2,1,0:T(8,128)(2,1)S(1)}, u32[]{:S(2)}, u32[]{:S(2)}) collective-permute-start(bf16[2,392,128]{2,1,0:T(8,128)(2,1)S(1)} %maximum_select_fusion.own_ref), channel_id=1, source_target_pairs={{0,12},{2,14},{4,0},{6,2},{8,4},{10,6},{12,8},{14,10},{1,13},{3,15... | collective-permute-start | bytes 602120 | tf_op jit(solution)/shard_map/ppermute | solution.py:346
  72.9 3.0 %collective-permute-start.2 = (bf16[2,392,128]{2,1,0:T(8,128)(2,1)S(1)}, bf16[2,392,128]{2,1,0:T(8,128)(2,1)S(1)}, u32[]{:S(2)}, u32[]{:S(2)}) collective-permute-start(bf16[2,392,128]{2,1,0:T(8,128)(2,1)S(1)} %maximum_select_fusion.own_ref), channel_id=1, source_target_pairs={{0,4},{2,6},{4,8},{6,10},{8,12},{10,14},{12,0},{14,2},{1,5},{3,7},... | collective-permute-start | bytes 602120 | tf_op jit(solution)/shard_map/ppermute | solution.py:346
  75.9 7.2 %collective-permute-done.4.two_down_ref = bf16[2,392,128]{2,1,0:T(8,128)(2,1)S(1)} collective-permute-done((bf16[2,392,128]{2,1,0:T(8,128)(2,1)S(1)}, bf16[2,392,128]{2,1,0:T(8,128)(2,1)S(1)}, u32[]{:S(2)}, u32[]{:S(2)}) %collective-permute-start.4) | collective-permute-done | bytes 200736 | tf_op jit(solution)/shard_map/ppermute | solution.py:346
  83.1 2.0 %collective-permute-done.2.two_up_ref = bf16[2,392,128]{2,1,0:T(8,128)(2,1)S(1)} collective-permute-done((bf16[2,392,128]{2,1,0:T(8,128)(2,1)S(1)}, bf16[2,392,128]{2,1,0:T(8,128)(2,1)S(1)}, u32[]{:S(2)}, u32[]{:S(2)}) %collective-permute-start.2) | collective-permute-done | bytes 200736 | tf_op jit(solution)/shard_map/ppermute | solution.py:346
  85.2 4.4 %collective-permute-start.5 = (bf16[4,392,128]{2,1,0:T(8,128)(2,1)S(1)}, bf16[4,392,128]{2,1,0:T(8,128)(2,1)S(1)}, u32[]{:S(2)}, u32[]{:S(2)}) collective-permute-start(bf16[4,392,128]{2,1,0:T(8,128)(2,1)S(1)} %get-tuple-element.33), channel_id=1, source_target_pairs={{0,14},{2,0},{4,2},{6,4},{8,6},{10,8},{12,10},{14,12},{1,15},{3,1}... | collective-permute-start | bytes 1204232 | tf_op jit(solution)/shard_map/ppermute | solution.py:346
  89.6 1.9 %collective-permute-start.3 = (bf16[4,392,128]{2,1,0:T(8,128)(2,1)S(1)}, bf16[4,392,128]{2,1,0:T(8,128)(2,1)S(1)}, u32[]{:S(2)}, u32[]{:S(2)}) collective-permute-start(bf16[4,392,128]{2,1,0:T(8,128)(2,1)S(1)} %get-tuple-element.34), channel_id=1, source_target_pairs={{0,2},{2,4},{4,6},{6,8},{8,10},{10,12},{12,14},{14,0},{1,3},{3,5},... | collective-permute-start | bytes 1204232 | tf_op jit(solution)/shard_map/ppermute | solution.py:346
  91.6 4.8 %collective-permute-start.6 = (bf16[2,392,128]{2,1,0:T(8,128)(2,1)S(1)}, bf16[2,392,128]{2,1,0:T(8,128)(2,1)S(1)}, u32[]{:S(2)}, u32[]{:S(2)}) collective-permute-start(bf16[2,392,128]{2,1,0:T(8,128)(2,1)S(1)} %broadcast_select_fusion), channel_id=1, source_target_pairs={{0,4},{1,13},{2,6},{3,15},{4,8},{5,1},{6,10},{7,3},{8,12},{9,5},{1... | collective-permute-start | bytes 602120 | tf_op jit(solution)/shard_map/ppermute | solution.py:354
  96.4 6.6 %collective-permute-done.6.four_ref = bf16[2,392,128]{2,1,0:T(8,128)(2,1)S(1)} collective-permute-done((bf16[2,392,128]{2,1,0:T(8,128)(2,1)S(1)}, bf16[2,392,128]{2,1,0:T(8,128)(2,1)S(1)}, u32[]{:S(2)}, u32[]{:S(2)}) %collective-permute-start.6) | collective-permute-done | bytes 200736 | tf_op jit(solution)/shard_map/ppermute | solution.py:354
  103.0 8.3 %shard_map.167 = (bf16[4,384,128]{2,1,0:T(8,128)(2,1)S(1)}, bf16[4,384,128]{2,1,0:T(8,128)(2,1)S(1)}, bf16[2,384,128]{2,1,0:T(8,128)(2,1)S(1)}, bf16[2,384,128]{...) custom-call(bf16[2,392,128]{2,1,0:T(8,128)(2,1)S(1)} %maximum_select, ...), custom_call_target="tpu_custom_call" | custom-call | flops 3623878656 | bytes 16000000 | tf_op jit(solution)/shard_map/pallas_call | solution.py:457
  111.3 3.7 %collective-permute-start.10 = (bf16[4,384,128]{2,1,0:T(8,128)(2,1)S(1)}, bf16[4,384,128]{2,1,0:T(8,128)(2,1)S(1)}, u32[]{:S(2)}, u32[]{:S(2)}) collective-permute-start(bf16[4,384,128]{2,1,0:T(8,128)(2,1)S(1)} %get-tuple-element.23), channel_id=1, source_target_pairs={{0,2},{2,4},{4,6},{6,8},{8,10},{10,12},{12,14},{14,0},{1,3},{3,5},... | collective-permute-start | bytes 1179656 | tf_op jit(solution)/shard_map/ppermute | solution.py:346
  115.0 2.8 %collective-permute-start.11 = (bf16[4,384,128]{2,1,0:T(8,128)(2,1)S(1)}, bf16[4,384,128]{2,1,0:T(8,128)(2,1)S(1)}, u32[]{:S(2)}, u32[]{:S(2)}) collective-permute-start(bf16[4,384,128]{2,1,0:T(8,128)(2,1)S(1)} %get-tuple-element.24), channel_id=1, source_target_pairs={{0,14},{2,0},{4,2},{6,4},{8,6},{10,8},{12,10},{14,12},{1,15},{3,1}... | collective-permute-start | bytes 1179656 | tf_op jit(solution)/shard_map/ppermute | solution.py:346
  117.8 4.7 %collective-permute-start.12 = (bf16[2,384,128]{2,1,0:T(8,128)(2,1)S(1)}, bf16[2,384,128]{2,1,0:T(8,128)(2,1)S(1)}, u32[]{:S(2)}, u32[]{:S(2)}) collective-permute-start(bf16[2,384,128]{2,1,0:T(8,128)(2,1)S(1)} %get-tuple-element.26), channel_id=1, source_target_pairs={{0,4},{1,13},{2,6},{3,15},{4,8},{5,1},{6,10},{7,3},{8,12},{9,5},{1... | collective-permute-start | bytes 589832 | tf_op jit(solution)/shard_map/ppermute | solution.py:354
  123.9 4.2 %collective-permute-done.12 = bf16[2,384,128]{2,1,0:T(8,128)(2,1)S(1)} collective-permute-done((bf16[2,384,128]{2,1,0:T(8,128)(2,1)S(1)}, bf16[2,384,128]{2,1,0:T(8,128)(2,1)S(1)}, u32[]{:S(2)}, u32[]{:S(2)}) %collective-permute-start.12) | collective-permute-done | bytes 196640 | tf_op jit(solution)/shard_map/ppermute | solution.py:354
  128.3 10.3 %collective-permute-start.13 = (bf16[2,384,128]{2,1,0:T(8,128)(2,1)S(1)}, bf16[2,384,128]{2,1,0:T(8,128)(2,1)S(1)}, u32[]{:S(2)}, u32[]{:S(2)}) collective-permute-start(bf16[2,384,128]{2,1,0:T(8,128)(2,1)S(1)} %get-tuple-element.37), channel_id=1, source_target_pairs={{0,4},{2,6},{4,8},{6,10},{8,12},{10,14},{12,0},{14,2},{1,5},{3,7},... | collective-permute-start | bytes 589832 | tf_op jit(solution)/shard_map/ppermute | solution.py:346
  138.6 1.9 %collective-permute-start.14 = (bf16[2,384,128]{2,1,0:T(8,128)(2,1)S(1)}, bf16[2,384,128]{2,1,0:T(8,128)(2,1)S(1)}, u32[]{:S(2)}, u32[]{:S(2)}) collective-permute-start(bf16[2,384,128]{2,1,0:T(8,128)(2,1)S(1)} %get-tuple-element.38), channel_id=1, source_target_pairs={{0,12},{2,14},{4,0},{6,2},{8,4},{10,6},{12,8},{14,10},{1,13},{3,15... | collective-permute-start | bytes 589832 | tf_op jit(solution)/shard_map/ppermute | solution.py:346
  140.6 5.7 %collective-permute-done.13 = bf16[2,384,128]{2,1,0:T(8,128)(2,1)S(1)} collective-permute-done((bf16[2,384,128]{2,1,0:T(8,128)(2,1)S(1)}, bf16[2,384,128]{2,1,0:T(8,128)(2,1)S(1)}, u32[]{:S(2)}, u32[]{:S(2)}) %collective-permute-start.13) | collective-permute-done | bytes 196640 | tf_op jit(solution)/shard_map/ppermute | solution.py:346
  146.2 3.5 %collective-permute-done.14 = bf16[2,384,128]{2,1,0:T(8,128)(2,1)S(1)} collective-permute-done((bf16[2,384,128]{2,1,0:T(8,128)(2,1)S(1)}, bf16[2,384,128]{2,1,0:T(8,128)(2,1)S(1)}, u32[]{:S(2)}, u32[]{:S(2)}) %collective-permute-start.14) | collective-permute-done | bytes 196640 | tf_op jit(solution)/shard_map/ppermute | solution.py:346
  149.8 2.4 %collective-permute-start.15 = (bf16[384,128]{1,0:T(8,128)(2,1)S(1)}, bf16[384,128]{1,0:T(8,128)(2,1)S(1)}, u32[]{:S(2)}, u32[]{:S(2)}) collective-permute-start(bf16[384,128]{1,0:T(8,128)(2,1)S(1)} %get-tuple-element.36), channel_id=1, source_target_pairs={{0,1},{1,0},{2,3},{3,2},{4,5},{5,4},{6,7},{7,6},{8,9},{9,8},{10,11... | collective-permute-start | bytes 294920 | tf_op jit(solution)/shard_map/ppermute | solution.py:342
  153.2 14.1 %all_to_all.20 = bf16[32,24,128]{2,1,0:T(8,128)(2,1)S(1)} all-to-all(bf16[32,24,128]{2,1,0:T(8,128)(2,1)S(1)} %bitcast.48), channel_id=1, replica_groups=mesh['z'=8,'x'=4,'y'=8,'c'=2] {'z','x'}, dimensions={0} | all-to-all | bytes 393216 | tf_op jit(solution)/shard_map/all_to_all | solution.py:366
  167.9 14.7 %all_to_all.21.stats_ref = f32[16,8,128]{2,1,0:T(8,128)S(1)} all-to-all(f32[16,8,128]{2,1,0:T(8,128)S(1)} %get-tuple-element.31), channel_id=1, replica_groups=mesh['z'=8,'x'=4,'y'=8,'c'=2] {'y','c'}, dimensions={0} | all-to-all | bytes 131072 | tf_op jit(solution)/shard_map/all_to_all | solution.py:362
  (52 shorter events, 7.8 us)
Async XLA Ops:
  1.4 7.2 %collective-permute-start = (bf16[136,256]{1,0:T(8,128)(2,1)}, bf16[136,256]{1,0:T(8,128)(2,1)}, u32[]{:S(2)}, u32[]{:S(2)}) collective-permute-start(bf16[136,256]{1,0:T(8,128)(2,1)} %shard_map.163), channel_id=1, source_target_pairs={{0,16},{16,32},{32,48},{48,64},{64,80},{80,96},{96,112},{112,128},... | collective-permute-start | bytes 208904 | tf_op jit(solution)/shard_map/ppermute | solution.py:411
  8.7 30.7 %copy-start = (bf16[1024,128]{1,0:T(8,128)(2,1)S(1)}, bf16[1024,128]{1,0:T(8,128)(2,1)}, u32[]{:S(2)}) copy-start(bf16[1024,128]{1,0:T(8,128)(2,1)} %weight_ref.1) | copy-start | bytes 786436
  8.7 0.9 copy-start.1
  9.6 11.2 %copy-start.9 = (bf16[1,2048,384]{2,1,0:T(8,128)(2,1)S(1)}, bf16[1,2048,384]{2,1,0:T(8,128)(2,1)}, u32[]{:S(2)}) copy-start(bf16[1,2048,384]{2,1,0:T(8,128)(2,1)} %param.29) | copy-start | bytes 4718596
  9.6 29.8 %copy-start.2 = (bf16[256,128]{1,0:T(8,128)(2,1)S(1)}, bf16[256,128]{1,0:T(8,128)(2,1)}, u32[]{:S(2)}) copy-start(bf16[256,128]{1,0:T(8,128)(2,1)} %residual_ref.1) | copy-start | bytes 196612
  9.6 29.8 %copy-start.3 = (f32[1024]{0:T(1024)S(1)}, f32[1024]{0:T(1024)}, u32[]{:S(2)}) copy-start(f32[1024]{0:T(1024)} %param.23) | copy-start | bytes 12292
  9.6 29.8 %copy-start.4 = (s32[256,2]{0,1:T(2,128)S(1)}, s32[256,2]{0,1:T(2,128)}, u32[]{:S(2)}) copy-start(s32[256,2]{0,1:T(2,128)} %param.27) | copy-start | bytes 6148
  12.8 26.6 %all-to-all-start = ((bf16[16,144,128]{2,1,0:T(8,128)(2,1)}), bf16[16,144,128]{2,1,0:T(8,128)(2,1)S(1)}, u32[]{:S(2)}, u32[]{:S(2)}) async-start(bf16[16,144,128]{2,1,0:T(8,128)(2,1)} %shard_map.165), calls=%async_computation | async-start | bytes 1179648 | tf_op jit(solution)/shard_map/all_to_all | solution.py:362
  20.9 70.7 %collective-permute-start.7 = (bf16[2048,384]{1,0:T(8,128)(2,1)S(1)}, bf16[2048,384]{1,0:T(8,128)(2,1)}, u32[]{:S(2)}, u32[]{:S(2)}) collective-permute-start(bf16[2048,384]{1,0:T(8,128)(2,1)S(1)} %bitcast.37), channel_id=1, source_target_pairs={{0,1},{1,0},{2,3},{3,2},{4,5},{5,4},{6,7},{7,6},{8,9},{9,8},{10,11... | collective-permute-start | bytes 4718600 | tf_op jit(solution)/shard_map/ppermute | solution.py:342
  41.1 25.0 %all-to-all-start.1 = ((bf16[32,24,128]{2,1,0:T(8,128)(2,1)}), bf16[32,24,128]{2,1,0:T(8,128)(2,1)S(1)}, u32[]{:S(2)}, u32[]{:S(2)}) async-start(bf16[32,24,128]{2,1,0:T(8,128)(2,1)} %bitcast.8), calls=%async_computation.1 | async-start | bytes 393216 | tf_op jit(solution)/shard_map/all_to_all | solution.py:366
  54.6 41.7 %collective-permute-start.8 = (bf16[2048,384]{1,0:T(8,128)(2,1)}, bf16[2048,384]{1,0:T(8,128)(2,1)S(1)}, u32[]{:S(2)}, u32[]{:S(2)}) collective-permute-start(bf16[2048,384]{1,0:T(8,128)(2,1)} %bitcast.39), channel_id=1, source_target_pairs={{0,1},{1,0},{2,3},{3,2},{4,5},{5,4},{6,7},{7,6},{8,9},{9,8},{10,11... | collective-permute-start | bytes 4718600 | tf_op jit(solution)/shard_map/ppermute | solution.py:342
  56.6 39.8 %collective-permute-start.9 = (bf16[384,2048]{1,0:T(8,128)(2,1)}, bf16[384,2048]{1,0:T(8,128)(2,1)}, u32[]{:S(2)}, u32[]{:S(2)}) collective-permute-start(bf16[384,2048]{1,0:T(8,128)(2,1)} %bitcast.41), channel_id=1, source_target_pairs={{0,1},{1,0},{2,3},{3,2},{4,5},{5,4},{6,7},{7,6},{8,9},{9,8},{10,11... | collective-permute-start | bytes 4718600 | tf_op jit(solution)/shard_map/ppermute | solution.py:342
  66.1 36.9 %copy-start.11 = (bf16[1,384,2048]{2,1,0:T(8,128)(2,1)S(1)}, bf16[1,384,2048]{2,1,0:T(8,128)(2,1)}, u32[]{:S(2)}) copy-start(bf16[1,384,2048]{2,1,0:T(8,128)(2,1)} %param.31) | copy-start | bytes 4718596
  66.1 36.9 %copy-start.10 = (bf16[1,2048,384]{2,1,0:T(8,128)(2,1)S(1)}, bf16[1,2048,384]{2,1,0:T(8,128)(2,1)}, u32[]{:S(2)}) copy-start(bf16[1,2048,384]{2,1,0:T(8,128)(2,1)} %param.30) | copy-start | bytes 4718596
  66.2 3.5 %collective-permute-start.1 = (bf16[392,128]{1,0:T(8,128)(2,1)S(1)}, bf16[392,128]{1,0:T(8,128)(2,1)S(1)}, u32[]{:S(2)}, u32[]{:S(2)}) collective-permute-start(bf16[392,128]{1,0:T(8,128)(2,1)S(1)} %fusion.7), channel_id=1, source_target_pairs={{0,1},{1,0},{2,3},{3,2},{4,5},{5,4},{6,7},{7,6},{8,9},{9,8},{10,11... | collective-permute-start | bytes 301064 | tf_op jit(solution)/shard_map/ppermute | solution.py:342
  69.7 13.4 %collective-permute-start.4 = (bf16[2,392,128]{2,1,0:T(8,128)(2,1)S(1)}, bf16[2,392,128]{2,1,0:T(8,128)(2,1)S(1)}, u32[]{:S(2)}, u32[]{:S(2)}) collective-permute-start(bf16[2,392,128]{2,1,0:T(8,128)(2,1)S(1)} %maximum_select_fusion.own_ref), channel_id=1, source_target_pairs={{0,12},{2,14},{4,0},{6,2},{8,4},{10,6},{12,8},{14,10},{1,13},{3,15... | collective-permute-start | bytes 602120 | tf_op jit(solution)/shard_map/ppermute | solution.py:346
  72.9 12.2 %collective-permute-start.2 = (bf16[2,392,128]{2,1,0:T(8,128)(2,1)S(1)}, bf16[2,392,128]{2,1,0:T(8,128)(2,1)S(1)}, u32[]{:S(2)}, u32[]{:S(2)}) collective-permute-start(bf16[2,392,128]{2,1,0:T(8,128)(2,1)S(1)} %maximum_select_fusion.own_ref), channel_id=1, source_target_pairs={{0,4},{2,6},{4,8},{6,10},{8,12},{10,14},{12,0},{14,2},{1,5},{3,7},... | collective-permute-start | bytes 602120 | tf_op jit(solution)/shard_map/ppermute | solution.py:346
  85.2 17.8 %collective-permute-start.5 = (bf16[4,392,128]{2,1,0:T(8,128)(2,1)S(1)}, bf16[4,392,128]{2,1,0:T(8,128)(2,1)S(1)}, u32[]{:S(2)}, u32[]{:S(2)}) collective-permute-start(bf16[4,392,128]{2,1,0:T(8,128)(2,1)S(1)} %get-tuple-element.33), channel_id=1, source_target_pairs={{0,14},{2,0},{4,2},{6,4},{8,6},{10,8},{12,10},{14,12},{1,15},{3,1}... | collective-permute-start | bytes 1204232 | tf_op jit(solution)/shard_map/ppermute | solution.py:346
  89.6 13.4 %collective-permute-start.3 = (bf16[4,392,128]{2,1,0:T(8,128)(2,1)S(1)}, bf16[4,392,128]{2,1,0:T(8,128)(2,1)S(1)}, u32[]{:S(2)}, u32[]{:S(2)}) collective-permute-start(bf16[4,392,128]{2,1,0:T(8,128)(2,1)S(1)} %get-tuple-element.34), channel_id=1, source_target_pairs={{0,2},{2,4},{4,6},{6,8},{8,10},{10,12},{12,14},{14,0},{1,3},{3,5},... | collective-permute-start | bytes 1204232 | tf_op jit(solution)/shard_map/ppermute | solution.py:346
  91.6 11.4 %collective-permute-start.6 = (bf16[2,392,128]{2,1,0:T(8,128)(2,1)S(1)}, bf16[2,392,128]{2,1,0:T(8,128)(2,1)S(1)}, u32[]{:S(2)}, u32[]{:S(2)}) collective-permute-start(bf16[2,392,128]{2,1,0:T(8,128)(2,1)S(1)} %broadcast_select_fusion), channel_id=1, source_target_pairs={{0,4},{1,13},{2,6},{3,15},{4,8},{5,1},{6,10},{7,3},{8,12},{9,5},{1... | collective-permute-start | bytes 602120 | tf_op jit(solution)/shard_map/ppermute | solution.py:354
  111.3 11.2 %collective-permute-start.10 = (bf16[4,384,128]{2,1,0:T(8,128)(2,1)S(1)}, bf16[4,384,128]{2,1,0:T(8,128)(2,1)S(1)}, u32[]{:S(2)}, u32[]{:S(2)}) collective-permute-start(bf16[4,384,128]{2,1,0:T(8,128)(2,1)S(1)} %get-tuple-element.23), channel_id=1, source_target_pairs={{0,2},{2,4},{4,6},{6,8},{8,10},{10,12},{12,14},{14,0},{1,3},{3,5},... | collective-permute-start | bytes 1179656 | tf_op jit(solution)/shard_map/ppermute | solution.py:346
  115.0 8.8 %collective-permute-start.11 = (bf16[4,384,128]{2,1,0:T(8,128)(2,1)S(1)}, bf16[4,384,128]{2,1,0:T(8,128)(2,1)S(1)}, u32[]{:S(2)}, u32[]{:S(2)}) collective-permute-start(bf16[4,384,128]{2,1,0:T(8,128)(2,1)S(1)} %get-tuple-element.24), channel_id=1, source_target_pairs={{0,14},{2,0},{4,2},{6,4},{8,6},{10,8},{12,10},{14,12},{1,15},{3,1}... | collective-permute-start | bytes 1179656 | tf_op jit(solution)/shard_map/ppermute | solution.py:346
  117.8 10.3 %collective-permute-start.12 = (bf16[2,384,128]{2,1,0:T(8,128)(2,1)S(1)}, bf16[2,384,128]{2,1,0:T(8,128)(2,1)S(1)}, u32[]{:S(2)}, u32[]{:S(2)}) collective-permute-start(bf16[2,384,128]{2,1,0:T(8,128)(2,1)S(1)} %get-tuple-element.26), channel_id=1, source_target_pairs={{0,4},{1,13},{2,6},{3,15},{4,8},{5,1},{6,10},{7,3},{8,12},{9,5},{1... | collective-permute-start | bytes 589832 | tf_op jit(solution)/shard_map/ppermute | solution.py:354
  128.3 39.1 %copy-start.5 = (f32[128]{0:T(128)S(1)}, f32[128]{0:T(128)}, u32[]{:S(2)}) copy-start(f32[128]{0:T(128)} %param.25) | copy-start | bytes 1540
  128.3 39.1 %copy-start.6 = (f32[128]{0:T(128)S(1)}, f32[128]{0:T(128)}, u32[]{:S(2)}) copy-start(f32[128]{0:T(128)} %param.26) | copy-start | bytes 1540
  128.3 39.1 %copy-start.12 = (f32[256,2]{0,1:T(2,128)S(1)}, f32[256,2]{0,1:T(2,128)}, u32[]{:S(2)}) copy-start(f32[256,2]{0,1:T(2,128)} %param.28) | copy-start | bytes 6148
  128.3 17.9 %collective-permute-start.13 = (bf16[2,384,128]{2,1,0:T(8,128)(2,1)S(1)}, bf16[2,384,128]{2,1,0:T(8,128)(2,1)S(1)}, u32[]{:S(2)}, u32[]{:S(2)}) collective-permute-start(bf16[2,384,128]{2,1,0:T(8,128)(2,1)S(1)} %get-tuple-element.37), channel_id=1, source_target_pairs={{0,4},{2,6},{4,8},{6,10},{8,12},{10,14},{12,0},{14,2},{1,5},{3,7},... | collective-permute-start | bytes 589832 | tf_op jit(solution)/shard_map/ppermute | solution.py:346
  138.6 11.0 %collective-permute-start.14 = (bf16[2,384,128]{2,1,0:T(8,128)(2,1)S(1)}, bf16[2,384,128]{2,1,0:T(8,128)(2,1)S(1)}, u32[]{:S(2)}, u32[]{:S(2)}) collective-permute-start(bf16[2,384,128]{2,1,0:T(8,128)(2,1)S(1)} %get-tuple-element.38), channel_id=1, source_target_pairs={{0,12},{2,14},{4,0},{6,2},{8,4},{10,6},{12,8},{14,10},{1,13},{3,15... | collective-permute-start | bytes 589832 | tf_op jit(solution)/shard_map/ppermute | solution.py:346
  149.7 32.9 %copy-start.7 = (f32[128]{0:T(128)S(1)}, f32[128]{0:T(128)}, u32[]{:S(2)}) copy-start(f32[128]{0:T(128)} %param.32) | copy-start | bytes 1540
  149.7 32.9 %copy-start.8 = (f32[128]{0:T(128)S(1)}, f32[128]{0:T(128)}, u32[]{:S(2)}) copy-start(f32[128]{0:T(128)} %param.33) | copy-start | bytes 1540
  149.8 3.3 %collective-permute-start.15 = (bf16[384,128]{1,0:T(8,128)(2,1)S(1)}, bf16[384,128]{1,0:T(8,128)(2,1)S(1)}, u32[]{:S(2)}, u32[]{:S(2)}) collective-permute-start(bf16[384,128]{1,0:T(8,128)(2,1)S(1)} %get-tuple-element.36), channel_id=1, source_target_pairs={{0,1},{1,0},{2,3},{3,2},{4,5},{5,4},{6,7},{7,6},{8,9},{9,8},{10,11... | collective-permute-start | bytes 294920 | tf_op jit(solution)/shard_map/ppermute | solution.py:342

commit v3 on v2

--- a/solution.py
+++ b/solution.py
@@ -88,9 +88,9 @@
 
 def prepare_kernel(
     residual_hbm, weight_hbm, gain_hbm, shift_hbm, keys_hbm, values_hbm, queries_hbm, docs_hbm,
-    out_ref,
+    sinks_hbm, out_ref,
     residual_ref, weight_ref, gain_ref, shift_ref, keys_ref, values_ref, queries_ref, docs_ref,
-    sems,
+    sinks_ref, sems,
 ):
     fetch(
         (
@@ -102,6 +102,7 @@
             (docs_hbm, docs_ref),
             (gain_hbm, gain_ref),
             (shift_hbm, shift_ref),
+            (sinks_hbm, sinks_ref),
         ),
         sems,
     )
@@ -113,6 +114,8 @@
     rows += [*high_low(gain_ref[...]), *high_low(shift_ref[...])]
     docs = docs_ref[...].astype(f32)
     rows += [docs[:, :WINDOW], docs[:, WINDOW:]]
+    sink = jnp.broadcast_to(sinks_ref[...], (1, LANES))
+    rows += [*high_low(sink), jnp.zeros((6, LANES), f32)]
     pick = kv_head() == 0
     heads = [head_of(pick, keys_ref[...]), head_of(pick, values_ref[...])]
     out_ref[:TOKENS, :] = jnp.concatenate(heads, axis=1)
@@ -132,9 +135,8 @@
     return jnp.where(pick, block[:, :HEAD_SIZE], block[:, HEAD_SIZE:]).astype(bf16)
 
 
-def attention_kernel(sinks_ref, halo_ref, prepared_ref, out_ref):
+def attention_kernel(halo_ref, prepared_ref, out_ref):
     first_block = (lax.axis_index("z") * 4 + lax.axis_index("x")) == 0
-    sink = sinks_ref[0:1, 0:1]
     pick = kv_head() == 0
     keys = [head_of(pick, halo_ref[:WINDOW, :LANES])]
     vals = [head_of(pick, halo_ref[:WINDOW, LANES:])]
@@ -143,7 +145,9 @@
         keys.append(prepared_ref[part, :HEAD_SIZE])
         vals.append(prepared_ref[part, HEAD_SIZE:])
     queries = prepared_ref[TOKENS : TOKENS + WINDOW, :]
-    tail = prepared_ref[TOKENS + WINDOW :, :]
+    tail = prepared_ref[TOKENS + WINDOW : TOKENS + WINDOW + 16, :]
+    sink = prepared_ref[TOKENS + WINDOW + 16 :, :].astype(f32)
+    sink = (sink[0:1] + sink[1:2])[:, 0:1]
     halo_docs = halo_ref[WINDOW : WINDOW + 8, :LANES].astype(f32)[0:1]
     halo_docs = jnp.where(first_block, -1.0, halo_docs)
     docs = tail.astype(f32)
@@ -170,16 +174,22 @@
             + jnp.dot(here, vals[i + 1], preferred_element_type=f32)
         )
     attended = jnp.concatenate(blocks, axis=1).astype(bf16)
-    for t in range(N_TP):
+    for t in range(Y):
         out_ref[t, :WINDOW, :] = attended
         out_ref[t, WINDOW:, :] = tail
 
 
 def mix_kernel(
-    gathered_ref, head_gain_ref, weight_ref, residual_ref, routes_ref,
+    mine_ref, other_ref, head_gain_ref, weight_ref, residual_ref, routes_ref,
     first_ref, outgoing_ref, stats_ref, slots_ref, affine_ref,
 ):
-    tails = [gathered_ref[t, WINDOW:, :].astype(f32) for t in range(N_TP)]
+    even = lax.axis_index("c") == 0
+
+    def sent_by(t, *at):
+        pair = mine_ref[t // 2, *at].astype(f32), other_ref[t // 2, *at].astype(f32)
+        return jnp.where(even, *pair) if t % 2 == 0 else jnp.where(even, *pair[::-1])
+
+    tails = [sent_by(t, slice(WINDOW, None), slice(None)) for t in range(N_TP)]
     total = functools.reduce(jnp.add, tails)
     for t in range(N_TP):
         lanes = slice(t * LANES, (t + 1) * LANES)
@@ -191,7 +201,7 @@
     for h in range(2):
         lanes = slice(h * HEAD_SIZE, (h + 1) * HEAD_SIZE)
         heads = jnp.concatenate(
-            [gathered_ref[t, :WINDOW, lanes].astype(f32) for t in range(N_TP)], axis=1
+            [sent_by(t, slice(0, WINDOW), lanes) for t in range(N_TP)], axis=1
         )
         spread = jnp.mean(heads * heads, axis=1, keepdims=True)
         scaled = (heads * lax.rsqrt(spread + NORM_EPS) * head_gain).astype(bf16)
@@ -231,38 +241,47 @@
 
 
 def expert_kernel(
-    own_ref, near_up_ref, near_down_ref, two_up_ref, two_down_ref, four_ref, affine_ref,
+    own_ref, mine_ref, other_ref, affine_ref,
     gate_ref, up_ref, down_ref, gate_other_ref, up_other_ref, down_other_ref,
     to_near_up_ref, to_near_down_ref, to_two_up_ref, to_two_down_ref, to_four_ref, to_own_ref,
     totals_ref, rows_ref,
 ):
-    y = lax.axis_index("y")
+    y, c = lax.axis_index("y"), lax.axis_index("c")
+    way = 1 - 2 * c
+    held = pl.ds(pl.multiple_of(c * HALF, HALF), HALF)
 
     def lanes_of(away):
         at = lax.rem(y + away + Y, Y) * 2 * LANES
         return pl.multiple_of(at, 2 * LANES)
 
-    blocks = []
-    for ref, i, away in (
-        (own_ref, 0, 0), (two_up_ref, 0, -2), (two_down_ref, 0, 2), (near_up_ref, 0, -1),
-        (near_up_ref, 2, -3), (near_down_ref, 0, 1), (near_down_ref, 2, 3), (four_ref, 0, 4),
-    ):
+    def lanes_at(away, half):
+        return pl.ds(pl.multiple_of(lanes_of(away) + half * LANES, LANES), LANES)
+
+    blocks = [(own_ref, h, held, lanes_at(0, h)) for h in range(2)]
+    for k in range(1, 4):
         for h in range(2):
-            blocks.append((ref, i + h, pl.ds(pl.multiple_of(lanes_of(away) + h * LANES, LANES), LANES)))
+            blocks.append((mine_ref, 2 * k - 2 + h, held, lanes_at(-way * k, h)))
+            blocks.append((other_ref, 2 * k - 2 + h, slice(0, HALF), lanes_at(way * k, h)))
+    blocks.append((mine_ref, 6, held, lanes_at(4, c)))
+    blocks.append((other_ref, 6, slice(0, HALF), lanes_at(4, 1 - c)))
     totals_ref[...] = functools.reduce(
-        jnp.add, [ref[i, :STAT_ROWS, :].astype(f32) for ref, i, _ in blocks]
+        jnp.add,
+        [
+            ref[i, HALF if ref is other_ref else SLOTS :, :].astype(f32)
+            for ref, i, _, _ in blocks
+        ],
     )
     total = square = 0.0
-    for ref, i, _ in blocks:
-        v = ref[i, STAT_ROWS:, :].astype(f32)
+    for ref, i, rows, _ in blocks:
+        v = ref[i, rows, :].astype(f32)
         total = total + v
         square = square + v * v
     center = jnp.sum(total, axis=1, keepdims=True) * (1.0 / D)
     spread = jnp.sum(square, axis=1, keepdims=True) * (1.0 / D) - center * center
     scale = lax.rsqrt(spread + NORM_EPS)
     offset = center * scale
-    for ref, i, lanes in blocks:
-        v = ref[i, STAT_ROWS:, :].astype(f32) * scale - offset
+    for ref, i, rows, lanes in blocks:
+        v = ref[i, rows, :].astype(f32) * scale - offset
         rows_ref[:, lanes] = (v * affine_ref[0:1, lanes] + affine_ref[1:2, lanes]).astype(bf16)
     middles = []
     for g, u in ((gate_ref, up_ref), (gate_other_ref, up_other_ref)):
@@ -367,12 +386,13 @@
 
 
 def gather_columns(own):
-    two_up = along(own, 2)
-    two_down = along(own, -2)
-    near_up = along(jnp.concatenate([own, two_up], axis=0), 1)
-    near_down = along(jnp.concatenate([own, two_down], axis=0), -1)
-    four = onward(by_core(two_up, two_down), 2)
-    return own, near_up, near_down, two_up, two_down, four
+    two = onward(own, 2)
+    one = onward(own, 1)
+    three = onward(two, 1)
+    four = onward(by_core(two[0:1], two[1:2]), 2)
+    mine = jnp.concatenate([one, two, three, four], axis=0)
+    passed = by_core(mine[:, HALF:SLOTS], mine[:, :HALF])
+    return own, mine, swap(jnp.concatenate([passed, mine[:, SLOTS:]], axis=1))
 
 
 def scatter_sum(near_up, near_down, two_up, two_down, four, own):
@@ -399,7 +419,7 @@
         shape((WINDOW + 8, 2 * LANES), bf16),
         1_000,
         140_000,
-        limit=FULL,
+        limit=FULL - 160_000,
         in_specs=[hbm] * 3,
         scratch_shapes=[
             pltpu.VMEM((WINDOW, LANES), bf16),
@@ -412,11 +432,11 @@
     gain, shift = norm_gain[None], norm_shift[None]
     prepared = call(
         prepare_kernel,
-        shape((TOKENS + WINDOW + 16, LANES), bf16),
+        shape((TOKENS + WINDOW + 24, LANES), bf16),
         3_000_000,
         600_000,
-        limit=FULL,
-        in_specs=[hbm] * 8,
+        limit=FULL - 240_000,
+        in_specs=[hbm] * 9,
         scratch_shapes=[
             pltpu.VMEM((TOKENS, LANES), bf16),
             pltpu.VMEM((1024, LANES), bf16),
@@ -426,13 +446,14 @@
             pltpu.VMEM((TOKENS, LANES), bf16),
             pltpu.VMEM((HEAD_SIZE, TOKENS), bf16),
             pltpu.VMEM((1, TOKENS), jnp.int32),
-            pltpu.SemaphoreType.DMA((8,)),
+            pltpu.VMEM((1, 1), f32),
+            pltpu.SemaphoreType.DMA((9,)),
         ],
-    )(residual, out_weight, gain, shift, keys, values, queries.T, docs)
+    )(residual, out_weight, gain, shift, keys, values, queries.T, docs, sinks[None])
     payload = call(
-        attention_kernel, shape((N_TP, WINDOW + 16, LANES), bf16), 60_000_000, 1_000_000
-    )(jnp.broadcast_to(sinks[None], (1, LANES)), halo, prepared)
-    gathered = to_all(payload)
+        attention_kernel, shape((Y, WINDOW + 16, LANES), bf16), 60_000_000, 1_000_000
+    )(halo, prepared)
+    gathered = lax.all_to_all(payload, "y", 0, 0, tiled=True)
     first, outgoing, stats, slots, affine = call(
         mix_kernel,
         (
@@ -444,12 +465,11 @@
         ),
         140_000_000,
         1_500_000,
-    )(gathered, head_gain[None], out_weight, residual, routes.T)
+    )(gathered, swap(gathered), head_gain[None], out_weight, residual, routes.T)
     arrived = over_sp(outgoing.reshape(N_SP, CAP, LANES)).reshape(SLOTS, LANES)
-    low = jnp.concatenate([stats, arrived[:HALF]], axis=0)
-    high = jnp.concatenate([stats, arrived[HALF:]], axis=0)
-    stay, partner = by_core(low, high), swap(by_core(high, low))
-    own = by_core(jnp.stack([stay, partner]), jnp.stack([partner, stay]))
+    block = jnp.concatenate([arrived, stats], axis=0)
+    partner = swap(block)
+    own = by_core(jnp.stack([block, partner]), jnp.stack([partner, block]))
     weights = (gate_weight[0], up_weight[0], down_weight[0])
     others = tuple(swap(w) for w in weights)
     pair = shape((2, HALF, LANES), bf16)

time: 184 us -> 176 us (0.957)
  blocking collectives: 28.8 us -> 69.4 us
  waiting for transfers between devices: 56.2 us -> 33.1 us
  starting transfers between devices: 77.8 us -> 55.1 us
  Pallas kernels: 17.9 us -> 13.7 us
    all_to_all x2 -> x0, waiting for transfers between devices: 23.6 us -> none  [the longest x1 16.5 us: to_all(): return lax.all_to_all(value, TP, 0, 0, tiled=True)]
    all_to_all x1 -> x2, blocking collectives: 14.1 us -> 37.5 us  [over_sp(): return lax.all_to_all(value, SP, 0, 0, tiled=True)]
    all_to_all x2 -> x0, starting transfers between devices: 21.6 us -> none  [the longest x1 13.5 us: over_sp(): return lax.all_to_all(value, SP, 0, 0, tiled=True)]
    all_to_all x0 -> x1, blocking collectives: none -> 17.3 us  [local(): gathered = lax.all_to_all(payload, 'y', 0, 0, tiled=True)]
    ppermute x8 -> x4, starting transfers between devices: 31.2 us -> 14.5 us  [along(): return lax.ppermute(v, 'y', [(y, (y + distance) % Y) for y in range(Y)])]
    ppermute x5 -> x7, starting transfers between devices: 10.9 us -> 25.7 us  [swap(): return lax.ppermute(v, 'c', [(0, 1), (1, 0)])]
    ppermute x8 -> x4, waiting for transfers between devices: 19.6 us -> 13.6 us  [along(): return lax.ppermute(v, 'y', [(y, (y + distance) % Y) for y in range(Y)])]
    ppermute x2 -> x5, waiting for transfers between devices: 10.8 us -> 14.6 us  [onward(): return lax.ppermute(v, TP, pairs)]
  transfers between devices with their start and end apart: 18 -> 17, of which waited for: 11 -> 13; matrix products, arithmetic and copies ran while one was open for 0% -> 0% of each run, Pallas kernels for 2% -> 1%
where the time goes in v3:
time: 176 us; the launch traced here: 175 us
  blocking collectives  69.4 us (39%)
  starting transfers between devices  55.1 us (31%)
  waiting for transfers between devices  33.1 us (19%)
  Pallas kernels  13.7 us (8%)
  local copies, waits for them, and re-layouts  2.05 us (1%)
    all_to_all x2, blocking collectives, over_sp(): return lax.all_to_all(value, SP, 0, 0, tiled=True)  37.5 us
    ppermute x7, starting transfers between devices, swap(): return lax.ppermute(v, 'c', [(0, 1), (1, 0)])  25.7 us
    all_to_all x1, blocking collectives, local(): gathered = lax.all_to_all(payload, 'y', 0, 0, tiled=True)  17.3 us
    all_to_all x1, blocking collectives, to_all(): return lax.all_to_all(value, TP, 0, 0, tiled=True)  14.6 us
    ppermute x5, waiting for transfers between devices, onward(): return lax.ppermute(v, TP, pairs)  14.6 us
    ppermute x4, starting transfers between devices, along(): return lax.ppermute(v, 'y', [(y, (y + distance) % Y) for y in range(Y)])  14.5 us
    ppermute x4, waiting for transfers between devices, along(): return lax.ppermute(v, 'y', [(y, (y + distance) % Y) for y in range(Y)])  13.6 us
    ppermute x5, starting transfers between devices, onward(): return lax.ppermute(v, TP, pairs)  11 us
  transfers between devices with their start and end apart: 17, of which 13 were waited for; matrix products, arithmetic and copies ran while one was open for 0% of the time, Pallas kernels for 1%

profile of v3, /device:TPU:1, one launch (start us, length us, event | category | flops | bytes accessed | tf_op | source)
XLA Modules:
  0.0 175.2 jit_solution(285580825584143002)
XLA Ops:
  0.0 1.5 shard_map.163
  1.5 3.9 %collective-permute-start = (bf16[136,256]{1,0:T(8,128)(2,1)}, bf16[136,256]{1,0:T(8,128)(2,1)S(1)}, u32[]{:S(2)}, u32[]{:S(2)}) collective-permute-start(bf16[136,256]{1,0:T(8,128)(2,1)} %shard_map.163), channel_id=1, source_target_pairs={{0,16},{16,32},{32,48},{48,64},{64,80},{80,96},{96,112},{112,128},... | collective-permute-start | bytes 208904 | tf_op jit(solution)/shard_map/ppermute | solution.py:431
  6.1 2.0 %shard_map.164.prepared_ref = bf16[408,128]{1,0:T(8,128)(2,1)} custom-call(bf16[256,128]{1,0:T(8,128)(2,1)} %residual_ref.1, bf16[1024,128]{1,0:T(8,128)(2,1)} %weight_ref.1, f32[1,128]{1,0:T(1,128)} %bitcast.31, f32[1,128]{1,0:T(1,128)} %bitcast.33, bf16[256,128]{1,0:T(8,128)(2,1)} %keys_hbm.3, bf16[256,128]{1,0:T(8,128)(2,1)} %values_hbm.3, ...), custom_call_target="tpu_custom_call" | custom-call | flops 3000000 | bytes 600000 | tf_op jit(solution)/shard_map/pallas_call | solution.py:433
  9.0 1.3 shard_map.165
  10.3 17.3 %all_to_all.20.mine_ref = bf16[8,144,128]{2,1,0:T(8,128)(2,1)S(1)} all-to-all(bf16[8,144,128]{2,1,0:T(8,128)(2,1)S(1)} %shard_map.165), channel_id=1, replica_groups=mesh['z'=8,'x'=4,'y'=8,'c'=2] {'y'}, dimensions={0} | all-to-all | bytes 589824 | tf_op jit(solution)/shard_map/all_to_all | solution.py:456
  27.7 4.7 %collective-permute-start.1 = (bf16[8,144,128]{2,1,0:T(8,128)(2,1)S(1)}, bf16[8,144,128]{2,1,0:T(8,128)(2,1)S(1)}, u32[]{:S(2)}, u32[]{:S(2)}) collective-permute-start(bf16[8,144,128]{2,1,0:T(8,128)(2,1)S(1)} %all_to_all.20.mine_ref), channel_id=1, source_target_pairs={{0,1},{1,0},{2,3},{3,2},{4,5},{5,4},{6,7},{7,6},{8,9},{9,8},{10,11... | collective-permute-start | bytes 884744 | tf_op jit(solution)/shard_map/ppermute | solution.py:361
  35.7 23.6 %all_to_all.21 = bf16[32,24,128]{2,1,0:T(8,128)(2,1)S(1)} all-to-all(bf16[32,24,128]{2,1,0:T(8,128)(2,1)S(1)} %bitcast.26), channel_id=1, replica_groups=mesh['z'=8,'x'=4,'y'=8,'c'=2] {'z','x'}, dimensions={0} | all-to-all | bytes 393216 | tf_op jit(solution)/shard_map/all_to_all | solution.py:385
  59.3 3.9 %collective-permute-start.2 = (bf16[776,128]{1,0:T(8,128)(2,1)S(1)}, bf16[776,128]{1,0:T(8,128)(2,1)S(1)}, u32[]{:S(2)}, u32[]{:S(2)}) collective-permute-start(bf16[776,128]{1,0:T(8,128)(2,1)S(1)} %get-tuple-element.34), channel_id=1, source_target_pairs={{0,1},{1,0},{2,3},{3,2},{4,5},{5,4},{6,7},{7,6},{8,9},{9,8},{10,11... | collective-permute-start | bytes 595976 | tf_op jit(solution)/shard_map/ppermute | solution.py:361
  64.3 2.1 %collective-permute-start.4 = (bf16[2,776,128]{2,1,0:T(8,128)(2,1)S(1)}, bf16[2,776,128]{2,1,0:T(8,128)(2,1)S(1)}, u32[]{:S(2)}, u32[]{:S(2)}) collective-permute-start(bf16[2,776,128]{2,1,0:T(8,128)(2,1)S(1)} %maximum_select_fusion.own_ref), channel_id=1, source_target_pairs={{0,4},{1,13},{2,6},{3,15},{4,8},{5,1},{6,10},{7,3},{8,12},{9,5},{1... | collective-permute-start | bytes 1191944 | tf_op jit(solution)/shard_map/ppermute | solution.py:373
  66.4 2.2 %collective-permute-start.3 = (bf16[2,776,128]{2,1,0:T(8,128)(2,1)S(1)}, bf16[2,776,128]{2,1,0:T(8,128)(2,1)S(1)}, u32[]{:S(2)}, u32[]{:S(2)}) collective-permute-start(bf16[2,776,128]{2,1,0:T(8,128)(2,1)S(1)} %maximum_select_fusion.own_ref), channel_id=1, source_target_pairs={{0,2},{1,15},{2,4},{3,1},{4,6},{5,3},{6,8},{7,5},{8,10},{9,7},{10,... | collective-permute-start | bytes 1191944 | tf_op jit(solution)/shard_map/ppermute | solution.py:373
  68.7 2.8 %collective-permute-start.8 = (bf16[2048,384]{1,0:T(8,128)(2,1)S(1)}, bf16[2048,384]{1,0:T(8,128)(2,1)S(1)}, u32[]{:S(2)}, u32[]{:S(2)}) collective-permute-start(bf16[2048,384]{1,0:T(8,128)(2,1)S(1)} %bitcast.35), channel_id=1, source_target_pairs={{0,1},{1,0},{2,3},{3,2},{4,5},{5,4},{6,7},{7,6},{8,9},{9,8},{10,11... | collective-permute-start | bytes 4718600 | tf_op jit(solution)/shard_map/ppermute | solution.py:361
  71.5 1.9 %collective-permute-start.9 = (bf16[2048,384]{1,0:T(8,128)(2,1)}, bf16[2048,384]{1,0:T(8,128)(2,1)S(1)}, u32[]{:S(2)}, u32[]{:S(2)}) collective-permute-start(bf16[2048,384]{1,0:T(8,128)(2,1)} %bitcast.37), channel_id=1, source_target_pairs={{0,1},{1,0},{2,3},{3,2},{4,5},{5,4},{6,7},{7,6},{8,9},{9,8},{10,11... | collective-permute-start | bytes 4718600 | tf_op jit(solution)/shard_map/ppermute | solution.py:361
  73.4 2.4 %collective-permute-start.10 = (bf16[384,2048]{1,0:T(8,128)(2,1)}, bf16[384,2048]{1,0:T(8,128)(2,1)S(1)}, u32[]{:S(2)}, u32[]{:S(2)}) collective-permute-start(bf16[384,2048]{1,0:T(8,128)(2,1)} %bitcast.39), channel_id=1, source_target_pairs={{0,1},{1,0},{2,3},{3,2},{4,5},{5,4},{6,7},{7,6},{8,9},{9,8},{10,11... | collective-permute-start | bytes 4718600 | tf_op jit(solution)/shard_map/ppermute | solution.py:361
  75.8 2.5 %collective-permute-done.4 = bf16[2,776,128]{2,1,0:T(8,128)(2,1)S(1)} collective-permute-done((bf16[2,776,128]{2,1,0:T(8,128)(2,1)S(1)}, bf16[2,776,128]{2,1,0:T(8,128)(2,1)S(1)}, u32[]{:S(2)}, u32[]{:S(2)}) %collective-permute-start.4) | collective-permute-done | bytes 397344 | tf_op jit(solution)/shard_map/ppermute | solution.py:373
  78.4 1.9 %collective-permute-start.5 = (bf16[2,776,128]{2,1,0:T(8,128)(2,1)S(1)}, bf16[2,776,128]{2,1,0:T(8,128)(2,1)S(1)}, u32[]{:S(2)}, u32[]{:S(2)}) collective-permute-start(bf16[2,776,128]{2,1,0:T(8,128)(2,1)S(1)} %collective-permute-done.4), channel_id=1, source_target_pairs={{0,2},{1,15},{2,4},{3,1},{4,6},{5,3},{6,8},{7,5},{8,10},{9,7},{10,... | collective-permute-start | bytes 1191944 | tf_op jit(solution)/shard_map/ppermute | solution.py:373
  81.5 2.8 %collective-permute-start.6 = (bf16[1,776,128]{2,1,0:T(8,128)(2,1)S(1)}, bf16[1,776,128]{2,1,0:T(8,128)(2,1)S(1)}, u32[]{:S(2)}, u32[]{:S(2)}) collective-permute-start(bf16[1,776,128]{2,1,0:T(8,128)(2,1)S(1)} %slice_select_fusion.1), channel_id=1, source_target_pairs={{0,4},{1,13},{2,6},{3,15},{4,8},{5,1},{6,10},{7,3},{8,12},{9,5},{1... | collective-permute-start | bytes 595976 | tf_op jit(solution)/shard_map/ppermute | solution.py:373
  84.4 3.9 %collective-permute-done.5 = bf16[2,776,128]{2,1,0:T(8,128)(2,1)S(1)} collective-permute-done((bf16[2,776,128]{2,1,0:T(8,128)(2,1)S(1)}, bf16[2,776,128]{2,1,0:T(8,128)(2,1)S(1)}, u32[]{:S(2)}, u32[]{:S(2)}) %collective-permute-start.5) | collective-permute-done | bytes 397344 | tf_op jit(solution)/shard_map/ppermute | solution.py:373
  88.4 2.0 %collective-permute-done.6 = bf16[1,776,128]{2,1,0:T(8,128)(2,1)S(1)} collective-permute-done((bf16[1,776,128]{2,1,0:T(8,128)(2,1)S(1)}, bf16[1,776,128]{2,1,0:T(8,128)(2,1)S(1)}, u32[]{:S(2)}, u32[]{:S(2)}) %collective-permute-start.6) | collective-permute-done | bytes 198688 | tf_op jit(solution)/shard_map/ppermute | solution.py:373
  90.6 7.7 %collective-permute-start.7 = (bf16[7,392,128]{2,1,0:T(8,128)(2,1)S(1)}, bf16[7,392,128]{2,1,0:T(8,128)(2,1)S(1)}, u32[]{:S(2)}, u32[]{:S(2)}) collective-permute-start(bf16[7,392,128]{2,1,0:T(8,128)(2,1)S(1)} %pad_maximum_fusion), channel_id=1, source_target_pairs={{0,1},{1,0},{2,3},{3,2},{4,5},{5,4},{6,7},{7,6},{8,9},{9,8},{10,11... | collective-permute-start | bytes 2107400 | tf_op jit(solution)/shard_map/ppermute | solution.py:361
  98.3 1.7 collective-permute-done.7.other_ref
  100.1 6.5 %shard_map.167 = (bf16[4,384,128]{2,1,0:T(8,128)(2,1)S(1)}, bf16[4,384,128]{2,1,0:T(8,128)(2,1)S(1)}, bf16[2,384,128]{2,1,0:T(8,128)(2,1)S(1)}, bf16[2,384,128]{...) custom-call(bf16[2,776,128]{2,1,0:T(8,128)(2,1)S(1)} %maximum_select, ...), custom_call_target="tpu_custom_call" | custom-call | flops 3623878656 | bytes 16000000 | tf_op jit(solution)/shard_map/pallas_call | solution.py:477
  106.5 1.9 %collective-permute-start.11 = (bf16[4,384,128]{2,1,0:T(8,128)(2,1)S(1)}, bf16[4,384,128]{2,1,0:T(8,128)(2,1)S(1)}, u32[]{:S(2)}, u32[]{:S(2)}) collective-permute-start(bf16[4,384,128]{2,1,0:T(8,128)(2,1)S(1)} %get-tuple-element.23), channel_id=1, source_target_pairs={{0,2},{2,4},{4,6},{6,8},{8,10},{10,12},{12,14},{14,0},{1,3},{3,5},... | collective-permute-start | bytes 1179656 | tf_op jit(solution)/shard_map/ppermute | solution.py:365
  108.5 4.6 %collective-permute-start.12 = (bf16[4,384,128]{2,1,0:T(8,128)(2,1)S(1)}, bf16[4,384,128]{2,1,0:T(8,128)(2,1)S(1)}, u32[]{:S(2)}, u32[]{:S(2)}) collective-permute-start(bf16[4,384,128]{2,1,0:T(8,128)(2,1)S(1)} %get-tuple-element.24), channel_id=1, source_target_pairs={{0,14},{2,0},{4,2},{6,4},{8,6},{10,8},{12,10},{14,12},{1,15},{3,1}... | collective-permute-start | bytes 1179656 | tf_op jit(solution)/shard_map/ppermute | solution.py:365
  113.0 1.9 %collective-permute-start.13 = (bf16[2,384,128]{2,1,0:T(8,128)(2,1)S(1)}, bf16[2,384,128]{2,1,0:T(8,128)(2,1)S(1)}, u32[]{:S(2)}, u32[]{:S(2)}) collective-permute-start(bf16[2,384,128]{2,1,0:T(8,128)(2,1)S(1)} %get-tuple-element.26), channel_id=1, source_target_pairs={{0,4},{1,13},{2,6},{3,15},{4,8},{5,1},{6,10},{7,3},{8,12},{9,5},{1... | collective-permute-start | bytes 589832 | tf_op jit(solution)/shard_map/ppermute | solution.py:373
  115.0 5.0 %collective-permute-done.11 = bf16[4,384,128]{2,1,0:T(8,128)(2,1)S(1)} collective-permute-done((bf16[4,384,128]{2,1,0:T(8,128)(2,1)S(1)}, bf16[4,384,128]{2,1,0:T(8,128)(2,1)S(1)}, u32[]{:S(2)}, u32[]{:S(2)}) %collective-permute-start.11) | collective-permute-done | bytes 393248 | tf_op jit(solution)/shard_map/ppermute | solution.py:365
  121.2 4.9 %collective-permute-done.13 = bf16[2,384,128]{2,1,0:T(8,128)(2,1)S(1)} collective-permute-done((bf16[2,384,128]{2,1,0:T(8,128)(2,1)S(1)}, bf16[2,384,128]{2,1,0:T(8,128)(2,1)S(1)}, u32[]{:S(2)}, u32[]{:S(2)}) %collective-permute-start.13) | collective-permute-done | bytes 196640 | tf_op jit(solution)/shard_map/ppermute | solution.py:373
  126.4 3.1 %collective-permute-start.14 = (bf16[2,384,128]{2,1,0:T(8,128)(2,1)S(1)}, bf16[2,384,128]{2,1,0:T(8,128)(2,1)S(1)}, u32[]{:S(2)}, u32[]{:S(2)}) collective-permute-start(bf16[2,384,128]{2,1,0:T(8,128)(2,1)S(1)} %get-tuple-element.37), channel_id=1, source_target_pairs={{0,4},{2,6},{4,8},{6,10},{8,12},{10,14},{12,0},{14,2},{1,5},{3,7},... | collective-permute-start | bytes 589832 | tf_op jit(solution)/shard_map/ppermute | solution.py:365
  129.4 4.9 %collective-permute-start.15 = (bf16[2,384,128]{2,1,0:T(8,128)(2,1)S(1)}, bf16[2,384,128]{2,1,0:T(8,128)(2,1)S(1)}, u32[]{:S(2)}, u32[]{:S(2)}) collective-permute-start(bf16[2,384,128]{2,1,0:T(8,128)(2,1)S(1)} %get-tuple-element.38), channel_id=1, source_target_pairs={{0,12},{2,14},{4,0},{6,2},{8,4},{10,6},{12,8},{14,10},{1,13},{3,15... | collective-permute-start | bytes 589832 | tf_op jit(solution)/shard_map/ppermute | solution.py:365
  134.4 6.8 %collective-permute-done.14 = bf16[2,384,128]{2,1,0:T(8,128)(2,1)S(1)} collective-permute-done((bf16[2,384,128]{2,1,0:T(8,128)(2,1)S(1)}, bf16[2,384,128]{2,1,0:T(8,128)(2,1)S(1)}, u32[]{:S(2)}, u32[]{:S(2)}) %collective-permute-start.14) | collective-permute-done | bytes 196640 | tf_op jit(solution)/shard_map/ppermute | solution.py:365
  142.0 2.4 %collective-permute-start.16 = (bf16[384,128]{1,0:T(8,128)(2,1)S(1)}, bf16[384,128]{1,0:T(8,128)(2,1)S(1)}, u32[]{:S(2)}, u32[]{:S(2)}) collective-permute-start(bf16[384,128]{1,0:T(8,128)(2,1)S(1)} %get-tuple-element.36), channel_id=1, source_target_pairs={{0,1},{1,0},{2,3},{3,2},{4,5},{5,4},{6,7},{7,6},{8,9},{9,8},{10,11... | collective-permute-start | bytes 294920 | tf_op jit(solution)/shard_map/ppermute | solution.py:361
  145.3 13.9 %all_to_all.22 = bf16[32,24,128]{2,1,0:T(8,128)(2,1)S(1)} all-to-all(bf16[32,24,128]{2,1,0:T(8,128)(2,1)S(1)} %bitcast.42), channel_id=1, replica_groups=mesh['z'=8,'x'=4,'y'=8,'c'=2] {'z','x'}, dimensions={0} | all-to-all | bytes 393216 | tf_op jit(solution)/shard_map/all_to_all | solution.py:385
  159.8 14.6 %all_to_all.23.stats_ref = f32[16,8,128]{2,1,0:T(8,128)S(1)} all-to-all(f32[16,8,128]{2,1,0:T(8,128)S(1)} %get-tuple-element.31), channel_id=1, replica_groups=mesh['z'=8,'x'=4,'y'=8,'c'=2] {'y','c'}, dimensions={0} | all-to-all | bytes 131072 | tf_op jit(solution)/shard_map/all_to_all | solution.py:381
  (55 shorter events, 11.5 us)
Async XLA Ops:
  0.0 33.6 %copy-start.2 = (bf16[256,128]{1,0:T(8,128)(2,1)S(1)}, bf16[256,128]{1,0:T(8,128)(2,1)}, u32[]{:S(2)}) copy-start(bf16[256,128]{1,0:T(8,128)(2,1)} %residual_ref.1) | copy-start | bytes 196612
  0.0 33.6 %copy-start.4 = (s32[256,2]{0,1:T(2,128)S(1)}, s32[256,2]{0,1:T(2,128)}, u32[]{:S(2)}) copy-start(s32[256,2]{0,1:T(2,128)} %param.27) | copy-start | bytes 6148
  0.0 33.6 %copy-start.3 = (f32[1024]{0:T(1024)S(1)}, f32[1024]{0:T(1024)}, u32[]{:S(2)}) copy-start(f32[1024]{0:T(1024)} %param.23) | copy-start | bytes 12292
  1.5 6.6 %collective-permute-start = (bf16[136,256]{1,0:T(8,128)(2,1)}, bf16[136,256]{1,0:T(8,128)(2,1)S(1)}, u32[]{:S(2)}, u32[]{:S(2)}) collective-permute-start(bf16[136,256]{1,0:T(8,128)(2,1)} %shard_map.163), channel_id=1, source_target_pairs={{0,16},{16,32},{32,48},{48,64},{64,80},{80,96},{96,112},{112,128},... | collective-permute-start | bytes 208904 | tf_op jit(solution)/shard_map/ppermute | solution.py:431
  8.1 0.9 copy-start.1
  27.7 5.9 %collective-permute-start.1 = (bf16[8,144,128]{2,1,0:T(8,128)(2,1)S(1)}, bf16[8,144,128]{2,1,0:T(8,128)(2,1)S(1)}, u32[]{:S(2)}, u32[]{:S(2)}) collective-permute-start(bf16[8,144,128]{2,1,0:T(8,128)(2,1)S(1)} %all_to_all.20.mine_ref), channel_id=1, source_target_pairs={{0,1},{1,0},{2,3},{3,2},{4,5},{5,4},{6,7},{7,6},{8,9},{9,8},{10,11... | collective-permute-start | bytes 884744 | tf_op jit(solution)/shard_map/ppermute | solution.py:361
  33.6 1.0 copy-start
  34.5 34.1 %copy-start.9 = (bf16[1,2048,384]{2,1,0:T(8,128)(2,1)S(1)}, bf16[1,2048,384]{2,1,0:T(8,128)(2,1)}, u32[]{:S(2)}) copy-start(bf16[1,2048,384]{2,1,0:T(8,128)(2,1)} %param.29) | copy-start | bytes 4718596
  59.3 4.9 %collective-permute-start.2 = (bf16[776,128]{1,0:T(8,128)(2,1)S(1)}, bf16[776,128]{1,0:T(8,128)(2,1)S(1)}, u32[]{:S(2)}, u32[]{:S(2)}) collective-permute-start(bf16[776,128]{1,0:T(8,128)(2,1)S(1)} %get-tuple-element.34), channel_id=1, source_target_pairs={{0,1},{1,0},{2,3},{3,2},{4,5},{5,4},{6,7},{7,6},{8,9},{9,8},{10,11... | collective-permute-start | bytes 595976 | tf_op jit(solution)/shard_map/ppermute | solution.py:361
  64.3 14.1 %collective-permute-start.4 = (bf16[2,776,128]{2,1,0:T(8,128)(2,1)S(1)}, bf16[2,776,128]{2,1,0:T(8,128)(2,1)S(1)}, u32[]{:S(2)}, u32[]{:S(2)}) collective-permute-start(bf16[2,776,128]{2,1,0:T(8,128)(2,1)S(1)} %maximum_select_fusion.own_ref), channel_id=1, source_target_pairs={{0,4},{1,13},{2,6},{3,15},{4,8},{5,1},{6,10},{7,3},{8,12},{9,5},{1... | collective-permute-start | bytes 1191944 | tf_op jit(solution)/shard_map/ppermute | solution.py:373
  66.4 15.1 %collective-permute-start.3 = (bf16[2,776,128]{2,1,0:T(8,128)(2,1)S(1)}, bf16[2,776,128]{2,1,0:T(8,128)(2,1)S(1)}, u32[]{:S(2)}, u32[]{:S(2)}) collective-permute-start(bf16[2,776,128]{2,1,0:T(8,128)(2,1)S(1)} %maximum_select_fusion.own_ref), channel_id=1, source_target_pairs={{0,2},{1,15},{2,4},{3,1},{4,6},{5,3},{6,8},{7,5},{8,10},{9,7},{10,... | collective-permute-start | bytes 1191944 | tf_op jit(solution)/shard_map/ppermute | solution.py:373
  68.7 29.6 %collective-permute-start.8 = (bf16[2048,384]{1,0:T(8,128)(2,1)S(1)}, bf16[2048,384]{1,0:T(8,128)(2,1)S(1)}, u32[]{:S(2)}, u32[]{:S(2)}) collective-permute-start(bf16[2048,384]{1,0:T(8,128)(2,1)S(1)} %bitcast.35), channel_id=1, source_target_pairs={{0,1},{1,0},{2,3},{3,2},{4,5},{5,4},{6,7},{7,6},{8,9},{9,8},{10,11... | collective-permute-start | bytes 4718600 | tf_op jit(solution)/shard_map/ppermute | solution.py:361
  71.5 26.8 %collective-permute-start.9 = (bf16[2048,384]{1,0:T(8,128)(2,1)}, bf16[2048,384]{1,0:T(8,128)(2,1)S(1)}, u32[]{:S(2)}, u32[]{:S(2)}) collective-permute-start(bf16[2048,384]{1,0:T(8,128)(2,1)} %bitcast.37), channel_id=1, source_target_pairs={{0,1},{1,0},{2,3},{3,2},{4,5},{5,4},{6,7},{7,6},{8,9},{9,8},{10,11... | collective-permute-start | bytes 4718600 | tf_op jit(solution)/shard_map/ppermute | solution.py:361
  73.4 24.9 %collective-permute-start.10 = (bf16[384,2048]{1,0:T(8,128)(2,1)}, bf16[384,2048]{1,0:T(8,128)(2,1)S(1)}, u32[]{:S(2)}, u32[]{:S(2)}) collective-permute-start(bf16[384,2048]{1,0:T(8,128)(2,1)} %bitcast.39), channel_id=1, source_target_pairs={{0,1},{1,0},{2,3},{3,2},{4,5},{5,4},{6,7},{7,6},{8,9},{9,8},{10,11... | collective-permute-start | bytes 4718600 | tf_op jit(solution)/shard_map/ppermute | solution.py:361
  78.4 10.0 %collective-permute-start.5 = (bf16[2,776,128]{2,1,0:T(8,128)(2,1)S(1)}, bf16[2,776,128]{2,1,0:T(8,128)(2,1)S(1)}, u32[]{:S(2)}, u32[]{:S(2)}) collective-permute-start(bf16[2,776,128]{2,1,0:T(8,128)(2,1)S(1)} %collective-permute-done.4), channel_id=1, source_target_pairs={{0,2},{1,15},{2,4},{3,1},{4,6},{5,3},{6,8},{7,5},{8,10},{9,7},{10,... | collective-permute-start | bytes 1191944 | tf_op jit(solution)/shard_map/ppermute | solution.py:373
  81.5 8.9 %collective-permute-start.6 = (bf16[1,776,128]{2,1,0:T(8,128)(2,1)S(1)}, bf16[1,776,128]{2,1,0:T(8,128)(2,1)S(1)}, u32[]{:S(2)}, u32[]{:S(2)}) collective-permute-start(bf16[1,776,128]{2,1,0:T(8,128)(2,1)S(1)} %slice_select_fusion.1), channel_id=1, source_target_pairs={{0,4},{1,13},{2,6},{3,15},{4,8},{5,1},{6,10},{7,3},{8,12},{9,5},{1... | collective-permute-start | bytes 595976 | tf_op jit(solution)/shard_map/ppermute | solution.py:373
  90.4 9.6 %copy-start.10 = (bf16[1,2048,384]{2,1,0:T(8,128)(2,1)S(1)}, bf16[1,2048,384]{2,1,0:T(8,128)(2,1)}, u32[]{:S(2)}) copy-start(bf16[1,2048,384]{2,1,0:T(8,128)(2,1)} %param.30) | copy-start | bytes 4718596
  90.4 9.6 %copy-start.11 = (bf16[1,384,2048]{2,1,0:T(8,128)(2,1)S(1)}, bf16[1,384,2048]{2,1,0:T(8,128)(2,1)}, u32[]{:S(2)}) copy-start(bf16[1,384,2048]{2,1,0:T(8,128)(2,1)} %param.31) | copy-start | bytes 4718596
  90.6 9.5 %collective-permute-start.7 = (bf16[7,392,128]{2,1,0:T(8,128)(2,1)S(1)}, bf16[7,392,128]{2,1,0:T(8,128)(2,1)S(1)}, u32[]{:S(2)}, u32[]{:S(2)}) collective-permute-start(bf16[7,392,128]{2,1,0:T(8,128)(2,1)S(1)} %pad_maximum_fusion), channel_id=1, source_target_pairs={{0,1},{1,0},{2,3},{3,2},{4,5},{5,4},{6,7},{7,6},{8,9},{9,8},{10,11... | collective-permute-start | bytes 2107400 | tf_op jit(solution)/shard_map/ppermute | solution.py:361
  106.5 13.4 %collective-permute-start.11 = (bf16[4,384,128]{2,1,0:T(8,128)(2,1)S(1)}, bf16[4,384,128]{2,1,0:T(8,128)(2,1)S(1)}, u32[]{:S(2)}, u32[]{:S(2)}) collective-permute-start(bf16[4,384,128]{2,1,0:T(8,128)(2,1)S(1)} %get-tuple-element.23), channel_id=1, source_target_pairs={{0,2},{2,4},{4,6},{6,8},{8,10},{10,12},{12,14},{14,0},{1,3},{3,5},... | collective-permute-start | bytes 1179656 | tf_op jit(solution)/shard_map/ppermute | solution.py:365
  108.5 12.7 %collective-permute-start.12 = (bf16[4,384,128]{2,1,0:T(8,128)(2,1)S(1)}, bf16[4,384,128]{2,1,0:T(8,128)(2,1)S(1)}, u32[]{:S(2)}, u32[]{:S(2)}) collective-permute-start(bf16[4,384,128]{2,1,0:T(8,128)(2,1)S(1)} %get-tuple-element.24), channel_id=1, source_target_pairs={{0,14},{2,0},{4,2},{6,4},{8,6},{10,8},{12,10},{14,12},{1,15},{3,1}... | collective-permute-start | bytes 1179656 | tf_op jit(solution)/shard_map/ppermute | solution.py:365
  113.0 13.1 %collective-permute-start.13 = (bf16[2,384,128]{2,1,0:T(8,128)(2,1)S(1)}, bf16[2,384,128]{2,1,0:T(8,128)(2,1)S(1)}, u32[]{:S(2)}, u32[]{:S(2)}) collective-permute-start(bf16[2,384,128]{2,1,0:T(8,128)(2,1)S(1)} %get-tuple-element.26), channel_id=1, source_target_pairs={{0,4},{1,13},{2,6},{3,15},{4,8},{5,1},{6,10},{7,3},{8,12},{9,5},{1... | collective-permute-start | bytes 589832 | tf_op jit(solution)/shard_map/ppermute | solution.py:373
  126.3 32.9 %copy-start.7 = (f32[128]{0:T(128)S(1)}, f32[128]{0:T(128)}, u32[]{:S(2)}) copy-start(f32[128]{0:T(128)} %param.25) | copy-start | bytes 1540
  126.3 32.9 %copy-start.8 = (f32[128]{0:T(128)S(1)}, f32[128]{0:T(128)}, u32[]{:S(2)}) copy-start(f32[128]{0:T(128)} %param.26) | copy-start | bytes 1540
  126.3 32.9 %copy-start.12 = (f32[256,2]{0,1:T(2,128)S(1)}, f32[256,2]{0,1:T(2,128)}, u32[]{:S(2)}) copy-start(f32[256,2]{0,1:T(2,128)} %param.28) | copy-start | bytes 6148
  126.4 14.8 %collective-permute-start.14 = (bf16[2,384,128]{2,1,0:T(8,128)(2,1)S(1)}, bf16[2,384,128]{2,1,0:T(8,128)(2,1)S(1)}, u32[]{:S(2)}, u32[]{:S(2)}) collective-permute-start(bf16[2,384,128]{2,1,0:T(8,128)(2,1)S(1)} %get-tuple-element.37), channel_id=1, source_target_pairs={{0,4},{2,6},{4,8},{6,10},{8,12},{10,14},{12,0},{14,2},{1,5},{3,7},... | collective-permute-start | bytes 589832 | tf_op jit(solution)/shard_map/ppermute | solution.py:365
  129.4 12.4 %collective-permute-start.15 = (bf16[2,384,128]{2,1,0:T(8,128)(2,1)S(1)}, bf16[2,384,128]{2,1,0:T(8,128)(2,1)S(1)}, u32[]{:S(2)}, u32[]{:S(2)}) collective-permute-start(bf16[2,384,128]{2,1,0:T(8,128)(2,1)S(1)} %get-tuple-element.38), channel_id=1, source_target_pairs={{0,12},{2,14},{4,0},{6,2},{8,4},{10,6},{12,8},{14,10},{1,13},{3,15... | collective-permute-start | bytes 589832 | tf_op jit(solution)/shard_map/ppermute | solution.py:365
  141.8 32.5 %copy-start.5 = (f32[128]{0:T(128)S(1)}, f32[128]{0:T(128)}, u32[]{:S(2)}) copy-start(f32[128]{0:T(128)} %param.32) | copy-start | bytes 1540
  141.8 32.5 %copy-start.6 = (f32[128]{0:T(128)S(1)}, f32[128]{0:T(128)}, u32[]{:S(2)}) copy-start(f32[128]{0:T(128)} %param.33) | copy-start | bytes 1540
  142.0 3.3 %collective-permute-start.16 = (bf16[384,128]{1,0:T(8,128)(2,1)S(1)}, bf16[384,128]{1,0:T(8,128)(2,1)S(1)}, u32[]{:S(2)}, u32[]{:S(2)}) collective-permute-start(bf16[384,128]{1,0:T(8,128)(2,1)S(1)} %get-tuple-element.36), channel_id=1, source_target_pairs={{0,1},{1,0},{2,3},{3,2},{4,5},{5,4},{6,7},{7,6},{8,9},{9,8},{10,11... | collective-permute-start | bytes 294920 | tf_op jit(solution)/shard_map/ppermute | solution.py:361

commit v4 on v3

--- a/solution.py
+++ b/solution.py
@@ -240,11 +240,29 @@
     outgoing_ref[...] = jnp.dot(place, source, preferred_element_type=f32).astype(bf16)
 
 
+def block_kernel(arrived_ref, stats_ref, out_ref):
+    out_ref[:SLOTS, :] = arrived_ref[...]
+    out_ref[SLOTS:, :] = stats_ref[...]
+
+
+def own_kernel(block_ref, partner_ref, out_ref):
+    even = lax.axis_index("c") == 0
+
+    @pl.when(even)
+    def _():
+        out_ref[0] = block_ref[...]
+        out_ref[1] = partner_ref[...]
+
+    @pl.when(jnp.logical_not(even))
+    def _():
+        out_ref[0] = partner_ref[...]
+        out_ref[1] = block_ref[...]
+
+
 def expert_kernel(
     own_ref, mine_ref, other_ref, affine_ref,
     gate_ref, up_ref, down_ref, gate_other_ref, up_other_ref, down_other_ref,
-    to_near_up_ref, to_near_down_ref, to_two_up_ref, to_two_down_ref, to_four_ref, to_own_ref,
-    totals_ref, rows_ref,
+    middle_ref, send_ref, totals_ref, rows_ref,
 ):
     y, c = lax.axis_index("y"), lax.axis_index("c")
     way = 1 - 2 * c
@@ -283,21 +301,33 @@
     for ref, i, rows, lanes in blocks:
         v = ref[i, rows, :].astype(f32) * scale - offset
         rows_ref[:, lanes] = (v * affine_ref[0:1, lanes] + affine_ref[1:2, lanes]).astype(bf16)
-    middles = []
-    for g, u in ((gate_ref, up_ref), (gate_other_ref, up_other_ref)):
+    for i, (g, u) in enumerate(((gate_ref, up_ref), (gate_other_ref, up_other_ref))):
         gate = jnp.dot(rows_ref[...], g[...], preferred_element_type=f32)
         up = jnp.dot(rows_ref[...], u[...], preferred_element_type=f32)
-        middles.append((gate / (1.0 + jnp.exp(-gate)) * up).astype(bf16))
-    for ref, i, away in (
-        (to_near_up_ref, 0, 1), (to_near_up_ref, 2, 3), (to_near_down_ref, 0, -1),
-        (to_near_down_ref, 2, -3), (to_four_ref, 0, 4), (to_two_up_ref, 0, 2),
-        (to_two_down_ref, 0, -2), (to_own_ref, 0, 0),
-    ):
-        lanes = pl.ds(lanes_of(away), 2 * LANES)
-        out = jnp.dot(middles[0], down_ref[:, lanes], preferred_element_type=f32)
-        out = out + jnp.dot(middles[1], down_other_ref[:, lanes], preferred_element_type=f32)
-        ref[i] = out[:, :LANES].astype(bf16)
-        ref[i + 1] = out[:, LANES:].astype(bf16)
+        middle_ref[i] = (gate / (1.0 + jnp.exp(-gate)) * up).astype(bf16)
+    project(middle_ref, down_ref, down_other_ref, send_ref, -way, 1 - c)
+
+
+def project(middle_ref, down_ref, down_other_ref, out_ref, way, half):
+    y = lax.axis_index("y")
+
+    def down(away, begin, width):
+        at = lax.rem(y + away + Y, Y) * 2 * LANES + begin
+        lanes = pl.ds(pl.multiple_of(at, LANES), width)
+        out = jnp.dot(middle_ref[0], down_ref[:, lanes], preferred_element_type=f32)
+        return out + jnp.dot(middle_ref[1], down_other_ref[:, lanes], preferred_element_type=f32)
+
+    for k in range(1, 4):
+        out = down(way * k, 0, 2 * LANES)
+        out_ref[2 * k - 2] = out[:, :LANES].astype(bf16)
+        out_ref[2 * k - 1] = out[:, LANES:].astype(bf16)
+    out_ref[6] = down(4, half * LANES, LANES).astype(bf16)
+    out_ref[7] = down(0, half * LANES, LANES).astype(bf16)
+
+
+def keep_kernel(middle_ref, down_ref, down_other_ref, keep_ref):
+    c = lax.axis_index("c")
+    project(middle_ref, down_ref, down_other_ref, keep_ref, 1 - 2 * c, c)
 
 
 def combine_kernel(
@@ -361,10 +391,6 @@
     return lax.ppermute(v, "c", [(0, 1), (1, 0)])
 
 
-def along(v, distance):
-    return lax.ppermute(v, "y", [(y, (y + distance) % Y) for y in range(Y)])
-
-
 def onward(v, distance):
     pairs = []
     for y in range(Y):
@@ -395,16 +421,23 @@
     return own, mine, swap(jnp.concatenate([passed, mine[:, SLOTS:]], axis=1))
 
 
-def scatter_sum(near_up, near_down, two_up, two_down, four, own):
-    four = onward(four, 2).astype(f32)
-    near_up = along(near_up, 1).astype(f32)
-    near_down = along(near_down, -1).astype(f32)
+def scatter_sum(keep, passed):
+    def full(begin, end):
+        own, other = keep[begin:end], passed[begin:end]
+        return by_core(
+            jnp.concatenate([own, other], axis=1), jnp.concatenate([other, own], axis=1)
+        )
+
+    three = onward(full(4, 6), 1)
+    four = onward(full(6, 7), 2)
+    one = onward(full(0, 2), 1)
+    four = four.astype(f32)
     none = jnp.zeros_like(four)
-    two_up = two_up.astype(f32) + near_up[2:] + by_core(four, none)
-    two_down = two_down.astype(f32) + near_down[2:] + by_core(none, four)
-    two_up = along(two_up.astype(bf16), 2).astype(f32)
-    two_down = along(two_down.astype(bf16), -2).astype(f32)
-    return own.astype(f32) + near_up[:2] + near_down[:2] + two_up + two_down
+    four = by_core(jnp.concatenate([four, none]), jnp.concatenate([none, four]))
+    two = onward((full(2, 4).astype(f32) + three.astype(f32) + four).astype(bf16), 2)
+    side = one.astype(f32) + two.astype(f32)
+    other = swap(by_core(side[1], side[0]).astype(bf16))
+    return by_core(side[0], side[1]) + other.astype(f32) + full(7, 8)[0].astype(f32)
 
 
 def local(
@@ -467,25 +500,29 @@
         1_500_000,
     )(gathered, swap(gathered), head_gain[None], out_weight, residual, routes.T)
     arrived = over_sp(outgoing.reshape(N_SP, CAP, LANES)).reshape(SLOTS, LANES)
-    block = jnp.concatenate([arrived, stats], axis=0)
-    partner = swap(block)
-    own = by_core(jnp.stack([block, partner]), jnp.stack([partner, block]))
+    rows = SLOTS + STAT_ROWS
+    block = call(block_kernel, shape((rows, LANES), bf16), 1_000, 400_000, limit=8 << 20)(
+        arrived, stats
+    )
+    own = call(own_kernel, shape((2, rows, LANES), bf16), 1_000, 800_000, limit=8 << 20)(
+        block, swap(block)
+    )
     weights = (gate_weight[0], up_weight[0], down_weight[0])
     others = tuple(swap(w) for w in weights)
-    pair = shape((2, HALF, LANES), bf16)
-    quad = shape((4, HALF, LANES), bf16)
-    *partial, totals = call(
+    blocks = shape((8, HALF, LANES), bf16)
+    middle, send, totals = call(
         expert_kernel,
-        (quad, quad, pair, pair, pair, pair, shape((STAT_ROWS, LANES), f32)),
-        2 * SLOTS * D * FF_LOCAL * 3,
-        16_000_000,
+        (shape((2, HALF, FF_LOCAL), bf16), blocks, shape((STAT_ROWS, LANES), f32)),
+        2 * HALF * D * FF_LOCAL * 5,
+        14_000_000,
         limit=24 << 20,
         scratch_shapes=[pltpu.VMEM((HALF, D), bf16)],
     )(*gather_columns(own), affine, *weights, *others)
-    summed = scatter_sum(*partial).astype(bf16)
-    partner = swap(by_core(summed[1], summed[0]))
-    stay = by_core(summed[0], summed[1])
-    summed = by_core(jnp.concatenate([stay, partner]), jnp.concatenate([partner, stay]))
+    passed = swap(send)
+    keep = call(keep_kernel, blocks, 2 * HALF * D * FF_LOCAL, 5_000_000)(
+        middle, weights[2], others[2]
+    )
+    summed = scatter_sum(keep, passed).astype(bf16)
     returned = over_sp(summed.reshape(N_SP, CAP, LANES)).reshape(SLOTS, LANES)
     second, last = call(
         combine_kernel,

time: 176 us -> 177 us (level)
  waiting for transfers between devices: 33.1 us -> 27.6 us
  Pallas kernels: 13.7 us -> 17 us
  blocking collectives: 69.4 us -> 67 us
  local copies, waits for them, and re-layouts: 2.05 us -> 4.17 us
    ppermute x4 -> x0, starting transfers between devices: 14.5 us -> none  [along(): return lax.ppermute(v, 'y', [(y, (y + distance) % Y) for y in range(Y)])]
    ppermute x4 -> x0, waiting for transfers between devices: 13.6 us -> none  [along(): return lax.ppermute(v, 'y', [(y, (y + distance) % Y) for y in range(Y)])]
    ppermute x5 -> x8, starting transfers between devices: 11 us -> 20.9 us  [onward(): return lax.ppermute(v, TP, pairs)]
    ppermute x5 -> x8, waiting for transfers between devices: 14.6 us -> 21.9 us  [onward(): return lax.ppermute(v, TP, pairs)]
    ppermute x7 -> x8, starting transfers between devices: 25.7 us -> 31.9 us  [swap(): return lax.ppermute(v, 'c', [(0, 1), (1, 0)])]
    pallas_call x1 -> x4, Pallas kernels: 6.46 us -> 9.72 us  [the longest x1 8.56 us: local(): call(expert_kernel, (shape((2, HALF, FF_LOCAL), bf16), blocks, shape((STA...]
    all_to_all x1, blocking collectives: 14.6 us -> 12.2 us  [to_all(): return lax.all_to_all(value, TP, 0, 0, tiled=True)]
    unnamed x29 -> x33, local copies, waits for them, and re-layouts: 2.02 us -> 4.03 us
  transfers between devices with their start and end apart: 17 -> 17, of which waited for: 13 -> 11; matrix products, arithmetic and copies ran while one was open for 0% -> 2% of each run, Pallas kernels for 1% -> 2%
where the time goes in v4:
time: 177 us; the launch traced here: 176 us
  blocking collectives  67 us (38%)
  starting transfers between devices  56.8 us (32%)
  waiting for transfers between devices  27.6 us (16%)
  Pallas kernels  17 us (10%)
  local copies, waits for them, and re-layouts  4.17 us (2%)
  other arithmetic  1.93 us (1%)
    all_to_all x2, blocking collectives, over_sp(): return lax.all_to_all(value, SP, 0, 0, tiled=True)  37.5 us
    ppermute x8, starting transfers between devices, swap(): return lax.ppermute(v, 'c', [(0, 1), (1, 0)])  31.9 us
    ppermute x8, waiting for transfers between devices, onward(): return lax.ppermute(v, TP, pairs)  21.9 us
    ppermute x8, starting transfers between devices, onward(): return lax.ppermute(v, TP, pairs)  20.9 us
    all_to_all x1, blocking collectives, local(): gathered = lax.all_to_all(payload, 'y', 0, 0, tiled=True)  17.3 us
    all_to_all x1, blocking collectives, to_all(): return lax.all_to_all(value, TP, 0, 0, tiled=True)  12.2 us
    pallas_call x1, Pallas kernels, local(): call(expert_kernel, (shape((2, HALF, FF_LOCAL), bf16), blocks, shape((STA...  8.56 us
    ppermute x8, waiting for transfers between devices, swap(): return lax.ppermute(v, 'c', [(0, 1), (1, 0)])  5.72 us
  transfers between devices with their start and end apart: 17, of which 11 were waited for; matrix products, arithmetic and copies ran while one was open for 2% of the time, Pallas kernels for 2%

profile of v4, /device:TPU:1, one launch (start us, length us, event | category | flops | bytes accessed | tf_op | source)
XLA Modules:
  0.0 175.6 jit_solution(4330305100568130814)
XLA Ops:
  0.0 1.5 shard_map.163
  1.5 3.9 %collective-permute-start = (bf16[136,256]{1,0:T(8,128)(2,1)}, bf16[136,256]{1,0:T(8,128)(2,1)S(1)}, u32[]{:S(2)}, u32[]{:S(2)}) collective-permute-start(bf16[136,256]{1,0:T(8,128)(2,1)} %shard_map.163), channel_id=1, source_target_pairs={{0,16},{16,32},{32,48},{48,64},{64,80},{80,96},{96,112},{112,128},... | collective-permute-start | bytes 208904 | tf_op jit(solution)/shard_map/ppermute | solution.py:464
  6.1 2.0 %shard_map.164.prepared_ref = bf16[408,128]{1,0:T(8,128)(2,1)} custom-call(bf16[256,128]{1,0:T(8,128)(2,1)} %residual_ref.1, bf16[1024,128]{1,0:T(8,128)(2,1)} %weight_ref.1, f32[1,128]{1,0:T(1,128)} %bitcast.40, f32[1,128]{1,0:T(1,128)} %bitcast.42, bf16[256,128]{1,0:T(8,128)(2,1)} %keys_hbm.3, bf16[256,128]{1,0:T(8,128)(2,1)} %values_hbm.3, ...), custom_call_target="tpu_custom_call" | custom-call | flops 3000000 | bytes 600000 | tf_op jit(solution)/shard_map/pallas_call | solution.py:466
  9.0 1.3 shard_map.165
  10.3 17.3 %all_to_all.20.mine_ref = bf16[8,144,128]{2,1,0:T(8,128)(2,1)S(1)} all-to-all(bf16[8,144,128]{2,1,0:T(8,128)(2,1)S(1)} %shard_map.165), channel_id=1, replica_groups=mesh['z'=8,'x'=4,'y'=8,'c'=2] {'y'}, dimensions={0} | all-to-all | bytes 589824 | tf_op jit(solution)/shard_map/all_to_all | solution.py:489
  27.7 4.8 %collective-permute-start.1 = (bf16[8,144,128]{2,1,0:T(8,128)(2,1)S(1)}, bf16[8,144,128]{2,1,0:T(8,128)(2,1)S(1)}, u32[]{:S(2)}, u32[]{:S(2)}) collective-permute-start(bf16[8,144,128]{2,1,0:T(8,128)(2,1)S(1)} %all_to_all.20.mine_ref), channel_id=1, source_target_pairs={{0,1},{1,0},{2,3},{3,2},{4,5},{5,4},{6,7},{7,6},{8,9},{9,8},{10,11... | collective-permute-start | bytes 884744 | tf_op jit(solution)/shard_map/ppermute | solution.py:391
  32.5 1.2 collective-permute-done.1.other_ref
  35.8 23.6 %all_to_all.21 = bf16[32,24,128]{2,1,0:T(8,128)(2,1)S(1)} all-to-all(bf16[32,24,128]{2,1,0:T(8,128)(2,1)S(1)} %bitcast.35), channel_id=1, replica_groups=mesh['z'=8,'x'=4,'y'=8,'c'=2] {'z','x'}, dimensions={0} | all-to-all | bytes 393216 | tf_op jit(solution)/shard_map/all_to_all | solution.py:411
  59.4 3.9 %collective-permute-start.2 = (bf16[776,128]{1,0:T(8,128)(2,1)S(1)}, bf16[776,128]{1,0:T(8,128)(2,1)S(1)}, u32[]{:S(2)}, u32[]{:S(2)}) collective-permute-start(bf16[776,128]{1,0:T(8,128)(2,1)S(1)} %shard_map.167.block_ref), channel_id=1, source_target_pairs={{0,1},{1,0},{2,3},{3,2},{4,5},{5,4},{6,7},{7,6},{8,9},{9,8},{10,11... | collective-permute-start | bytes 595976 | tf_op jit(solution)/shard_map/ppermute | solution.py:391
  64.4 2.1 %collective-permute-start.4 = (bf16[2,776,128]{2,1,0:T(8,128)(2,1)S(1)}, bf16[2,776,128]{2,1,0:T(8,128)(2,1)}, u32[]{:S(2)}, u32[]{:S(2)}) collective-permute-start(bf16[2,776,128]{2,1,0:T(8,128)(2,1)S(1)} %shard_map.168.own_ref), channel_id=1, source_target_pairs={{0,4},{1,13},{2,6},{3,15},{4,8},{5,1},{6,10},{7,3},{8,12},{9,5},{1... | collective-permute-start | bytes 1191944 | tf_op jit(solution)/shard_map/ppermute | solution.py:399
  66.5 2.2 %collective-permute-start.3 = (bf16[2,776,128]{2,1,0:T(8,128)(2,1)S(1)}, bf16[2,776,128]{2,1,0:T(8,128)(2,1)}, u32[]{:S(2)}, u32[]{:S(2)}) collective-permute-start(bf16[2,776,128]{2,1,0:T(8,128)(2,1)S(1)} %shard_map.168.own_ref), channel_id=1, source_target_pairs={{0,2},{1,15},{2,4},{3,1},{4,6},{5,3},{6,8},{7,5},{8,10},{9,7},{10,... | collective-permute-start | bytes 1191944 | tf_op jit(solution)/shard_map/ppermute | solution.py:399
  68.7 2.8 %collective-permute-start.8 = (bf16[2048,384]{1,0:T(8,128)(2,1)}, bf16[2048,384]{1,0:T(8,128)(2,1)}, u32[]{:S(2)}, u32[]{:S(2)}) collective-permute-start(bf16[2048,384]{1,0:T(8,128)(2,1)} %bitcast.9.gate_ref), channel_id=1, source_target_pairs={{0,1},{1,0},{2,3},{3,2},{4,5},{5,4},{6,7},{7,6},{8,9},{9,8},{10,11... | collective-permute-start | bytes 4718600 | tf_op jit(solution)/shard_map/ppermute | solution.py:391
  71.5 1.9 %collective-permute-start.9 = (bf16[2048,384]{1,0:T(8,128)(2,1)}, bf16[2048,384]{1,0:T(8,128)(2,1)}, u32[]{:S(2)}, u32[]{:S(2)}) collective-permute-start(bf16[2048,384]{1,0:T(8,128)(2,1)} %bitcast.10.up_ref), channel_id=1, source_target_pairs={{0,1},{1,0},{2,3},{3,2},{4,5},{5,4},{6,7},{7,6},{8,9},{9,8},{10,11... | collective-permute-start | bytes 4718600 | tf_op jit(solution)/shard_map/ppermute | solution.py:391
  73.5 2.4 %collective-permute-start.10 = (bf16[384,2048]{1,0:T(8,128)(2,1)S(1)}, bf16[384,2048]{1,0:T(8,128)(2,1)S(1)}, u32[]{:S(2)}, u32[]{:S(2)}) collective-permute-start(bf16[384,2048]{1,0:T(8,128)(2,1)S(1)} %bitcast.30), channel_id=1, source_target_pairs={{0,1},{1,0},{2,3},{3,2},{4,5},{5,4},{6,7},{7,6},{8,9},{9,8},{10,11... | collective-permute-start | bytes 4718600 | tf_op jit(solution)/shard_map/ppermute | solution.py:391
  75.9 2.6 %collective-permute-done.4 = bf16[2,776,128]{2,1,0:T(8,128)(2,1)} collective-permute-done((bf16[2,776,128]{2,1,0:T(8,128)(2,1)S(1)}, bf16[2,776,128]{2,1,0:T(8,128)(2,1)}, u32[]{:S(2)}, u32[]{:S(2)}) %collective-permute-start.4) | collective-permute-done | bytes 397344 | tf_op jit(solution)/shard_map/ppermute | solution.py:399
  78.5 1.9 %collective-permute-start.5 = (bf16[2,776,128]{2,1,0:T(8,128)(2,1)}, bf16[2,776,128]{2,1,0:T(8,128)(2,1)S(1)}, u32[]{:S(2)}, u32[]{:S(2)}) collective-permute-start(bf16[2,776,128]{2,1,0:T(8,128)(2,1)} %collective-permute-done.4), channel_id=1, source_target_pairs={{0,2},{1,15},{2,4},{3,1},{4,6},{5,3},{6,8},{7,5},{8,10},{9,7},{10,... | collective-permute-start | bytes 1191944 | tf_op jit(solution)/shard_map/ppermute | solution.py:399
  81.7 3.7 %collective-permute-start.6 = (bf16[1,776,128]{2,1,0:T(8,128)(2,1)S(1)}, bf16[1,776,128]{2,1,0:T(8,128)(2,1)S(1)}, u32[]{:S(2)}, u32[]{:S(2)}) collective-permute-start(bf16[1,776,128]{2,1,0:T(8,128)(2,1)S(1)} %slice_select_fusion.1), channel_id=1, source_target_pairs={{0,4},{1,13},{2,6},{3,15},{4,8},{5,1},{6,10},{7,3},{8,12},{9,5},{1... | collective-permute-start | bytes 595976 | tf_op jit(solution)/shard_map/ppermute | solution.py:399
  87.5 1.3 collective-permute-done.5
  88.9 1.6 collective-permute-done.6
  90.6 6.6 %collective-permute-start.7 = (bf16[7,392,128]{2,1,0:T(8,128)(2,1)S(1)}, bf16[7,392,128]{2,1,0:T(8,128)(2,1)S(1)}, u32[]{:S(2)}, u32[]{:S(2)}) collective-permute-start(bf16[7,392,128]{2,1,0:T(8,128)(2,1)S(1)} %pad_maximum_fusion), channel_id=1, source_target_pairs={{0,1},{1,0},{2,3},{3,2},{4,5},{5,4},{6,7},{7,6},{8,9},{9,8},{10,11... | collective-permute-start | bytes 2107400 | tf_op jit(solution)/shard_map/ppermute | solution.py:391
  97.2 1.7 collective-permute-done.7.other_ref
  99.0 8.6 %shard_map.169 = (bf16[2,384,384]{2,1,0:T(8,128)(2,1)S(1)}, bf16[8,384,128]{2,1,0:T(8,128)(2,1)S(1)}, f32[8,128]{1,0:T(8,128)S(1)}) custom-call(bf16[2,776,128]{2,1,0:T(8,128)(2,1)S(1)} %shard_map.168.own_ref, bf16[7,776,128]{2,1,0:T(8,128)(2,1)S(1)} %constant_dynamic-update-slice_fusion.mine_ref, bf16[7,392,128]{2,1,0:T(8,128)(2,1)S(1)} %collective-permute-done.7.other_ref, ...), custom_call_target="tpu_custom_call" | custom-call | flops 3019898880 | bytes 14000000 | tf_op jit(solution)/shard_map/pallas_call | solution.py:513
  107.5 2.3 %collective-permute-start.11 = (bf16[8,384,128]{2,1,0:T(8,128)(2,1)S(1)}, bf16[8,384,128]{2,1,0:T(8,128)(2,1)S(1)}, u32[]{:S(2)}, u32[]{:S(2)}) collective-permute-start(bf16[8,384,128]{2,1,0:T(8,128)(2,1)S(1)} %get-tuple-element.19), channel_id=1, source_target_pairs={{0,1},{1,0},{2,3},{3,2},{4,5},{5,4},{6,7},{7,6},{8,9},{9,8},{10,11... | collective-permute-start | bytes 2359304 | tf_op jit(solution)/shard_map/ppermute | solution.py:391
  111.9 3.3 %collective-permute-start.13 = (bf16[2,768,128]{2,1,0:T(8,128)(2,1)S(1)}, bf16[2,768,128]{2,1,0:T(8,128)(2,1)S(1)}, u32[]{:S(2)}, u32[]{:S(2)}) collective-permute-start(bf16[2,768,128]{2,1,0:T(8,128)(2,1)S(1)} %maximum_select_fusion.2), channel_id=1, source_target_pairs={{0,2},{1,15},{2,4},{3,1},{4,6},{5,3},{6,8},{7,5},{8,10},{9,7},{10,... | collective-permute-start | bytes 1179656 | tf_op jit(solution)/shard_map/ppermute | solution.py:399
  115.2 1.9 %collective-permute-start.14 = (bf16[1,768,128]{2,1,0:T(8,128)(2,1)S(1)}, bf16[1,768,128]{2,1,0:T(8,128)(2,1)S(1)}, u32[]{:S(2)}, u32[]{:S(2)}) collective-permute-start(bf16[1,768,128]{2,1,0:T(8,128)(2,1)S(1)} %maximum_select_fusion.3), channel_id=1, source_target_pairs={{0,4},{1,13},{2,6},{3,15},{4,8},{5,1},{6,10},{7,3},{8,12},{9,5},{1... | collective-permute-start | bytes 589832 | tf_op jit(solution)/shard_map/ppermute | solution.py:399
  117.3 2.6 %collective-permute-start.12 = (bf16[2,768,128]{2,1,0:T(8,128)(2,1)S(1)}, bf16[2,768,128]{2,1,0:T(8,128)(2,1)S(1)}, u32[]{:S(2)}, u32[]{:S(2)}) collective-permute-start(bf16[2,768,128]{2,1,0:T(8,128)(2,1)S(1)} %maximum_select_fusion), channel_id=1, source_target_pairs={{0,2},{1,15},{2,4},{3,1},{4,6},{5,3},{6,8},{7,5},{8,10},{9,7},{10,... | collective-permute-start | bytes 1179656 | tf_op jit(solution)/shard_map/ppermute | solution.py:399
  119.9 7.0 %collective-permute-done.14 = bf16[1,768,128]{2,1,0:T(8,128)(2,1)S(1)} collective-permute-done((bf16[1,768,128]{2,1,0:T(8,128)(2,1)S(1)}, bf16[1,768,128]{2,1,0:T(8,128)(2,1)S(1)}, u32[]{:S(2)}, u32[]{:S(2)}) %collective-permute-start.14) | collective-permute-done | bytes 196640 | tf_op jit(solution)/shard_map/ppermute | solution.py:399
  127.2 3.2 %collective-permute-start.15 = (bf16[2,768,128]{2,1,0:T(8,128)(2,1)S(1)}, bf16[2,768,128]{2,1,0:T(8,128)(2,1)S(1)}, u32[]{:S(2)}, u32[]{:S(2)}) collective-permute-start(bf16[2,768,128]{2,1,0:T(8,128)(2,1)S(1)} %add_convert_fusion), channel_id=1, source_target_pairs={{0,4},{1,13},{2,6},{3,15},{4,8},{5,1},{6,10},{7,3},{8,12},{9,5},{1... | collective-permute-start | bytes 1179656 | tf_op jit(solution)/shard_map/ppermute | solution.py:399
  130.4 9.2 %collective-permute-done.15 = bf16[2,768,128]{2,1,0:T(8,128)(2,1)S(1)} collective-permute-done((bf16[2,768,128]{2,1,0:T(8,128)(2,1)S(1)}, bf16[2,768,128]{2,1,0:T(8,128)(2,1)S(1)}, u32[]{:S(2)}, u32[]{:S(2)}) %collective-permute-start.15) | collective-permute-done | bytes 393248 | tf_op jit(solution)/shard_map/ppermute | solution.py:399
  139.8 7.2 %collective-permute-start.16 = (bf16[768,128]{1,0:T(8,128)(2,1)S(1)}, bf16[768,128]{1,0:T(8,128)(2,1)S(1)}, u32[]{:S(2)}, u32[]{:S(2)}) collective-permute-start(bf16[768,128]{1,0:T(8,128)(2,1)S(1)} %fusion.2), channel_id=1, source_target_pairs={{0,1},{1,0},{2,3},{3,2},{4,5},{5,4},{6,7},{7,6},{8,9},{9,8},{10,11... | collective-permute-start | bytes 589832 | tf_op jit(solution)/shard_map/ppermute | solution.py:391
  148.1 13.9 %all_to_all.22 = bf16[32,24,128]{2,1,0:T(8,128)(2,1)S(1)} all-to-all(bf16[32,24,128]{2,1,0:T(8,128)(2,1)S(1)} %bitcast.45), channel_id=1, replica_groups=mesh['z'=8,'x'=4,'y'=8,'c'=2] {'z','x'}, dimensions={0} | all-to-all | bytes 393216 | tf_op jit(solution)/shard_map/all_to_all | solution.py:411
  162.6 12.2 %all_to_all.23.stats_ref = f32[16,8,128]{2,1,0:T(8,128)S(1)} all-to-all(f32[16,8,128]{2,1,0:T(8,128)S(1)} %get-tuple-element.23), channel_id=1, replica_groups=mesh['z'=8,'x'=4,'y'=8,'c'=2] {'y','c'}, dimensions={0} | all-to-all | bytes 131072 | tf_op jit(solution)/shard_map/all_to_all | solution.py:407
  (66 shorter events, 12.7 us)
Async XLA Ops:
  0.0 33.7 %copy-start.3 = (bf16[256,128]{1,0:T(8,128)(2,1)S(1)}, bf16[256,128]{1,0:T(8,128)(2,1)}, u32[]{:S(2)}) copy-start(bf16[256,128]{1,0:T(8,128)(2,1)} %residual_ref.1) | copy-start | bytes 196612
  0.0 33.7 %copy-start.7 = (s32[256,2]{0,1:T(2,128)S(1)}, s32[256,2]{0,1:T(2,128)}, u32[]{:S(2)}) copy-start(s32[256,2]{0,1:T(2,128)} %param.27) | copy-start | bytes 6148
  0.0 33.7 %copy-start.6 = (f32[1024]{0:T(1024)S(1)}, f32[1024]{0:T(1024)}, u32[]{:S(2)}) copy-start(f32[1024]{0:T(1024)} %param.23) | copy-start | bytes 12292
  1.5 6.6 %collective-permute-start = (bf16[136,256]{1,0:T(8,128)(2,1)}, bf16[136,256]{1,0:T(8,128)(2,1)S(1)}, u32[]{:S(2)}, u32[]{:S(2)}) collective-permute-start(bf16[136,256]{1,0:T(8,128)(2,1)} %shard_map.163), channel_id=1, source_target_pairs={{0,16},{16,32},{32,48},{48,64},{64,80},{80,96},{96,112},{112,128},... | collective-permute-start | bytes 208904 | tf_op jit(solution)/shard_map/ppermute | solution.py:464
  8.1 0.9 copy-start.2
  27.7 45.8 %copy-start = (bf16[1,384,2048]{2,1,0:T(8,128)(2,1)S(1)}, bf16[1,384,2048]{2,1,0:T(8,128)(2,1)}, u32[]{:S(2)}) copy-start(bf16[1,384,2048]{2,1,0:T(8,128)(2,1)} %param.31) | copy-start | bytes 4718596
  27.7 6.0 %collective-permute-start.1 = (bf16[8,144,128]{2,1,0:T(8,128)(2,1)S(1)}, bf16[8,144,128]{2,1,0:T(8,128)(2,1)S(1)}, u32[]{:S(2)}, u32[]{:S(2)}) collective-permute-start(bf16[8,144,128]{2,1,0:T(8,128)(2,1)S(1)} %all_to_all.20.mine_ref), channel_id=1, source_target_pairs={{0,1},{1,0},{2,3},{3,2},{4,5},{5,4},{6,7},{7,6},{8,9},{9,8},{10,11... | collective-permute-start | bytes 884744 | tf_op jit(solution)/shard_map/ppermute | solution.py:391
  33.7 1.0 copy-start.1
  35.8 37.7 %copy-start.4 = (f32[2,2048]{1,0:T(2,128)}, f32[2,2048]{1,0:T(2,128)S(1)}, u32[]{:S(2)}) copy-start(f32[2,2048]{1,0:T(2,128)S(1)} %get-tuple-element.17.affine_ref) | copy-start | bytes 49156
  35.8 37.7 %copy-start.12 = (f32[256,128]{1,0:T(8,128)}, f32[256,128]{1,0:T(8,128)S(1)}, u32[]{:S(2)}) copy-start(f32[256,128]{1,0:T(8,128)S(1)} %get-tuple-element.20.first_ref) | copy-start | bytes 393220
  59.4 4.9 %collective-permute-start.2 = (bf16[776,128]{1,0:T(8,128)(2,1)S(1)}, bf16[776,128]{1,0:T(8,128)(2,1)S(1)}, u32[]{:S(2)}, u32[]{:S(2)}) collective-permute-start(bf16[776,128]{1,0:T(8,128)(2,1)S(1)} %shard_map.167.block_ref), channel_id=1, source_target_pairs={{0,1},{1,0},{2,3},{3,2},{4,5},{5,4},{6,7},{7,6},{8,9},{9,8},{10,11... | collective-permute-start | bytes 595976 | tf_op jit(solution)/shard_map/ppermute | solution.py:391
  64.4 14.2 %collective-permute-start.4 = (bf16[2,776,128]{2,1,0:T(8,128)(2,1)S(1)}, bf16[2,776,128]{2,1,0:T(8,128)(2,1)}, u32[]{:S(2)}, u32[]{:S(2)}) collective-permute-start(bf16[2,776,128]{2,1,0:T(8,128)(2,1)S(1)} %shard_map.168.own_ref), channel_id=1, source_target_pairs={{0,4},{1,13},{2,6},{3,15},{4,8},{5,1},{6,10},{7,3},{8,12},{9,5},{1... | collective-permute-start | bytes 1191944 | tf_op jit(solution)/shard_map/ppermute | solution.py:399
  66.5 15.2 %collective-permute-start.3 = (bf16[2,776,128]{2,1,0:T(8,128)(2,1)S(1)}, bf16[2,776,128]{2,1,0:T(8,128)(2,1)}, u32[]{:S(2)}, u32[]{:S(2)}) collective-permute-start(bf16[2,776,128]{2,1,0:T(8,128)(2,1)S(1)} %shard_map.168.own_ref), channel_id=1, source_target_pairs={{0,2},{1,15},{2,4},{3,1},{4,6},{5,3},{6,8},{7,5},{8,10},{9,7},{10,... | collective-permute-start | bytes 1191944 | tf_op jit(solution)/shard_map/ppermute | solution.py:399
  68.7 28.5 %collective-permute-start.8 = (bf16[2048,384]{1,0:T(8,128)(2,1)}, bf16[2048,384]{1,0:T(8,128)(2,1)}, u32[]{:S(2)}, u32[]{:S(2)}) collective-permute-start(bf16[2048,384]{1,0:T(8,128)(2,1)} %bitcast.9.gate_ref), channel_id=1, source_target_pairs={{0,1},{1,0},{2,3},{3,2},{4,5},{5,4},{6,7},{7,6},{8,9},{9,8},{10,11... | collective-permute-start | bytes 4718600 | tf_op jit(solution)/shard_map/ppermute | solution.py:391
  71.5 25.7 %collective-permute-start.9 = (bf16[2048,384]{1,0:T(8,128)(2,1)}, bf16[2048,384]{1,0:T(8,128)(2,1)}, u32[]{:S(2)}, u32[]{:S(2)}) collective-permute-start(bf16[2048,384]{1,0:T(8,128)(2,1)} %bitcast.10.up_ref), channel_id=1, source_target_pairs={{0,1},{1,0},{2,3},{3,2},{4,5},{5,4},{6,7},{7,6},{8,9},{9,8},{10,11... | collective-permute-start | bytes 4718600 | tf_op jit(solution)/shard_map/ppermute | solution.py:391
  73.5 23.7 %collective-permute-start.10 = (bf16[384,2048]{1,0:T(8,128)(2,1)S(1)}, bf16[384,2048]{1,0:T(8,128)(2,1)S(1)}, u32[]{:S(2)}, u32[]{:S(2)}) collective-permute-start(bf16[384,2048]{1,0:T(8,128)(2,1)S(1)} %bitcast.30), channel_id=1, source_target_pairs={{0,1},{1,0},{2,3},{3,2},{4,5},{5,4},{6,7},{7,6},{8,9},{9,8},{10,11... | collective-permute-start | bytes 4718600 | tf_op jit(solution)/shard_map/ppermute | solution.py:391
  78.5 10.3 %collective-permute-start.5 = (bf16[2,776,128]{2,1,0:T(8,128)(2,1)}, bf16[2,776,128]{2,1,0:T(8,128)(2,1)S(1)}, u32[]{:S(2)}, u32[]{:S(2)}) collective-permute-start(bf16[2,776,128]{2,1,0:T(8,128)(2,1)} %collective-permute-done.4), channel_id=1, source_target_pairs={{0,2},{1,15},{2,4},{3,1},{4,6},{5,3},{6,8},{7,5},{8,10},{9,7},{10,... | collective-permute-start | bytes 1191944 | tf_op jit(solution)/shard_map/ppermute | solution.py:399
  81.7 8.8 %collective-permute-start.6 = (bf16[1,776,128]{2,1,0:T(8,128)(2,1)S(1)}, bf16[1,776,128]{2,1,0:T(8,128)(2,1)S(1)}, u32[]{:S(2)}, u32[]{:S(2)}) collective-permute-start(bf16[1,776,128]{2,1,0:T(8,128)(2,1)S(1)} %slice_select_fusion.1), channel_id=1, source_target_pairs={{0,4},{1,13},{2,6},{3,15},{4,8},{5,1},{6,10},{7,3},{8,12},{9,5},{1... | collective-permute-start | bytes 595976 | tf_op jit(solution)/shard_map/ppermute | solution.py:399
  90.5 8.5 %copy-start.5 = (f32[2,2048]{1,0:T(2,128)S(1)}, f32[2,2048]{1,0:T(2,128)}, u32[]{:S(2)}) copy-start(f32[2,2048]{1,0:T(2,128)} %copy-done.4) | copy-start | bytes 49156
  90.6 8.3 %collective-permute-start.7 = (bf16[7,392,128]{2,1,0:T(8,128)(2,1)S(1)}, bf16[7,392,128]{2,1,0:T(8,128)(2,1)S(1)}, u32[]{:S(2)}, u32[]{:S(2)}) collective-permute-start(bf16[7,392,128]{2,1,0:T(8,128)(2,1)S(1)} %pad_maximum_fusion), channel_id=1, source_target_pairs={{0,1},{1,0},{2,3},{3,2},{4,5},{5,4},{6,7},{7,6},{8,9},{9,8},{10,11... | collective-permute-start | bytes 2107400 | tf_op jit(solution)/shard_map/ppermute | solution.py:391
  107.5 4.2 %collective-permute-start.11 = (bf16[8,384,128]{2,1,0:T(8,128)(2,1)S(1)}, bf16[8,384,128]{2,1,0:T(8,128)(2,1)S(1)}, u32[]{:S(2)}, u32[]{:S(2)}) collective-permute-start(bf16[8,384,128]{2,1,0:T(8,128)(2,1)S(1)} %get-tuple-element.19), channel_id=1, source_target_pairs={{0,1},{1,0},{2,3},{3,2},{4,5},{5,4},{6,7},{7,6},{8,9},{9,8},{10,11... | collective-permute-start | bytes 2359304 | tf_op jit(solution)/shard_map/ppermute | solution.py:391
  111.9 15.1 %collective-permute-start.13 = (bf16[2,768,128]{2,1,0:T(8,128)(2,1)S(1)}, bf16[2,768,128]{2,1,0:T(8,128)(2,1)S(1)}, u32[]{:S(2)}, u32[]{:S(2)}) collective-permute-start(bf16[2,768,128]{2,1,0:T(8,128)(2,1)S(1)} %maximum_select_fusion.2), channel_id=1, source_target_pairs={{0,2},{1,15},{2,4},{3,1},{4,6},{5,3},{6,8},{7,5},{8,10},{9,7},{10,... | collective-permute-start | bytes 1179656 | tf_op jit(solution)/shard_map/ppermute | solution.py:399
  115.2 11.7 %collective-permute-start.14 = (bf16[1,768,128]{2,1,0:T(8,128)(2,1)S(1)}, bf16[1,768,128]{2,1,0:T(8,128)(2,1)S(1)}, u32[]{:S(2)}, u32[]{:S(2)}) collective-permute-start(bf16[1,768,128]{2,1,0:T(8,128)(2,1)S(1)} %maximum_select_fusion.3), channel_id=1, source_target_pairs={{0,4},{1,13},{2,6},{3,15},{4,8},{5,1},{6,10},{7,3},{8,12},{9,5},{1... | collective-permute-start | bytes 589832 | tf_op jit(solution)/shard_map/ppermute | solution.py:399
  117.3 13.1 %collective-permute-start.12 = (bf16[2,768,128]{2,1,0:T(8,128)(2,1)S(1)}, bf16[2,768,128]{2,1,0:T(8,128)(2,1)S(1)}, u32[]{:S(2)}, u32[]{:S(2)}) collective-permute-start(bf16[2,768,128]{2,1,0:T(8,128)(2,1)S(1)} %maximum_select_fusion), channel_id=1, source_target_pairs={{0,2},{1,15},{2,4},{3,1},{4,6},{5,3},{6,8},{7,5},{8,10},{9,7},{10,... | collective-permute-start | bytes 1179656 | tf_op jit(solution)/shard_map/ppermute | solution.py:399
  127.2 12.4 %collective-permute-start.15 = (bf16[2,768,128]{2,1,0:T(8,128)(2,1)S(1)}, bf16[2,768,128]{2,1,0:T(8,128)(2,1)S(1)}, u32[]{:S(2)}, u32[]{:S(2)}) collective-permute-start(bf16[2,768,128]{2,1,0:T(8,128)(2,1)S(1)} %add_convert_fusion), channel_id=1, source_target_pairs={{0,4},{1,13},{2,6},{3,15},{4,8},{5,1},{6,10},{7,3},{8,12},{9,5},{1... | collective-permute-start | bytes 1179656 | tf_op jit(solution)/shard_map/ppermute | solution.py:399
  139.6 22.4 %copy-start.10 = (f32[128]{0:T(128)S(1)}, f32[128]{0:T(128)}, u32[]{:S(2)}) copy-start(f32[128]{0:T(128)} %param.25) | copy-start | bytes 1540
  139.7 22.4 %copy-start.11 = (f32[128]{0:T(128)S(1)}, f32[128]{0:T(128)}, u32[]{:S(2)}) copy-start(f32[128]{0:T(128)} %param.26) | copy-start | bytes 1540
  139.7 22.4 %copy-start.13 = (f32[256,128]{1,0:T(8,128)S(1)}, f32[256,128]{1,0:T(8,128)}, u32[]{:S(2)}) copy-start(f32[256,128]{1,0:T(8,128)} %copy-done.12) | copy-start | bytes 393220
  139.7 22.4 %copy-start.14 = (f32[256,2]{0,1:T(2,128)S(1)}, f32[256,2]{0,1:T(2,128)}, u32[]{:S(2)}) copy-start(f32[256,2]{0,1:T(2,128)} %param.28) | copy-start | bytes 6148
  139.7 35.1 %copy-start.8 = (f32[128]{0:T(128)S(1)}, f32[128]{0:T(128)}, u32[]{:S(2)}) copy-start(f32[128]{0:T(128)} %param.32) | copy-start | bytes 1540
  139.7 35.1 %copy-start.9 = (f32[128]{0:T(128)S(1)}, f32[128]{0:T(128)}, u32[]{:S(2)}) copy-start(f32[128]{0:T(128)} %param.33) | copy-start | bytes 1540
  139.8 8.3 %collective-permute-start.16 = (bf16[768,128]{1,0:T(8,128)(2,1)S(1)}, bf16[768,128]{1,0:T(8,128)(2,1)S(1)}, u32[]{:S(2)}, u32[]{:S(2)}) collective-permute-start(bf16[768,128]{1,0:T(8,128)(2,1)S(1)} %fusion.2), channel_id=1, source_target_pairs={{0,1},{1,0},{2,3},{3,2},{4,5},{5,4},{6,7},{7,6},{8,9},{9,8},{10,11... | collective-permute-start | bytes 589832 | tf_op jit(solution)/shard_map/ppermute | solution.py:391
